TPU v7x, 32 devices: a whole 2x2x4 slice. The times are simulated.
32 devices in a mesh: grp: 2 (over y), sp: 4 (over z), tp: 4 (over x, core).
Axes of the slice: x: 2, y: 2, z: 4, core: 2. Of those that a mesh axis runs over, the one named last changes fastest.
Arguments:
- latent: bfloat16 [12288, 2048], P(('grp', 'sp')), parts along dimension 0, may hold values from -6 to 6
- condition: bfloat16 [4096], P('grp'), parts along dimension 0, may hold values from -6 to 6
- context_tokens: bfloat16 [512, 2048], P(('grp', 'sp')), parts along dimension 0, may hold values from -6 to 6
- context_condition: bfloat16 [2048], replicated, may hold values from -6 to 6
- shift_weight: bfloat16 [2048, 2048], P('sp', 'tp'), may hold values from -0.25 to 0.25
- scale_weight: bfloat16 [2048, 2048], P('sp', 'tp'), may hold values from -0.25 to 0.25
- gate_weight: bfloat16 [2048, 2048], P('sp', 'tp'), may hold values from -0.25 to 0.25
- norm_gain: bfloat16 [2048], replicated, may hold values from 0.099609375 to 1.8984375
- query_weight: bfloat16 [2048, 1024], P(None, 'tp'), may hold values from -0.125 to 0.125
- key_weight: bfloat16 [2048, 1024], P(None, 'tp'), may hold values from -0.125 to 0.125
- value_weight: bfloat16 [2048, 1024], P(None, 'tp'), may hold values from -0.125 to 0.125
- out_weight: bfloat16 [1024, 2048], replicated, may hold values from -0.1875 to 0.1875
- offset_bias: float32 [16, 15, 31], P('tp'), may hold values from 0.5 to 260
Outputs:
- mixed_latent: bfloat16 [12288, 2048], P(('grp', 'sp', 'tp')), parts along dimension 0
There are 2 independent parts, one for each index of `grp`. A program takes and returns all parts, laid end to end along the dimension named above; an argument that names none is the same for every part. Nothing has to cross between parts.
All inputs are finite; a program needn't handle non-finite values.
Results may differ from a plain program's by a relative error of at most 0.011.
Values may be sent and summed in bfloat16 or wider, within the bound.
No kernel may reach another device: no remote copies, remote signals or barrier semaphores. Data moves between devices by JAX's collectives and lax.ppermute only.
A program may use at most 192 MiB of HBM per device.

v0:
```python
import functools
import math

import jax
import jax.numpy as jnp
from jax import lax
from jax.experimental import pallas as pl
from jax.experimental.pallas import tpu as pltpu
from jax.sharding import PartitionSpec as P

HEAD_DIM = 64
GRID_W = 64
WIN_ROWS = 8
WIN_COLS = 16
ROW_OFFSETS = 2 * WIN_ROWS - 1
COL_OFFSETS = 2 * WIN_COLS - 1
LANES = 128
HALO_ROWS = WIN_ROWS // 2
TILE = HALO_ROWS * GRID_W
NEAR = WIN_ROWS * GRID_W
ONES = 16

epsilon = 1e-06
masked_score = -1e30
log2e = math.log2(math.e)
SMEM = pltpu.SMEM
VMEM = pltpu.VMEM
f32 = jnp.float32
bf16 = jnp.bfloat16


def shift_along(block, axis, step):
    count = lax.axis_size(axis)
    return lax.ppermute(block, axis, [(i, (i + step) % count) for i in range(count)])


HBM = pltpu.HBM


def whole(memory_space=VMEM):
    return pl.BlockSpec(memory_space=memory_space)


def call(kernel, out_shape, *, vmem=16 << 20, flops=0, **kwargs):
    cost = pl.CostEstimate(flops=flops, transcendentals=0, bytes_accessed=0)
    return pl.pallas_call(
        kernel,
        out_shape=out_shape,
        compiler_params=pltpu.CompilerParams(vmem_limit_bytes=vmem),
        cost_estimate=cost if flops else None,
        **kwargs,
    )


def in_hbm(values):
    return [pltpu.with_memory_space_constraint(value, HBM) for value in values]


def array(shape, dtype=bf16):
    return jax.ShapeDtypeStruct(tuple(shape), dtype)


def modulation_kernel(sp_ref, tp_ref, gain_in_ref, *refs):
    inputs, (out_ref, spot_ref, gain_ref, cond_ref, ctx_ref, weights_ref, sems) = refs[:5], refs[5:]
    spot_ref[0] = sp_ref[0]
    spot_ref[1] = tp_ref[0]
    rows = weights_ref.shape[1]
    part = pl.ds(pl.multiple_of(sp_ref[0] * rows, LANES), rows)
    copies = [
        pltpu.make_async_copy(inputs[0].at[:, part], cond_ref, sems.at[0]),
        pltpu.make_async_copy(inputs[1].at[:, part], ctx_ref, sems.at[1]),
    ]
    copies += [
        pltpu.make_async_copy(inputs[2 + i], weights_ref.at[i], sems.at[2 + i]) for i in range(3)
    ]
    for copy in copies:
        copy.start()

    def act(ref):
        v = ref[...].astype(f32)
        return (v / (1.0 + jnp.exp(-v))).astype(bf16)

    copies[0].wait()
    copies[1].wait()
    both = jnp.concatenate([act(cond_ref), act(ctx_ref), jnp.zeros((14, rows), bf16)], axis=0)
    for index in range(3):
        copies[2 + index].wait()
        terms = jnp.dot(both, weights_ref[index], preferred_element_type=f32)
        out_ref[2 * index : 2 * index + 2, :] = terms[0:2]
    out_ref[6:8, :] = jnp.zeros_like(out_ref[6:8, :])
    gain_ref[...] = gain_in_ref[...].astype(f32)


def modulation_terms(sp_index, tp_index, gain, condition, context_condition, *weights):
    rows, width = weights[0].shape
    return call(
        modulation_kernel,
        [array((8, width), f32), array((2,), jnp.int32), array(gain.shape, f32)],
        in_specs=[whole(SMEM)] * 2 + [whole()] + [whole(HBM)] * 5,
        out_specs=[whole(), whole(SMEM), whole()],
        scratch_shapes=[
            VMEM((1, rows), bf16),
            VMEM((1, rows), bf16),
            VMEM((3, rows, width), bf16),
            pltpu.SemaphoreType.DMA((5,)),
        ],
    )(sp_index, tp_index, gain, *in_hbm((condition.reshape(1, -1), context_condition.reshape(1, -1), *weights)))


def sum_kernel(token_ref, *refs):
    total = refs[0][...]
    for ref in refs[1:-1]:
        total += ref[...]
    refs[-1][...] = total


def summed_terms(token, partials):
    return call(
        sum_kernel,
        array(partials[0].shape, f32),
        in_specs=[whole()] * (1 + len(partials)),
        out_specs=whole(),
    )(token, *partials)


def stage_kernel(token_ref, bias_ref, latent_ref, *refs):
    weights, targets = refs[:3], refs[3:-3]
    table_ref, lines_ref, sems = refs[-3:]
    tiles = len(targets) - 3
    sources = [latent_ref.at[i * TILE : (i + 1) * TILE] for i in range(tiles)]
    sources = [*sources[:1], *sources[-1:], *weights, *sources[1:-1]]
    targets = [targets[0], targets[tiles - 1], *targets[tiles:], *targets[1 : tiles - 1]]
    copies = [
        pltpu.make_async_copy(source, target, sems.at[index])
        for index, (source, target) in enumerate(zip(sources, targets))
    ]
    for copy in copies:
        copy.start()
    heads = bias_ref.shape[0]
    lane = lax.broadcasted_iota(jnp.int32, (ROW_OFFSETS + 1, LANES), 1)
    for head in range(heads):
        lines_ref[:, :] = jnp.zeros_like(lines_ref)
        lines_ref[0:ROW_OFFSETS, 0:COL_OFFSETS] = bias_ref[head] * log2e
        lines = lines_ref[...]
        first = pltpu.roll(lines, LANES - (WIN_COLS - 1), 1)
        second = pltpu.roll(lines, GRID_W - (WIN_COLS - 1), 1)
        for pair in range((ROW_OFFSETS + 1) // 2):
            line = first[2 * pair : 2 * pair + 1] + second[2 * pair + 1 : 2 * pair + 2]
            line = jnp.broadcast_to(line, (GRID_W, LANES))
            table_ref[head * GRID_W : (head + 1) * GRID_W, pair * LANES : (pair + 1) * LANES] = (
                pltpu.roll(line, 0, 1, stride=1, stride_axis=0)
            )
    for copy in copies:
        copy.wait()


def flip_kernel(token_ref, table_ref, out_ref):
    width = table_ref.shape[0]
    key = lax.broadcasted_iota(jnp.int32, (LANES, LANES), 0) % GRID_W
    query = lax.broadcasted_iota(jnp.int32, (LANES, LANES), 1) % GRID_W
    first = jnp.clip(query - WIN_COLS // 2, 0, GRID_W - WIN_COLS)
    inside = (key >= first) & (key < first + WIN_COLS)
    for row in range((ROW_OFFSETS + 1) // 2):
        for col in range(width // LANES):
            rows, cols = slice(row * LANES, (row + 1) * LANES), slice(col * LANES, (col + 1) * LANES)
            out_ref[rows, cols] = jnp.where(inside, table_ref[cols, rows].T, masked_score)


def staged(token, offset_bias, latent, *weights):
    heads = offset_bias.shape[0]
    rows = (ROW_OFFSETS + 1) * GRID_W
    tiles = latent.shape[0] // TILE
    sources = (latent, *weights)
    out = call(
        stage_kernel,
        [array((TILE, latent.shape[1]))] * tiles
        + [array(weight.shape) for weight in weights]
        + [array((heads * HEAD_DIM, rows), f32)],
        in_specs=[whole(), whole()] + [whole(HBM)] * len(sources),
        out_specs=[whole()] * (tiles + len(weights) + 1),
        scratch_shapes=[
            VMEM((ROW_OFFSETS + 1, LANES), f32),
            pltpu.SemaphoreType.DMA((tiles + len(weights),)),
        ],
        flops=5_000_000_000,
    )(token, offset_bias, *in_hbm(sources))
    return out[:tiles], out[tiles:-1], out[-1]


def bias_table(token, rows):
    return call(
        flip_kernel,
        array(rows.shape[::-1], f32),
        in_specs=[whole()] * 2,
        out_specs=whole(),
        flops=1_000_000_000,
    )(token, rows)


def modulators(tp, pieces, gain_ref, scale_row, shift_row, a_ref, b_ref):
    width = pieces[0].shape[1]
    count = len(pieces)
    for step, piece in enumerate(pieces):
        owner = lax.rem(tp - step + count, count)
        part = pl.ds(pl.multiple_of(owner * width, LANES), width)
        a_ref[:, part] = gain_ref[:, part] * (1.0 + piece[scale_row : scale_row + 1, :])
        b_ref[:, part] = piece[shift_row : shift_row + 1, :]


def modulated(x, a, b):
    values = x.astype(f32)
    inverse = lax.rsqrt(jnp.mean(values * values, axis=-1, keepdims=True) + epsilon)
    return ((values * inverse) * a + b).astype(bf16)


query_factor = log2e * HEAD_DIM ** (-0.5)


def edge_kernel(count, spot_ref, first_x_ref, last_x_ref, gain_ref, wq_ref, wk_ref, wv_ref, *rest):
    pieces = rest[:count]
    q_ref, low_ref, high_ref, a_ref, b_ref, first_ref, second_ref = rest[count:]
    modulators(spot_ref[1], pieces, gain_ref, 2, 0, a_ref, b_ref)
    scratch = (first_ref, second_ref)
    outs = (low_ref, high_ref)
    for x_ref, ref in zip((first_x_ref, last_x_ref), scratch):
        ref[...] = modulated(x_ref[...], a_ref[...], b_ref[...])
    for ref, out_ref in zip(scratch, outs):
        out_ref[0] = jnp.dot(ref[...], wk_ref[...], preferred_element_type=f32).astype(bf16)
        out_ref[1] = jnp.dot(ref[...], wv_ref[...], preferred_element_type=f32).astype(bf16)
    for index, ref in enumerate(scratch):
        queries = jnp.dot(ref[...], wq_ref[...], preferred_element_type=f32)
        q_ref[index * TILE : (index + 1) * TILE] = (queries * query_factor).astype(bf16)


def edge_projections(spot, first, last, gain, weights, pieces):
    width = first.shape[1]
    out = weights[0].shape[1]
    return call(
        functools.partial(edge_kernel, len(pieces)),
        [
            array((2 * TILE, out)),
            array((2, TILE, out)),
            array((2, TILE, out)),
            array((1, width), f32),
            array((1, width), f32),
        ],
        in_specs=[whole(SMEM)] + [whole()] * (6 + len(pieces)),
        out_specs=[whole()] * 5,
        scratch_shapes=[VMEM((TILE, width), bf16), VMEM((TILE, width), bf16)],
        flops=2_000_000_000,
    )(spot, first, last, gain, *weights, *pieces)


def main_kernel(count, spot_ref, a_ref, b_ref, gain_ref, wq_ref, wk_ref, wv_ref, qe_ref, low_ref, high_ref, *rest):
    inner, rest = rest[: count[2]], rest[count[2] :]
    contexts, pieces = rest[: count[0]], rest[count[0] : count[0] + count[1]]
    q_ref, k_ref, v_ref, kc_ref, vc_ref, ac_ref, bc_ref, *scratch = rest[sum(count[:2]) :]
    tokens, width = k_ref.shape
    tiles = tokens // TILE
    modulators(spot_ref[1], pieces, gain_ref, 3, 1, ac_ref, bc_ref)

    def load(index):
        ref = scratch[index % 2]
        if index < tiles - 1:
            ref[...] = modulated(inner[index - 1][...], a_ref[...], b_ref[...])
        else:
            height = contexts[0].shape[0]
            for part, context in enumerate(contexts):
                ref[part * height : (part + 1) * height] = modulated(
                    context[...], ac_ref[...], bc_ref[...]
                )

    def values_at(start, values):
        turned = values.T
        v_ref[0, 0:width, start : start + TILE] = turned.astype(bf16)
        rolled = pltpu.roll(turned, TILE - GRID_W, 1).astype(bf16)
        v_ref[1, 0:width, start : start + TILE - GRID_W] = rolled[:, 0 : TILE - GRID_W]
        if start:
            v_ref[1, 0:width, start - GRID_W : start] = rolled[:, TILE - GRID_W :]

    def multiply(index):
        hidden = scratch[index % 2][...]
        keys = jnp.dot(hidden, wk_ref[...], preferred_element_type=f32).astype(bf16)
        values = jnp.dot(hidden, wv_ref[...], preferred_element_type=f32)
        if index < tiles - 1:
            rows = slice(index * TILE, (index + 1) * TILE)
            queries = jnp.dot(hidden, wq_ref[...], preferred_element_type=f32)
            q_ref[rows] = (queries * query_factor).astype(bf16)
            k_ref[rows] = keys
            values_at(index * TILE, values)
        else:
            far = kc_ref.shape[0]
            kc_ref[...] = keys[0:far]
            vc_ref[0:width, :] = values[0:far].T.astype(bf16)

    load(1)
    q_ref[0:TILE] = qe_ref[0:TILE]
    q_ref[tokens - TILE :] = qe_ref[TILE:]
    k_ref[0:TILE] = low_ref[0]
    k_ref[tokens - TILE :] = high_ref[0]
    v_ref[0, width:, :] = jnp.ones((ONES, tokens), bf16)
    v_ref[1, width:, :] = jnp.ones((ONES, tokens), bf16)
    vc_ref[width:, :] = jnp.ones((ONES, vc_ref.shape[1]), bf16)
    values_at(0, low_ref[1].astype(f32))
    for index in range(1, tiles):
        if index + 1 < tiles:
            load(index + 1)
        multiply(index)
    values_at(tokens - TILE, high_ref[1].astype(f32))
    v_ref[1, 0:width, tokens - GRID_W :] = jnp.zeros((width, GRID_W), bf16)


def main_projections(spot, inner, a, b, gain, weights, edges, contexts, pieces):
    width = inner[0].shape[1]
    tokens = (len(inner) + 2) * TILE
    out = weights[0].shape[1]
    far = len(contexts) * contexts[0].shape[0]
    return call(
        functools.partial(main_kernel, (len(contexts), len(pieces), len(inner))),
        [
            array((tokens, out)),
            array((tokens, out)),
            array((2, out + ONES, tokens)),
            array((far, out)),
            array((out + ONES, far)),
        ],
        in_specs=[whole(SMEM)] + [whole()] * (9 + len(inner) + len(contexts) + len(pieces)),
        out_specs=[whole()] * 5,
        scratch_shapes=[
            VMEM((1, width), f32),
            VMEM((1, width), f32),
            VMEM((TILE, width), bf16),
            VMEM((TILE, width), bf16),
        ],
        flops=5_000_000_000,
    )(spot, a, b, gain, *weights, *edges, *inner, *contexts, *pieces)


def attend_rows(rows, q_ref, kc_ref, vc_ref, t_ref, out_ref, scores, probs):
    width = q_ref.shape[1]
    heads = width // HEAD_DIM
    lane_head = lax.broadcasted_iota(jnp.int32, (1, width), 1) // HEAD_DIM
    head_mask = [(lane_head == h).astype(f32).astype(bf16) for h in range(heads)]
    lower = lax.broadcasted_iota(jnp.int32, (HEAD_DIM, LANES), 1) < GRID_W
    dims = (((1,), (1,)), ((), ()))

    def score(index):
        row, k_ref, _, start, offset = rows[index]
        s_ref = scores[index % len(scores)]
        q = q_ref[row * GRID_W : (row + 1) * GRID_W, :]
        big = jnp.concatenate([q * mask for mask in head_mask], axis=0)
        keys = k_ref[part(start * GRID_W, GRID_W, NEAR), :]
        near = lax.dot_general(keys, big, dims, preferred_element_type=f32)
        near += t_ref[part(offset * GRID_W, GRID_W, NEAR), :]
        far = lax.dot_general(kc_ref[...], big, dims, preferred_element_type=f32)
        s_ref[0:NEAR, :] = near
        s_ref[NEAR:, :] = far
        return jnp.maximum(
            jnp.max(near, axis=0, keepdims=True), jnp.max(far, axis=0, keepdims=True)
        )

    def weigh(index, peak):
        s_ref, p_ref = scores[index % len(scores)], probs[index % len(probs)]
        p_ref[...] = jnp.exp2(s_ref[...] - peak).astype(bf16)

    def gather(index):
        _, _, v_ref, start, _ = rows[index]
        p_ref = probs[index % len(probs)]
        values = v_ref[start % 2, :, part(start // 2 * LANES, LANES, NEAR)]
        out = jnp.dot(values, p_ref[0:NEAR, :], preferred_element_type=f32)
        out += jnp.dot(vc_ref[...], p_ref[NEAR:, :], preferred_element_type=f32)
        return out[0:width] * (1.0 / out[width : width + 1])

    def store(index, left, right):
        row = rows[index][0]
        lanes = slice(row * GRID_W, row * GRID_W + LANES)
        for pair in range(heads // 2):
            cols = slice(pair * LANES, (pair + 1) * LANES)
            for half in range(2):
                at = slice(pair * LANES + half * HEAD_DIM, pair * LANES + (half + 1) * HEAD_DIM)
                a, b = left[at, cols], right[at, cols]
                if half == 0:
                    b = pltpu.roll(b, GRID_W, 1)
                else:
                    a = pltpu.roll(a, GRID_W, 1)
                out_ref[at, lanes] = jnp.where(lower, a, b).astype(bf16)

    peaks, outs = {}, {}
    for index in range(len(rows) + 2):
        if index < len(rows):
            peaks[index] = score(index)
        if 0 <= index - 1 < len(rows):
            weigh(index - 1, peaks.pop(index - 1))
        if 0 <= index - 2:
            outs[index - 2] = gather(index - 2)
            if (index - 2) % 2:
                store(index - 3, outs.pop(index - 3), outs.pop(index - 2))


def part(start, unit, size):
    if isinstance(start, int):
        return slice(start, start + size)
    return pl.ds(pl.multiple_of(start, unit), size)


def inner_kernel(q_ref, k_ref, v_ref, kc_ref, vc_ref, t_ref, out_ref, *scratch):
    grid_rows = q_ref.shape[0] // GRID_W
    rows = [
        (row, k_ref, v_ref, row - HALO_ROWS, WIN_ROWS - 1 - HALO_ROWS)
        for row in range(HALO_ROWS, grid_rows - HALO_ROWS)
    ]
    attend_rows(rows, q_ref, kc_ref, vc_ref, t_ref, out_ref, scratch[0:2], scratch[2:4])


def outer_kernel(sp_count, spot_ref, done_ref, latent_ref, weight_ref, q_ref, k_ref, v_ref, kc_ref, vc_ref, t_ref, low_ref, high_ref, out_ref, own_ref, held_ref, *rest):
    share, tp_count = own_ref.shape[0], q_ref.shape[0] // own_ref.shape[0]
    aligned = share % LANES == 0
    block_refs, rest = (rest[:tp_count], rest[tp_count:]) if aligned else ((), rest)
    sems, *scratch = rest
    copies = [
        pltpu.make_async_copy(weight_ref, held_ref, sems.at[0]),
        pltpu.make_async_copy(
            latent_ref.at[part(spot_ref[1] * share, GRID_W, share)], own_ref, sems.at[1]
        ),
    ]
    for copy in copies:
        copy.start()
    tokens, width = q_ref.shape
    grid_rows = tokens // GRID_W
    kl_ref, kh_ref, vl_ref, vh_ref = scratch[0:4]
    strip = 3 * TILE
    ones = jnp.ones((ONES, strip), bf16)
    kl_ref[0:TILE] = low_ref[0]
    kl_ref[TILE:] = k_ref[0 : 2 * TILE]
    kh_ref[0 : 2 * TILE] = k_ref[tokens - 2 * TILE :]
    kh_ref[2 * TILE :] = high_ref[0]
    low = low_ref[1].astype(f32).T
    high = high_ref[1].astype(f32).T
    for ref in (vl_ref, vh_ref):
        ref[0, width:, :] = ones
        ref[1, width:, :] = ones
    rolled = pltpu.roll(low, TILE - GRID_W, 1).astype(bf16)
    vl_ref[0, 0:width, 0:TILE] = low.astype(bf16)
    vl_ref[0, 0:width, TILE:] = v_ref[0, 0:width, 0 : 2 * TILE]
    vl_ref[1, 0:width, 0 : TILE - GRID_W] = rolled[:, 0 : TILE - GRID_W]
    first = pltpu.roll(v_ref[0, 0:width, 0:LANES].astype(f32), GRID_W, 1).astype(bf16)
    vl_ref[1, 0:width, TILE - GRID_W : TILE] = first[:, GRID_W:]
    vl_ref[1, 0:width, TILE:] = v_ref[1, 0:width, 0 : 2 * TILE]
    rolled = pltpu.roll(high, TILE - GRID_W, 1).astype(bf16)
    vh_ref[0, 0:width, 0 : 2 * TILE] = v_ref[0, 0:width, tokens - 2 * TILE :]
    vh_ref[0, 0:width, 2 * TILE :] = high.astype(bf16)
    vh_ref[1, 0:width, 0 : 2 * TILE] = v_ref[1, 0:width, tokens - 2 * TILE :]
    vh_ref[1, 0:width, 2 * TILE - GRID_W : 2 * TILE] = rolled[:, TILE - GRID_W :]
    vh_ref[1, 0:width, 2 * TILE : strip - GRID_W] = rolled[:, 0 : TILE - GRID_W]
    vh_ref[1, 0:width, strip - GRID_W :] = jnp.zeros((width, GRID_W), bf16)
    sp = spot_ref[0]
    total = grid_rows * sp_count
    rows = []
    for row in (*range(HALO_ROWS), *range(grid_rows - HALO_ROWS, grid_rows)):
        own = sp * grid_rows
        first = jnp.clip(own + row - HALO_ROWS, 0, total - WIN_ROWS)
        offset = first - (own + row) + WIN_ROWS - 1
        if row < HALO_ROWS:
            rows.append((row, kl_ref, vl_ref, first - own + HALO_ROWS, offset))
        else:
            rows.append((row, kh_ref, vh_ref, first - own - (grid_rows - WIN_ROWS), offset))
    attend_rows(rows, q_ref, kc_ref, vc_ref, t_ref, out_ref, scratch[4:6], scratch[6:8])
    for step, block_ref in enumerate(block_refs):
        target = lax.rem(spot_ref[1] + step, tp_count)
        block_ref[...] = out_ref[:, part(target * share, LANES, share)]
    for copy in copies:
        copy.wait()


def attention_scratch(total, width):
    return [VMEM((total, width), f32)] * 2 + [VMEM((total, width), bf16)] * 2


def inner_attention(queries, keys, values, far_keys, far_values, table):
    tokens, width = queries.shape
    return call(
        inner_kernel,
        array((width, tokens)),
        in_specs=[whole()] * 6,
        out_specs=whole(),
        scratch_shapes=attention_scratch(NEAR + far_keys.shape[0], width),
        flops=6_000_000_000,
    )(queries, keys, values, far_keys, far_values, table)


def outer_attention(spot, latent, weight, done, queries, keys, values, far_keys, far_values, table, low, high):
    tokens, width = queries.shape
    strip = 3 * TILE
    tp_count = lax.axis_size("tp")
    share = tokens // tp_count
    blocks = [array((width, share))] * (tp_count if share % LANES == 0 else 0)
    attended, own, held, *blocks = call(
        functools.partial(outer_kernel, lax.axis_size("sp")),
        [array((width, tokens)), array((share, latent.shape[1])), array(weight.shape), *blocks],
        in_specs=[whole(SMEM), whole()] + [whole(HBM)] * 2 + [whole()] * 8,
        out_specs=[whole()] * (3 + len(blocks)),
        input_output_aliases={1: 0},
        scratch_shapes=[pltpu.SemaphoreType.DMA((2,))]
        + [VMEM((strip, width), bf16)] * 2
        + [VMEM((2, width + ONES, strip), bf16)] * 2
        + attention_scratch(NEAR + far_keys.shape[0], width),
        flops=3_000_000_000,
    )(
        spot,
        done,
        *in_hbm((latent, weight)),
        queries,
        keys,
        values,
        far_keys,
        far_values,
        table,
        low,
        high,
    )
    if not blocks:
        for step in range(tp_count):
            target = lax.rem(spot[1] + step, tp_count)
            blocks.append(lax.dynamic_slice_in_dim(attended, target * share, share, 1))
    return own, held, blocks


def output_kernel(count, spot_ref, x_ref, w_ref, *rest):
    blocks, pieces = rest[:count], rest[count : 2 * count]
    out_ref, gate_ref = rest[2 * count :]
    tp = spot_ref[1]
    height, _ = blocks[0].shape
    dims = (((0,), (0,)), ((), ()))
    tile = w_ref.shape[1] // count
    for index, piece in enumerate(pieces):
        owner = lax.rem(tp - index + count, count)
        gate_ref[:, part(owner * tile, LANES, tile)] = piece[4:5, :]
    for step in range(count):
        cols = slice(step * tile, (step + 1) * tile)
        total = None
        for index, block in enumerate(blocks):
            owner = lax.rem(tp - index + count, count)
            weight = w_ref[part(owner * height, LANES, height), cols]
            term = lax.dot_general(block[...], weight, dims, preferred_element_type=f32)
            total = term if total is None else total + term
        out_ref[:, cols] = (x_ref[:, cols].astype(f32) + gate_ref[:, cols] * total).astype(bf16)


def output(spot, x, weight, blocks, pieces):
    count = len(blocks)
    share = x.shape[0]
    return call(
        functools.partial(output_kernel, count),
        array((share, x.shape[1])),
        in_specs=[whole(SMEM)] + [whole()] * (2 + 2 * count),
        out_specs=whole(),
        scratch_shapes=[VMEM((1, x.shape[1]), f32)],
        flops=2_000_000_000,
    )(spot, x, weight, *blocks, *pieces)


def gathered(block, axis):
    return [block] + [shift_along(block, axis, step) for step in range(1, lax.axis_size(axis))]


def local(
    latent,
    condition,
    context_tokens,
    context_condition,
    shift_weight,
    scale_weight,
    gate_weight,
    norm_gain,
    query_weight,
    key_weight,
    value_weight,
    out_weight,
    offset_bias,
):
    sp_index = lax.axis_index("sp").astype(jnp.int32).reshape(1)
    tp_index = lax.axis_index("tp").astype(jnp.int32).reshape(1)
    gain = norm_gain.reshape(1, -1)
    terms, spot, gain = modulation_terms(
        sp_index, tp_index, gain, condition, context_condition, shift_weight, scale_weight, gate_weight
    )
    partials = gathered(terms, "sp")
    tiles, weights, rows = staged(
        terms, offset_bias, latent, query_weight, key_weight, value_weight
    )
    summed = summed_terms(rows, partials)
    pieces = gathered(summed, "tp")
    table = bias_table(summed, rows)
    context_tokens, summed = lax.optimization_barrier((context_tokens, summed))
    contexts = gathered(context_tokens, "sp")
    *edges, a, b = edge_projections(spot, tiles[0], tiles[-1], gain, weights, pieces)
    count = lax.axis_size("sp")
    from_left = lax.ppermute(edges[2], "sp", [(i, i + 1) for i in range(count - 1)])
    from_right = lax.ppermute(edges[1], "sp", [(i + 1, i) for i in range(count - 1)])
    fields = main_projections(spot, tiles[1:-1], a, b, gain, weights, edges, contexts, pieces)
    inner = inner_attention(*fields, table)
    own, wo, blocks = outer_attention(
        spot, latent, out_weight, inner, *fields, table, from_left, from_right
    )
    received = blocks[:1] + [
        shift_along(block, "tp", step) for step, block in enumerate(blocks) if step
    ]
    return output(spot, own, wo, received, pieces)


def solution(mesh):
    placed = (
        P(("grp", "sp"), None),
        P("grp"),
        P(("grp", "sp"), None),
        P(),
        P("sp", "tp"),
        P("sp", "tp"),
        P("sp", "tp"),
        P(),
        P(None, "tp"),
        P(None, "tp"),
        P(None, "tp"),
        P(),
        P("tp", None, None),
    )
    return jax.shard_map(
        local, mesh=mesh, in_specs=placed, out_specs=P(("grp", "sp", "tp"), None), check_vma=False
    )
```

profile of v0, /device:TPU:9, one launch (start us, length us, event | category | flops | bytes accessed | tf_op | source)
XLA Modules:
  0.0 76.2 jit_solution(5775717322827547327)
XLA Ops:
  0.0 0.7 reshape.17.gain_in_ref
  0.7 1.3 %reshape.18.refs_0_ = bf16[1,2048]{1,0:T(2,128)(2,1)} reshape(bf16[2048]{0:T(1024)(128)(2,1)} %param.14) | data formatting | bytes 8192 | tf_op jit(solution)/shard_map/reshape | solution.py:107
  2.0 1.3 %reshape.19.refs_1_ = bf16[1,2048]{1,0:T(2,128)(2,1)} reshape(bf16[2048]{0:T(1024)(128)(2,1)} %param.16) | data formatting | bytes 8192 | tf_op jit(solution)/shard_map/reshape | solution.py:107
  3.3 2.1 %shard_map.127 = (f32[8,512]{1,0:T(8,128)S(1)}, s32[2]{0:T(128)S(1)}, f32[1,2048]{1,0:T(1,128)S(1)}) custom-call(s32[1]{0:T(128)} %bitcast.sp_ref, s32[1]{0:T(128)} %bitcast.1.tp_ref, bf16[1,2048]{1,0:T(2,128)(2,1)S(1)} %reshape.17.gain_in_ref, bf16[1,2048]{1,0:T(2,128)(2,1)} %reshape.18.refs_0_, bf16[1,2048]{1,0:T(2,128)(2,1)} %reshape.19.refs_1_, ...), custom_call_target="tpu_custom_call" | custom-call | tf_op jit(solution)/shard_map/pallas_call | solution.py:96
  5.4 1.3 %collective-permute-start = (f32[8,512]{1,0:T(8,128)S(1)}, f32[8,512]{1,0:T(8,128)S(1)}, u32[]{:S(2)}, u32[]{:S(2)}) collective-permute-start(f32[8,512]{1,0:T(8,128)S(1)} %get-tuple-element.36.token_ref.refs_0_), channel_id=1, source_target_pairs={{0,4},{4,8},{8,12},{12,0},{1,5},{5,9},{9,13},{13,1},{2,6},{6,10},{... | collective-permute-start | bytes 49160 | tf_op jit(solution)/shard_map/ppermute | solution.py:34
  6.7 1.1 %collective-permute-start.1 = (f32[8,512]{1,0:T(8,128)S(1)}, f32[8,512]{1,0:T(8,128)S(1)}, u32[]{:S(2)}, u32[]{:S(2)}) collective-permute-start(f32[8,512]{1,0:T(8,128)S(1)} %get-tuple-element.36.token_ref.refs_0_), channel_id=1, source_target_pairs={{0,8},{4,12},{8,0},{12,4},{1,9},{5,13},{9,1},{13,5},{2,10},{6,14},... | collective-permute-start | bytes 49160 | tf_op jit(solution)/shard_map/ppermute | solution.py:34
  7.8 1.4 %collective-permute-start.2 = (f32[8,512]{1,0:T(8,128)S(1)}, f32[8,512]{1,0:T(8,128)S(1)}, u32[]{:S(2)}, u32[]{:S(2)}) collective-permute-start(f32[8,512]{1,0:T(8,128)S(1)} %get-tuple-element.36.token_ref.refs_0_), channel_id=1, source_target_pairs={{0,12},{4,0},{8,4},{12,8},{1,13},{5,1},{9,5},{13,9},{2,14},{6,2},{... | collective-permute-start | bytes 49160 | tf_op jit(solution)/shard_map/ppermute | solution.py:34
  9.2 0.8 copy.15.bias_ref
  9.9 4.0 %shard_map.128 = (bf16[256,2048]{1,0:T(8,128)(2,1)S(1)}, bf16[256,2048]{1,0:T(8,128)(2,1)S(1)}, bf16[256,2048]{1,0:T(8,128)(2,1)S(1)}, bf16[256,2048]{1,0:T(8,12...) custom-call(f32[8,512]{1,0:T(8,128)S(1)} %get-tuple-element.36.token, ...), custom_call_target="tpu_custom_call" | custom-call | flops 5000000000 | tf_op jit(solution)/shard_map/pallas_call | solution.py:174
  14.0 0.0 collective-permute-done.refs_1_
  14.0 0.0 collective-permute-done.1.refs_2_
  14.0 2.7 %collective-permute-start.3 = (f32[8,512]{1,0:T(8,128)S(1)}, f32[8,512]{1,0:T(8,128)S(1)}, u32[]{:S(2)}, u32[]{:S(2)}) collective-permute-start(f32[8,512]{1,0:T(8,128)S(1)} %shard_map.129.rest_0_.rest_8_.token_ref.rest_4_), channel_id=1, source_target_pairs={{0,1},{1,2},{2,3},{3,0},{4,5},{5,6},{6,7},{7,4},{8,9},{9,10},{10,1... | collective-permute-start | bytes 49160 | tf_op jit(solution)/shard_map/ppermute | solution.py:34
  16.7 0.3 collective-permute-start.4
  16.9 0.2 collective-permute-start.5
  17.2 3.1 %collective-permute-start.7 = (bf16[64,2048]{1,0:T(8,128)(2,1)S(1)}, bf16[64,2048]{1,0:T(8,128)(2,1)S(1)}, u32[]{:S(2)}, u32[]{:S(2)}) collective-permute-start(bf16[64,2048]{1,0:T(8,128)(2,1)S(1)} %copy-done), channel_id=1, source_target_pairs={{0,8},{4,12},{8,0},{12,4},{1,9},{5,13},{9,1},{13,5},{2,10},{6,14},... | collective-permute-start | bytes 786440 | tf_op jit(solution)/shard_map/ppermute | solution.py:34
  20.3 0.0 collective-permute-done.3.rest_1_.rest_9_.rest_5_
  20.3 0.0 collective-permute-start.8
  20.3 0.3 shard_map.132.t_ref
  20.7 2.8 %shard_map.130 = (bf16[512,256]{1,0:T(8,128)(2,1)S(1)}, bf16[2,256,256]{2,1,0:T(8,128)(2,1)S(1)}, bf16[2,256,256]{2,1,0:T(8,128)(2,1)S(1)}, f32[1,2048]{1,0:T(1,128)S(1)}, f32[1,2048]{1,0:T(1,128)S(1)}) custom-call(s32[2]{0:T(128)S(1)} %get-tuple-element.35.spot_ref, bf16[256,2048]{1,0:T(8,128)(2,1)S(1)} %get-tuple-element.37.first_x_ref, ...), custom_call_target="tpu_custom_call" | custom-call | flops 2000000000 | tf_op jit(solution)/shard_map/pallas_call | solution.py:238
  23.5 3.1 %collective-permute-start.10 = (bf16[2,256,256]{2,1,0:T(8,128)(2,1)S(1)}, bf16[2,256,256]{2,1,0:T(8,128)(2,1)S(1)}, u32[]{:S(2)}, u32[]{:S(2)}) collective-permute-start(bf16[2,256,256]{2,1,0:T(8,128)(2,1)S(1)} %get-tuple-element.47.low_ref), channel_id=1, source_target_pairs={{4,0},{8,4},{12,8},{5,1},{9,5},{13,9},{6,2},{10,6},{14,10},{7,3},{... | collective-permute-start | bytes 786440 | tf_op jit(solution)/shard_map/ppermute | solution.py:599
  26.6 2.4 %collective-permute-start.9 = (bf16[2,256,256]{2,1,0:T(8,128)(2,1)S(1)}, bf16[2,256,256]{2,1,0:T(8,128)(2,1)S(1)}, u32[]{:S(2)}, u32[]{:S(2)}) collective-permute-start(bf16[2,256,256]{2,1,0:T(8,128)(2,1)S(1)} %get-tuple-element.48.high_ref), channel_id=1, source_target_pairs={{0,4},{4,8},{8,12},{1,5},{5,9},{9,13},{2,6},{6,10},{10,14},{3,7},{... | collective-permute-start | bytes 786440 | tf_op jit(solution)/shard_map/ppermute | solution.py:598
  29.0 9.3 %collective-permute-done.7.rest_6_ = bf16[64,2048]{1,0:T(8,128)(2,1)S(1)} collective-permute-done((bf16[64,2048]{1,0:T(8,128)(2,1)S(1)}, bf16[64,2048]{1,0:T(8,128)(2,1)S(1)}, u32[]{:S(2)}, u32[]{:S(2)}) %collective-permute-start.7) | collective-permute-done | bytes 262176 | tf_op jit(solution)/shard_map/ppermute | solution.py:34
  38.3 4.8 %collective-permute-done.8.rest_7_ = bf16[64,2048]{1,0:T(8,128)(2,1)S(1)} collective-permute-done((bf16[64,2048]{1,0:T(8,128)(2,1)S(1)}, bf16[64,2048]{1,0:T(8,128)(2,1)S(1)}, u32[]{:S(2)}, u32[]{:S(2)}) %collective-permute-start.8) | collective-permute-done | bytes 262176 | tf_op jit(solution)/shard_map/ppermute | solution.py:34
  43.0 5.7 %shard_map.131 = (bf16[1536,256]{1,0:T(8,128)(2,1)S(1)}, bf16[1536,256]{1,0:T(8,128)(2,1)S(1)}, bf16[2,272,1536]{2,1,0:T(8,128)(2,1)S(1)}, bf16[256,256]{1,0:T(8,128)(2,1)S(1)}, bf16[272,256]{1,0:T(8,128)(2,1)S(1)}) custom-call(s32[2]{0:T(128)S(1)} %get-tuple-element.35.spot_ref, f32[1,2048]{1,0:T(1,128)S(1)} %get-tuple-element.44.a_ref, ...), custom_call_target="tpu_custom_call" | custom-call | flops 5000000000 | tf_op jit(solution)/shard_map/pallas_call | solution.py:318
  48.8 5.6 %shard_map.133.done_ref = bf16[256,1536]{1,0:T(8,128)(2,1)S(1)} custom-call(bf16[1536,256]{1,0:T(8,128)(2,1)S(1)} %get-tuple-element.54.q_ref, bf16[1536,256]{1,0:T(8,128)(2,1)S(1)} %get-tuple-element.55.k_ref, bf16[2,272,1536]{2,1,0:T(8,128)(2,1)S(1)} %get-tuple-element.56.v_ref, bf16[256,256]{1,0:T(8,128)(2,1)S(1)} %get-tuple-element.57.kc_ref, ...), custom_call_target="tpu_custom_call" | custom-call | flops 6000000000 | tf_op jit(solution)/shard_map/pallas_call | solution.py:481
  54.4 5.9 %shard_map.134 = (bf16[256,1536]{1,0:T(8,128)(2,1)S(1)}, bf16[384,2048]{1,0:T(8,128)(2,1)S(1)}, bf16[1024,2048]{1,0:T(8,128)(2,1)S(1)}, bf16[256,384]{1,0:T(8,12...) custom-call(s32[2]{0:T(128)S(1)} %get-tuple-element.35.spot_ref, ...), custom_call_target="tpu_custom_call", output_to_operand_aliasing={{0}: (1, {})} | custom-call | flops 3000000000 | tf_op jit(solution)/shard_map/pallas_call | solution.py:497
  60.3 2.5 %collective-permute-start.11 = (bf16[256,384]{1,0:T(8,128)(2,1)S(1)}, bf16[256,384]{1,0:T(8,128)(2,1)S(1)}, u32[]{:S(2)}, u32[]{:S(2)}) collective-permute-start(bf16[256,384]{1,0:T(8,128)(2,1)S(1)} %get-tuple-element.62), channel_id=1, source_target_pairs={{0,1},{1,2},{2,3},{3,0},{4,5},{5,6},{6,7},{7,4},{8,9},{9,10},{10,1... | collective-permute-start | bytes 589832 | tf_op jit(solution)/shard_map/ppermute | solution.py:34
  62.8 0.5 collective-permute-start.12
  63.3 3.6 %collective-permute-done.11.rest_1_ = bf16[256,384]{1,0:T(8,128)(2,1)S(1)} collective-permute-done((bf16[256,384]{1,0:T(8,128)(2,1)S(1)}, bf16[256,384]{1,0:T(8,128)(2,1)S(1)}, u32[]{:S(2)}, u32[]{:S(2)}) %collective-permute-start.11) | collective-permute-done | bytes 196640 | tf_op jit(solution)/shard_map/ppermute | solution.py:34
  66.8 5.1 %collective-permute-done.12.rest_2_ = bf16[256,384]{1,0:T(8,128)(2,1)S(1)} collective-permute-done((bf16[256,384]{1,0:T(8,128)(2,1)S(1)}, bf16[256,384]{1,0:T(8,128)(2,1)S(1)}, u32[]{:S(2)}, u32[]{:S(2)}) %collective-permute-start.12) | collective-permute-done | bytes 196640 | tf_op jit(solution)/shard_map/ppermute | solution.py:34
  72.0 0.7 collective-permute-done.13.rest_3_
  72.6 3.5 %shard_map.135 = bf16[384,2048]{1,0:T(8,128)(2,1)} custom-call(s32[2]{0:T(128)S(1)} %get-tuple-element.35.spot_ref, bf16[384,2048]{1,0:T(8,128)(2,1)S(1)} %get-tuple-element.59.x_ref, bf16[1024,2048]{1,0:T(8,128)(2,1)S(1)} %get-tuple-element.60.w_ref, bf16[256,384]{1,0:T(8,128)(2,1)S(1)} %get-tuple-element.61.rest_0_, ...), custom_call_target="tpu_custom_call" | custom-call | flops 2000000000 | tf_op jit(solution)/shard_map/pallas_call | solution.py:552
  (11 shorter events, 0.0 us)
Async XLA Ops:
  5.4 8.6 %collective-permute-start = (f32[8,512]{1,0:T(8,128)S(1)}, f32[8,512]{1,0:T(8,128)S(1)}, u32[]{:S(2)}, u32[]{:S(2)}) collective-permute-start(f32[8,512]{1,0:T(8,128)S(1)} %get-tuple-element.36.token_ref.refs_0_), channel_id=1, source_target_pairs={{0,4},{4,8},{8,12},{12,0},{1,5},{5,9},{9,13},{13,1},{2,6},{6,10},{... | collective-permute-start | bytes 49160 | tf_op jit(solution)/shard_map/ppermute | solution.py:34
  6.7 7.3 %collective-permute-start.1 = (f32[8,512]{1,0:T(8,128)S(1)}, f32[8,512]{1,0:T(8,128)S(1)}, u32[]{:S(2)}, u32[]{:S(2)}) collective-permute-start(f32[8,512]{1,0:T(8,128)S(1)} %get-tuple-element.36.token_ref.refs_0_), channel_id=1, source_target_pairs={{0,8},{4,12},{8,0},{12,4},{1,9},{5,13},{9,1},{13,5},{2,10},{6,14},... | collective-permute-start | bytes 49160 | tf_op jit(solution)/shard_map/ppermute | solution.py:34
  7.8 6.2 %collective-permute-start.2 = (f32[8,512]{1,0:T(8,128)S(1)}, f32[8,512]{1,0:T(8,128)S(1)}, u32[]{:S(2)}, u32[]{:S(2)}) collective-permute-start(f32[8,512]{1,0:T(8,128)S(1)} %get-tuple-element.36.token_ref.refs_0_), channel_id=1, source_target_pairs={{0,12},{4,0},{8,4},{12,8},{1,13},{5,1},{9,5},{13,9},{2,14},{6,2},{... | collective-permute-start | bytes 49160 | tf_op jit(solution)/shard_map/ppermute | solution.py:34
  9.9 7.2 %copy-start = (bf16[64,2048]{1,0:T(8,128)(2,1)S(1)}, bf16[64,2048]{1,0:T(8,128)(2,1)}, u32[]{:S(2)}) copy-start(bf16[64,2048]{1,0:T(8,128)(2,1)} %rest_4_) | copy-start | bytes 786436
  14.0 6.3 %collective-permute-start.3 = (f32[8,512]{1,0:T(8,128)S(1)}, f32[8,512]{1,0:T(8,128)S(1)}, u32[]{:S(2)}, u32[]{:S(2)}) collective-permute-start(f32[8,512]{1,0:T(8,128)S(1)} %shard_map.129.rest_0_.rest_8_.token_ref.rest_4_), channel_id=1, source_target_pairs={{0,1},{1,2},{2,3},{3,0},{4,5},{5,6},{6,7},{7,4},{8,9},{9,10},{10,1... | collective-permute-start | bytes 49160 | tf_op jit(solution)/shard_map/ppermute | solution.py:34
  16.7 4.0 %collective-permute-start.4 = (f32[8,512]{1,0:T(8,128)S(1)}, f32[8,512]{1,0:T(8,128)S(1)}, u32[]{:S(2)}, u32[]{:S(2)}) collective-permute-start(f32[8,512]{1,0:T(8,128)S(1)} %shard_map.129.rest_0_.rest_8_.token_ref.rest_4_), channel_id=1, source_target_pairs={{0,2},{1,3},{2,0},{3,1},{4,6},{5,7},{6,4},{7,5},{8,10},{9,11},{10,... | collective-permute-start | bytes 49160 | tf_op jit(solution)/shard_map/ppermute | solution.py:34
  16.9 3.7 %collective-permute-start.5 = (f32[8,512]{1,0:T(8,128)S(1)}, f32[8,512]{1,0:T(8,128)S(1)}, u32[]{:S(2)}, u32[]{:S(2)}) collective-permute-start(f32[8,512]{1,0:T(8,128)S(1)} %shard_map.129.rest_0_.rest_8_.token_ref.rest_4_), channel_id=1, source_target_pairs={{0,3},{1,0},{2,1},{3,2},{4,7},{5,4},{6,5},{7,6},{8,11},{9,8},{10,9... | collective-permute-start | bytes 49160 | tf_op jit(solution)/shard_map/ppermute | solution.py:34
  17.2 11.8 %collective-permute-start.6 = (bf16[64,2048]{1,0:T(8,128)(2,1)S(1)}, bf16[64,2048]{1,0:T(8,128)(2,1)S(1)}, u32[]{:S(2)}, u32[]{:S(2)}) collective-permute-start(bf16[64,2048]{1,0:T(8,128)(2,1)S(1)} %copy-done), channel_id=1, source_target_pairs={{0,4},{4,8},{8,12},{12,0},{1,5},{5,9},{9,13},{13,1},{2,6},{6,10},{... | collective-permute-start | bytes 786440 | tf_op jit(solution)/shard_map/ppermute | solution.py:34
  17.2 21.1 %collective-permute-start.7 = (bf16[64,2048]{1,0:T(8,128)(2,1)S(1)}, bf16[64,2048]{1,0:T(8,128)(2,1)S(1)}, u32[]{:S(2)}, u32[]{:S(2)}) collective-permute-start(bf16[64,2048]{1,0:T(8,128)(2,1)S(1)} %copy-done), channel_id=1, source_target_pairs={{0,8},{4,12},{8,0},{12,4},{1,9},{5,13},{9,1},{13,5},{2,10},{6,14},... | collective-permute-start | bytes 786440 | tf_op jit(solution)/shard_map/ppermute | solution.py:34
  20.3 22.7 %collective-permute-start.8 = (bf16[64,2048]{1,0:T(8,128)(2,1)S(1)}, bf16[64,2048]{1,0:T(8,128)(2,1)S(1)}, u32[]{:S(2)}, u32[]{:S(2)}) collective-permute-start(bf16[64,2048]{1,0:T(8,128)(2,1)S(1)} %copy-done), channel_id=1, source_target_pairs={{0,12},{4,0},{8,4},{12,8},{1,13},{5,1},{9,5},{13,9},{2,14},{6,2},{... | collective-permute-start | bytes 786440 | tf_op jit(solution)/shard_map/ppermute | solution.py:34
  23.5 30.9 %collective-permute-start.10 = (bf16[2,256,256]{2,1,0:T(8,128)(2,1)S(1)}, bf16[2,256,256]{2,1,0:T(8,128)(2,1)S(1)}, u32[]{:S(2)}, u32[]{:S(2)}) collective-permute-start(bf16[2,256,256]{2,1,0:T(8,128)(2,1)S(1)} %get-tuple-element.47.low_ref), channel_id=1, source_target_pairs={{4,0},{8,4},{12,8},{5,1},{9,5},{13,9},{6,2},{10,6},{14,10},{7,3},{... | collective-permute-start | bytes 786440 | tf_op jit(solution)/shard_map/ppermute | solution.py:599
  26.6 27.8 %collective-permute-start.9 = (bf16[2,256,256]{2,1,0:T(8,128)(2,1)S(1)}, bf16[2,256,256]{2,1,0:T(8,128)(2,1)S(1)}, u32[]{:S(2)}, u32[]{:S(2)}) collective-permute-start(bf16[2,256,256]{2,1,0:T(8,128)(2,1)S(1)} %get-tuple-element.48.high_ref), channel_id=1, source_target_pairs={{0,4},{4,8},{8,12},{1,5},{5,9},{9,13},{2,6},{6,10},{10,14},{3,7},{... | collective-permute-start | bytes 786440 | tf_op jit(solution)/shard_map/ppermute | solution.py:598
  60.3 6.6 %collective-permute-start.11 = (bf16[256,384]{1,0:T(8,128)(2,1)S(1)}, bf16[256,384]{1,0:T(8,128)(2,1)S(1)}, u32[]{:S(2)}, u32[]{:S(2)}) collective-permute-start(bf16[256,384]{1,0:T(8,128)(2,1)S(1)} %get-tuple-element.62), channel_id=1, source_target_pairs={{0,1},{1,2},{2,3},{3,0},{4,5},{5,6},{6,7},{7,4},{8,9},{9,10},{10,1... | collective-permute-start | bytes 589832 | tf_op jit(solution)/shard_map/ppermute | solution.py:34
  62.8 9.2 %collective-permute-start.12 = (bf16[256,384]{1,0:T(8,128)(2,1)S(1)}, bf16[256,384]{1,0:T(8,128)(2,1)S(1)}, u32[]{:S(2)}, u32[]{:S(2)}) collective-permute-start(bf16[256,384]{1,0:T(8,128)(2,1)S(1)} %get-tuple-element.63), channel_id=1, source_target_pairs={{0,2},{1,3},{2,0},{3,1},{4,6},{5,7},{6,4},{7,5},{8,10},{9,11},{10,... | collective-permute-start | bytes 589832 | tf_op jit(solution)/shard_map/ppermute | solution.py:34
  63.3 9.4 %collective-permute-start.13 = (bf16[256,384]{1,0:T(8,128)(2,1)S(1)}, bf16[256,384]{1,0:T(8,128)(2,1)S(1)}, u32[]{:S(2)}, u32[]{:S(2)}) collective-permute-start(bf16[256,384]{1,0:T(8,128)(2,1)S(1)} %get-tuple-element.64), channel_id=1, source_target_pairs={{0,3},{1,0},{2,1},{3,2},{4,7},{5,4},{6,5},{7,6},{8,11},{9,8},{10,9... | collective-permute-start | bytes 589832 | tf_op jit(solution)/shard_map/ppermute | solution.py:34
where the time goes:
time: 76.5 us; the launch traced here: 76.2 us
  Pallas kernels  30 us (39%)
  waiting for transfers between devices  23.4 us (31%)
  starting transfers between devices  18.6 us (24%)
  local copies, waits for them, and re-layouts  4.03 us (5%)
    ppermute x12, waiting for transfers between devices, shift_along(): lax.ppermute(block, axis, [(i, (i + step) % count) for i in range(count)])  23.4 us
    ppermute x12, starting transfers between devices, shift_along(): lax.ppermute(block, axis, [(i, (i + step) % count) for i in range(count)])  13.1 us
    pallas_call x1, Pallas kernels, outer_attention(): call(functools.partial(outer_kernel, lax.axis_size('sp')), [array((width,...  5.89 us
    pallas_call x1, Pallas kernels, main_projections(): call(functools.partial(main_kernel, (len(contexts), len(pieces), len(inne...  5.74 us
    pallas_call x1, Pallas kernels, inner_attention(): call(inner_kernel, array((width, tokens)), in_specs=[whole()] * 6, out_sp...  5.57 us
    pallas_call x1, Pallas kernels, staged(): call(stage_kernel, [array((TILE, latent.shape[1]))] * tiles + [array(weig...  4.02 us
    pallas_call x1, Pallas kernels, output(): call(functools.partial(output_kernel, count), array((share, x.shape[1])),...  3.54 us
    ppermute x1, starting transfers between devices, local(): lax.ppermute(edges[1], 'sp', [(i + 1, i) for i in range(count - 1)])  3.09 us
  transfers between devices with their start and end apart: 14, of which 5 were waited for; matrix products, arithmetic and copies ran while one was open for 1% of the time, Pallas kernels for 24%

commit v1 on v0

v1 whole, which is shorter than its diff:
```python
import functools
import math

import jax
import jax.numpy as jnp
from jax import lax
from jax.experimental import pallas as pl
from jax.experimental.pallas import tpu as pltpu
from jax.sharding import PartitionSpec as P

HEAD_DIM = 64
GRID_W = 64
WIN_ROWS = 8
WIN_COLS = 16
ROW_OFFSETS = 2 * WIN_ROWS - 1
COL_OFFSETS = 2 * WIN_COLS - 1
LANES = 128
HALO_ROWS = WIN_ROWS // 2
TILE = HALO_ROWS * GRID_W
NEAR = WIN_ROWS * GRID_W
ONES = 16

epsilon = 1e-06
masked_score = -1e30
log2e = math.log2(math.e)
VMEM = pltpu.VMEM
f32 = jnp.float32
bf16 = jnp.bfloat16


def shift_along(block, axis, step):
    count = lax.axis_size(axis)
    return lax.ppermute(block, axis, [(i, (i + step) % count) for i in range(count)])


HBM = pltpu.HBM


def exchange(block, axis, step):
    count = lax.axis_size(axis)
    if count & (count - 1):
        return shift_along(block, axis, step)
    return lax.ppermute(block, axis, [(i, i ^ step) for i in range(count)])


def origin(axis, step):
    count = lax.axis_size(axis)
    index = lax.axis_index(axis)
    if count & (count - 1):
        return lax.rem(index - step + count, count)
    return jnp.bitwise_xor(index, step)


def target(axis, step):
    count = lax.axis_size(axis)
    index = lax.axis_index(axis)
    if count & (count - 1):
        return lax.rem(index + step, count)
    return jnp.bitwise_xor(index, step)


def whole(memory_space=VMEM):
    return pl.BlockSpec(memory_space=memory_space)


def call(kernel, out_shape, *, vmem=16 << 20, flops=0, **kwargs):
    cost = pl.CostEstimate(flops=flops, transcendentals=0, bytes_accessed=0)
    return pl.pallas_call(
        kernel,
        out_shape=out_shape,
        compiler_params=pltpu.CompilerParams(vmem_limit_bytes=vmem),
        cost_estimate=cost if flops else None,
        **kwargs,
    )


def in_hbm(values):
    return [pltpu.with_memory_space_constraint(value, HBM) for value in values]


def array(shape, dtype=bf16):
    return jax.ShapeDtypeStruct(tuple(shape), dtype)


def modulation_kernel(*refs):
    inputs, (out_ref, gain_ref, line_ref, cond_ref, ctx_ref, act_ref, weights_ref, sems) = refs[:6], refs[6:]
    rows = weights_ref.shape[1]
    mine = pl.ds(pl.multiple_of(lax.axis_index("sp") * rows, LANES), rows)
    targets = (cond_ref, ctx_ref, *(weights_ref.at[i] for i in range(3)), line_ref)
    copies = [
        pltpu.make_async_copy(source, target, sems.at[index])
        for index, (source, target) in enumerate(zip(inputs, targets))
    ]
    for copy in copies:
        copy.start()

    act_ref[...] = jnp.zeros_like(act_ref)
    for row, ref in enumerate((cond_ref, ctx_ref)):
        copies[row].wait()
        v = ref[...].reshape(1, -1).astype(f32)
        act_ref[row : row + 1, :] = v / (1.0 + jnp.exp(-v))
    both = act_ref[:, mine].astype(bf16)
    for index in range(3):
        copies[2 + index].wait()
        terms = jnp.dot(both, weights_ref[index], preferred_element_type=f32)
        out_ref[2 * index : 2 * index + 2, :] = terms[0:2]
    out_ref[6:8, :] = jnp.zeros_like(out_ref[6:8, :])
    copies[5].wait()
    gain_ref[...] = line_ref[...].reshape(gain_ref.shape).astype(f32)


def modulation_terms(condition, context_condition, *rest):
    rows, width = rest[0].shape
    whole_line = VMEM(condition.shape, bf16)
    return call(
        modulation_kernel,
        [array((8, width), f32), array((1, *rest[-1].shape), f32)],
        in_specs=[whole(HBM)] * 6,
        out_specs=[whole()] * 2,
        scratch_shapes=[
            whole_line,
            whole_line,
            whole_line,
            VMEM((16, *condition.shape), f32),
            VMEM((3, rows, width), bf16),
            pltpu.SemaphoreType.DMA((6,)),
        ],
    )(*in_hbm((condition, context_condition, *rest)))


def sum_kernel(token_ref, *refs):
    total = refs[0][...]
    for ref in refs[1:-1]:
        total += ref[...]
    refs[-1][...] = total


def summed_terms(token, partials):
    return call(
        sum_kernel,
        array(partials[0].shape, f32),
        in_specs=[whole()] * (1 + len(partials)),
        out_specs=whole(),
    )(token, *partials)


def rows_kernel(token_ref, source_ref, *refs):
    table_ref, bias_ref, lines_ref, sems = refs[-4:]
    count = (len(refs) - 4) // 2
    pairs = [(source_ref, bias_ref), *zip(refs[:count], refs[count:-4])]
    copies = [
        pltpu.make_async_copy(source, target, sems.at[index])
        for index, (source, target) in enumerate(pairs)
    ]
    for copy in copies:
        copy.start()
    copies[0].wait()
    heads = bias_ref.shape[1]
    for head in range(heads):
        lines_ref[:, :] = jnp.zeros_like(lines_ref)
        lines_ref[0:ROW_OFFSETS, 0:COL_OFFSETS] = bias_ref[:, head, :] * log2e
        lines = lines_ref[...]
        first = pltpu.roll(lines, LANES - (WIN_COLS - 1), 1)
        second = pltpu.roll(lines, GRID_W - (WIN_COLS - 1), 1)
        for pair in range((ROW_OFFSETS + 1) // 2):
            line = first[2 * pair : 2 * pair + 1] + second[2 * pair + 1 : 2 * pair + 2]
            line = jnp.broadcast_to(line, (GRID_W, LANES))
            table_ref[head * GRID_W : (head + 1) * GRID_W, pair * LANES : (pair + 1) * LANES] = (
                pltpu.roll(line, 0, 1, stride=1, stride_axis=0)
            )
    for copy in copies[1:]:
        copy.wait()


def bias_rows(token, offset_bias, *weights):
    heads = offset_bias.shape[0]
    rows = (ROW_OFFSETS + 1) * GRID_W
    return call(
        rows_kernel,
        [array(weight.shape) for weight in weights] + [array((heads * HEAD_DIM, rows), f32)],
        in_specs=[whole()] + [whole(HBM)] * (1 + len(weights)),
        out_specs=[whole()] * (1 + len(weights)),
        scratch_shapes=[
            VMEM((ROW_OFFSETS, heads, COL_OFFSETS), f32),
            VMEM((ROW_OFFSETS + 1, LANES), f32),
            pltpu.SemaphoreType.DMA((1 + len(weights),)),
        ],
        flops=500_000_000,
    )(token, *in_hbm((jnp.transpose(offset_bias, (1, 0, 2)), *weights)))


def flip_kernel(token_ref, table_ref, out_ref):
    width = table_ref.shape[0]
    key = lax.broadcasted_iota(jnp.int32, (LANES, LANES), 0) % GRID_W
    query = lax.broadcasted_iota(jnp.int32, (LANES, LANES), 1) % GRID_W
    first = jnp.clip(query - WIN_COLS // 2, 0, GRID_W - WIN_COLS)
    inside = (key >= first) & (key < first + WIN_COLS)
    for row in range((ROW_OFFSETS + 1) // 2):
        for col in range(width // LANES):
            rows, cols = slice(row * LANES, (row + 1) * LANES), slice(col * LANES, (col + 1) * LANES)
            out_ref[rows, cols] = jnp.where(inside, table_ref[cols, rows].T, masked_score)


def bias_table(token, rows):
    return call(
        flip_kernel,
        array(rows.shape[::-1], f32),
        in_specs=[whole()] * 2,
        out_specs=whole(),
        flops=1_000_000_000,
    )(token, rows)


def modulators(pieces, gain_ref, scale_row, shift_row, a_ref, b_ref):
    width = pieces[0].shape[1]
    for step, piece in enumerate(pieces):
        owner = origin("tp", step)
        part = pl.ds(pl.multiple_of(owner * width, LANES), width)
        a_ref[:, part] = gain_ref[:, part] * (1.0 + piece[scale_row : scale_row + 1, :])
        b_ref[:, part] = piece[shift_row : shift_row + 1, :]


def modulated(x, a, b):
    values = x.astype(f32)
    inverse = lax.rsqrt(jnp.mean(values * values, axis=-1, keepdims=True) + epsilon)
    return ((values * inverse) * a + b).astype(bf16)


query_factor = log2e * HEAD_DIM ** (-0.5)


def edge_kernel(count, x_ref, context_ref, gain_ref, wq_ref, wk_ref, wv_ref, *rest):
    pieces = rest[:count]
    q_ref, low_ref, high_ref, even_ref, odd_ref, far_ref, a_ref, b_ref, ac_ref, bc_ref, first_ref, second_ref = rest[count:]
    modulators(pieces, gain_ref, 3, 1, ac_ref, bc_ref)
    hidden = modulated(context_ref[...], ac_ref[...], bc_ref[...])
    far_ref[0] = jnp.dot(hidden, wk_ref[...], preferred_element_type=f32).astype(bf16)
    far_ref[1] = jnp.dot(hidden, wv_ref[...], preferred_element_type=f32).astype(bf16)
    modulators(pieces, gain_ref, 2, 0, a_ref, b_ref)
    scratch = (first_ref, second_ref)
    outs = (low_ref, high_ref)
    tokens = x_ref.shape[0]
    for start, ref in zip((0, tokens - TILE), scratch):
        ref[...] = modulated(x_ref[start : start + TILE], a_ref[...], b_ref[...])
    for ref, out_ref in zip(scratch, outs):
        out_ref[0] = jnp.dot(ref[...], wk_ref[...], preferred_element_type=f32).astype(bf16)
        out_ref[1] = jnp.dot(ref[...], wv_ref[...], preferred_element_type=f32).astype(bf16)
    even = lax.axis_index("sp") % 2 == 0
    even_ref[...] = jnp.where(even, high_ref[...], low_ref[...])
    odd_ref[...] = jnp.where(even, low_ref[...], high_ref[...])
    for index, ref in enumerate(scratch):
        queries = jnp.dot(ref[...], wq_ref[...], preferred_element_type=f32)
        q_ref[index * TILE : (index + 1) * TILE] = (queries * query_factor).astype(bf16)


def edge_projections(latent, context, gain, weights, pieces):
    width = latent.shape[1]
    out = weights[0].shape[1]
    return call(
        functools.partial(edge_kernel, len(pieces)),
        [
            array((2 * TILE, out)),
            *[array((2, TILE, out))] * 4,
            array((2, context.shape[0], out)),
            array((1, width), f32),
            array((1, width), f32),
        ],
        in_specs=[whole()] * (6 + len(pieces)),
        out_specs=[whole()] * 8,
        scratch_shapes=[
            VMEM((1, width), f32),
            VMEM((1, width), f32),
            VMEM((TILE, width), bf16),
            VMEM((TILE, width), bf16),
        ],
        flops=2_000_000_000,
    )(latent, context, gain, *weights, *pieces)


def main_kernel(x_ref, a_ref, b_ref, wq_ref, wk_ref, wv_ref, qe_ref, low_ref, high_ref, *rest):
    q_ref, k_ref, v_ref, *scratch = rest
    tokens, width = k_ref.shape
    tiles = tokens // TILE

    def load(index):
        rows = slice(index * TILE, (index + 1) * TILE)
        scratch[index % 2][...] = modulated(x_ref[rows], a_ref[...], b_ref[...])

    def values_at(start, values):
        turned = values.T
        v_ref[0, 0:width, start : start + TILE] = turned.astype(bf16)
        rolled = pltpu.roll(turned, TILE - GRID_W, 1).astype(bf16)
        v_ref[1, 0:width, start : start + TILE - GRID_W] = rolled[:, 0 : TILE - GRID_W]
        if start:
            v_ref[1, 0:width, start - GRID_W : start] = rolled[:, TILE - GRID_W :]

    def multiply(index):
        hidden = scratch[index % 2][...]
        keys = jnp.dot(hidden, wk_ref[...], preferred_element_type=f32).astype(bf16)
        values = jnp.dot(hidden, wv_ref[...], preferred_element_type=f32)
        rows = slice(index * TILE, (index + 1) * TILE)
        queries = jnp.dot(hidden, wq_ref[...], preferred_element_type=f32)
        q_ref[rows] = (queries * query_factor).astype(bf16)
        k_ref[rows] = keys
        values_at(index * TILE, values)

    load(1)
    q_ref[0:TILE] = qe_ref[0:TILE]
    q_ref[tokens - TILE :] = qe_ref[TILE:]
    k_ref[0:TILE] = low_ref[0]
    k_ref[tokens - TILE :] = high_ref[0]
    v_ref[0, width:, :] = jnp.ones((ONES, tokens), bf16)
    v_ref[1, width:, :] = jnp.ones((ONES, tokens), bf16)
    values_at(0, low_ref[1].astype(f32))
    for index in range(1, tiles - 1):
        if index + 2 < tiles:
            load(index + 1)
        multiply(index)
    values_at(tokens - TILE, high_ref[1].astype(f32))
    v_ref[1, 0:width, tokens - GRID_W :] = jnp.zeros((width, GRID_W), bf16)


def main_projections(latent, a, b, weights, edges):
    tokens, width = latent.shape
    out = weights[0].shape[1]
    return call(
        main_kernel,
        [array((tokens, out)), array((tokens, out)), array((2, out + ONES, tokens))],
        in_specs=[whole()] * 9,
        out_specs=[whole()] * 3,
        scratch_shapes=[VMEM((TILE, width), bf16), VMEM((TILE, width), bf16)],
        flops=5_000_000_000,
    )(latent, a, b, *weights, *edges)


def attend_rows(rows, q_ref, kc_ref, vc_ref, t_ref, out_ref, scores, probs):
    width = q_ref.shape[1]
    heads = width // HEAD_DIM
    lane_head = lax.broadcasted_iota(jnp.int32, (1, width), 1) // HEAD_DIM
    head_mask = [(lane_head == h).astype(f32).astype(bf16) for h in range(heads)]
    lower = lax.broadcasted_iota(jnp.int32, (HEAD_DIM, LANES), 1) < GRID_W
    dims = (((1,), (1,)), ((), ()))

    def score(index):
        row, k_ref, _, start, offset = rows[index]
        s_ref = scores[index % len(scores)]
        q = q_ref[row * GRID_W : (row + 1) * GRID_W, :]
        big = jnp.concatenate([q * mask for mask in head_mask], axis=0)
        keys = k_ref[part(start * GRID_W, GRID_W, NEAR), :]
        near = lax.dot_general(keys, big, dims, preferred_element_type=f32)
        near += t_ref[part(offset * GRID_W, GRID_W, NEAR), :]
        far = lax.dot_general(kc_ref[...], big, dims, preferred_element_type=f32)
        s_ref[0:NEAR, :] = near
        s_ref[NEAR:, :] = far
        return jnp.maximum(
            jnp.max(near, axis=0, keepdims=True), jnp.max(far, axis=0, keepdims=True)
        )

    def weigh(index, peak):
        s_ref, p_ref = scores[index % len(scores)], probs[index % len(probs)]
        p_ref[...] = jnp.exp2(s_ref[...] - peak).astype(bf16)

    def gather(index):
        _, _, v_ref, start, _ = rows[index]
        p_ref = probs[index % len(probs)]
        values = v_ref[start % 2, :, part(start // 2 * LANES, LANES, NEAR)]
        out = jnp.dot(values, p_ref[0:NEAR, :], preferred_element_type=f32)
        out += jnp.dot(vc_ref[...], p_ref[NEAR:, :], preferred_element_type=f32)
        return out[0:width] * (1.0 / out[width : width + 1])

    def store(index, left, right):
        row = rows[index][0]
        lanes = slice(row * GRID_W, row * GRID_W + LANES)
        for pair in range(heads // 2):
            cols = slice(pair * LANES, (pair + 1) * LANES)
            for half in range(2):
                at = slice(pair * LANES + half * HEAD_DIM, pair * LANES + (half + 1) * HEAD_DIM)
                a, b = left[at, cols], right[at, cols]
                if half == 0:
                    b = pltpu.roll(b, GRID_W, 1)
                else:
                    a = pltpu.roll(a, GRID_W, 1)
                out_ref[at, lanes] = jnp.where(lower, a, b).astype(bf16)

    peaks, outs = {}, {}
    for index in range(len(rows) + 2):
        if index < len(rows):
            peaks[index] = score(index)
        if 0 <= index - 1 < len(rows):
            weigh(index - 1, peaks.pop(index - 1))
        if 0 <= index - 2:
            outs[index - 2] = gather(index - 2)
            if (index - 2) % 2:
                store(index - 3, outs.pop(index - 3), outs.pop(index - 2))


def part(start, unit, size):
    if isinstance(start, int):
        return slice(start, start + size)
    return pl.ds(pl.multiple_of(start, unit), size)


def inner_kernel(count, q_ref, k_ref, v_ref, t_ref, *rest):
    contexts, (out_ref, kc_ref, vc_ref, *scratch) = rest[:count], rest[count:]
    width = q_ref.shape[1]
    grid_rows = q_ref.shape[0] // GRID_W
    height = contexts[0].shape[1]
    for index, context in enumerate(contexts):
        kc_ref[index * height : (index + 1) * height] = context[0]
    far_values = jnp.concatenate([context[1] for context in contexts], axis=0)
    vc_ref[0:width, :] = far_values.astype(f32).T.astype(bf16)
    vc_ref[width:, :] = jnp.ones((ONES, vc_ref.shape[1]), bf16)
    rows = [
        (row, k_ref, v_ref, row - HALO_ROWS, WIN_ROWS - 1 - HALO_ROWS)
        for row in range(HALO_ROWS, grid_rows - HALO_ROWS)
    ]
    attend_rows(rows, q_ref, kc_ref, vc_ref, t_ref, out_ref, scratch[0:2], scratch[2:4])


def outer_kernel(sp_count, done_ref, latent_ref, weight_ref, q_ref, k_ref, v_ref, kc_ref, vc_ref, t_ref, first_ref, second_ref, out_ref, own_ref, held_ref, *rest):
    share, tp_count = own_ref.shape[0], q_ref.shape[0] // own_ref.shape[0]
    aligned = share % LANES == 0
    block_refs, rest = (rest[:tp_count], rest[tp_count:]) if aligned else ((), rest)
    sems, *scratch = rest
    copies = [
        pltpu.make_async_copy(weight_ref, held_ref, sems.at[0]),
        pltpu.make_async_copy(
            latent_ref.at[part(lax.axis_index("tp") * share, GRID_W, share)], own_ref, sems.at[1]
        ),
    ]
    for copy in copies:
        copy.start()
    tokens, width = q_ref.shape
    grid_rows = tokens // GRID_W
    kl_ref, kh_ref, vl_ref, vh_ref = scratch[0:4]
    strip = 3 * TILE
    ones = jnp.ones((ONES, strip), bf16)
    even = lax.axis_index("sp") % 2 == 0
    low_halo = jnp.where(even, second_ref[...], first_ref[...])
    high_halo = jnp.where(even, first_ref[...], second_ref[...])
    kl_ref[0:TILE] = low_halo[0]
    kl_ref[TILE:] = k_ref[0 : 2 * TILE]
    kh_ref[0 : 2 * TILE] = k_ref[tokens - 2 * TILE :]
    kh_ref[2 * TILE :] = high_halo[0]
    low = low_halo[1].astype(f32).T
    high = high_halo[1].astype(f32).T
    for ref in (vl_ref, vh_ref):
        ref[0, width:, :] = ones
        ref[1, width:, :] = ones
    rolled = pltpu.roll(low, TILE - GRID_W, 1).astype(bf16)
    vl_ref[0, 0:width, 0:TILE] = low.astype(bf16)
    vl_ref[0, 0:width, TILE:] = v_ref[0, 0:width, 0 : 2 * TILE]
    vl_ref[1, 0:width, 0 : TILE - GRID_W] = rolled[:, 0 : TILE - GRID_W]
    first = pltpu.roll(v_ref[0, 0:width, 0:LANES].astype(f32), GRID_W, 1).astype(bf16)
    vl_ref[1, 0:width, TILE - GRID_W : TILE] = first[:, GRID_W:]
    vl_ref[1, 0:width, TILE:] = v_ref[1, 0:width, 0 : 2 * TILE]
    rolled = pltpu.roll(high, TILE - GRID_W, 1).astype(bf16)
    vh_ref[0, 0:width, 0 : 2 * TILE] = v_ref[0, 0:width, tokens - 2 * TILE :]
    vh_ref[0, 0:width, 2 * TILE :] = high.astype(bf16)
    vh_ref[1, 0:width, 0 : 2 * TILE] = v_ref[1, 0:width, tokens - 2 * TILE :]
    vh_ref[1, 0:width, 2 * TILE - GRID_W : 2 * TILE] = rolled[:, TILE - GRID_W :]
    vh_ref[1, 0:width, 2 * TILE : strip - GRID_W] = rolled[:, 0 : TILE - GRID_W]
    vh_ref[1, 0:width, strip - GRID_W :] = jnp.zeros((width, GRID_W), bf16)
    sp = lax.axis_index("sp")
    total = grid_rows * sp_count
    rows = []
    for row in (*range(HALO_ROWS), *range(grid_rows - HALO_ROWS, grid_rows)):
        own = sp * grid_rows
        first = jnp.clip(own + row - HALO_ROWS, 0, total - WIN_ROWS)
        offset = first - (own + row) + WIN_ROWS - 1
        if row < HALO_ROWS:
            rows.append((row, kl_ref, vl_ref, first - own + HALO_ROWS, offset))
        else:
            rows.append((row, kh_ref, vh_ref, first - own - (grid_rows - WIN_ROWS), offset))
    attend_rows(rows, q_ref, kc_ref, vc_ref, t_ref, out_ref, scratch[4:6], scratch[6:8])
    for step, block_ref in enumerate(block_refs):
        block_ref[...] = out_ref[:, part(target("tp", step) * share, LANES, share)]
    for copy in copies:
        copy.wait()


def attention_scratch(total, width):
    return [VMEM((total, width), f32)] * 2 + [VMEM((total, width), bf16)] * 2


def inner_attention(queries, keys, values, table, contexts):
    tokens, width = queries.shape
    far = len(contexts) * contexts[0].shape[1]
    return call(
        functools.partial(inner_kernel, len(contexts)),
        [array((width, tokens)), array((far, width)), array((width + ONES, far))],
        in_specs=[whole()] * (4 + len(contexts)),
        out_specs=[whole()] * 3,
        scratch_shapes=attention_scratch(NEAR + far, width),
        flops=6_000_000_000,
    )(queries, keys, values, table, *contexts)


def outer_attention(latent, weight, done, queries, keys, values, far_keys, far_values, table, low, high):
    tokens, width = queries.shape
    strip = 3 * TILE
    tp_count = lax.axis_size("tp")
    share = tokens // tp_count
    blocks = [array((width, share))] * (tp_count if share % LANES == 0 else 0)
    attended, own, held, *blocks = call(
        functools.partial(outer_kernel, lax.axis_size("sp")),
        [array((width, tokens)), array((share, latent.shape[1])), array(weight.shape), *blocks],
        in_specs=[whole()] + [whole(HBM)] * 2 + [whole()] * 8,
        out_specs=[whole()] * (3 + len(blocks)),
        input_output_aliases={0: 0},
        scratch_shapes=[pltpu.SemaphoreType.DMA((2,))]
        + [VMEM((strip, width), bf16)] * 2
        + [VMEM((2, width + ONES, strip), bf16)] * 2
        + attention_scratch(NEAR + far_keys.shape[0], width),
        flops=3_000_000_000,
    )(
        done,
        *in_hbm((latent, weight)),
        queries,
        keys,
        values,
        far_keys,
        far_values,
        table,
        low,
        high,
    )
    if not blocks:
        for step in range(tp_count):
            start = target("tp", step) * share
            blocks.append(lax.dynamic_slice_in_dim(attended, start, share, 1))
    return own, held, blocks


def output_kernel(count, x_ref, w_ref, *rest):
    blocks, pieces = rest[:count], rest[count : 2 * count]
    out_ref, gate_ref = rest[2 * count :]
    height, _ = blocks[0].shape
    dims = (((0,), (0,)), ((), ()))
    tile = w_ref.shape[1] // count
    for index, piece in enumerate(pieces):
        owner = origin("tp", index)
        gate_ref[:, part(owner * tile, LANES, tile)] = piece[4:5, :]
    for step in range(count):
        cols = slice(step * tile, (step + 1) * tile)
        total = None
        for index, block in enumerate(blocks):
            owner = origin("tp", index)
            weight = w_ref[part(owner * height, LANES, height), cols]
            term = lax.dot_general(block[...], weight, dims, preferred_element_type=f32)
            total = term if total is None else total + term
        out_ref[:, cols] = (x_ref[:, cols].astype(f32) + gate_ref[:, cols] * total).astype(bf16)


def output(x, weight, blocks, pieces):
    count = len(blocks)
    share = x.shape[0]
    return call(
        functools.partial(output_kernel, count),
        array((share, x.shape[1])),
        in_specs=[whole()] * (2 + 2 * count),
        out_specs=whole(),
        scratch_shapes=[VMEM((1, x.shape[1]), f32)],
        flops=2_000_000_000,
    )(x, weight, *blocks, *pieces)


def gathered(block, axis):
    return [block] + [exchange(block, axis, step) for step in range(1, lax.axis_size(axis))]


def local(
    latent,
    condition,
    context_tokens,
    context_condition,
    shift_weight,
    scale_weight,
    gate_weight,
    norm_gain,
    query_weight,
    key_weight,
    value_weight,
    out_weight,
    offset_bias,
):
    terms, gain = modulation_terms(
        condition, context_condition, shift_weight, scale_weight, gate_weight, norm_gain
    )
    partials = gathered(terms, "sp")
    *weights, rows = bias_rows(terms, offset_bias, query_weight, key_weight, value_weight)
    summed = summed_terms(rows, partials)
    pieces = gathered(summed, "tp")
    table = bias_table(summed, rows)
    *edges, far, a, b = edge_projections(
        latent, context_tokens, gain, weights, pieces
    )
    count = lax.axis_size("sp")
    contexts = gathered(far, "sp")
    pairs = [(i, i ^ 1) for i in range(count) if i ^ 1 < count]
    first = lax.ppermute(edges[3], "sp", pairs)
    pairs = [(i, j) for i in range(count) for j in [((i + 1) ^ 1) - 1] if 0 <= j < count]
    second = lax.ppermute(edges[4], "sp", pairs)
    fields = main_projections(latent, a, b, weights, edges[:3])
    inner, *fars = inner_attention(*fields, table, contexts)
    own, wo, blocks = outer_attention(
        latent, out_weight, inner, *fields, *fars, table, first, second
    )
    received = blocks[:1] + [
        exchange(block, "tp", step) for step, block in enumerate(blocks) if step
    ]
    return output(own, wo, received, pieces)


def solution(mesh):
    placed = (
        P(("grp", "sp"), None),
        P("grp"),
        P(("grp", "sp"), None),
        P(),
        P("sp", "tp"),
        P("sp", "tp"),
        P("sp", "tp"),
        P(),
        P(None, "tp"),
        P(None, "tp"),
        P(None, "tp"),
        P(),
        P("tp", None, None),
    )
    return jax.shard_map(
        local, mesh=mesh, in_specs=placed, out_specs=P(("grp", "sp", "tp"), None), check_vma=False
    )
```

time: 76.5 us -> 54 us (0.71)
  waiting for transfers between devices: 23.4 us -> 10.9 us
  Pallas kernels: 30 us -> 24.4 us
  local copies, waits for them, and re-layouts: 4.03 us -> 0.01 us
    ppermute x14, waiting for transfers between devices: 23.4 us -> 10.9 us  [the longest x12 10.9 us: exchange(): return lax.ppermute(block, axis, [(i, i ^ step) for i in range(count)])]
    pallas_call x4, Pallas kernels: 17.4 us -> 13.1 us  [the longest x1 5.21 us: inner_attention(): call(functools.partial(inner_kernel, len(contexts)), [array((width, token...]
    reshape x3 -> x0, local copies, waits for them, and re-layouts: 3.27 us -> none  [the longest x1 1.29 us: modulation_terms(): condition.reshape(1, -1)]
  transfers between devices with their start and end apart: 14 -> 14, of which waited for: 5 -> 4; matrix products, arithmetic and copies ran while one was open for 1% -> 0% of each run, Pallas kernels for 24% -> 22%
where the time goes in v1:
time: 54 us; the launch traced here: 53.8 us
  Pallas kernels  24.4 us (45%)
  starting transfers between devices  18.4 us (34%)
  waiting for transfers between devices  10.9 us (20%)
    ppermute x12, starting transfers between devices, exchange(): return lax.ppermute(block, axis, [(i, i ^ step) for i in range(count)])  14.3 us
    ppermute x12, waiting for transfers between devices, exchange(): return lax.ppermute(block, axis, [(i, i ^ step) for i in range(count)])  10.9 us
    pallas_call x1, Pallas kernels, outer_attention(): call(functools.partial(outer_kernel, lax.axis_size('sp')), [array((width,...  5.42 us
    pallas_call x1, Pallas kernels, inner_attention(): call(functools.partial(inner_kernel, len(contexts)), [array((width, token...  5.21 us
    pallas_call x1, Pallas kernels, main_projections(): call(main_kernel, [array((tokens, out)), array((tokens, out)), array((2,...  4.31 us
    pallas_call x1, Pallas kernels, output(): call(functools.partial(output_kernel, count), array((share, x.shape[1])),...  3 us
    ppermute x1, starting transfers between devices, local(): second = lax.ppermute(edges[4], 'sp', pairs)  2.6 us
    pallas_call x1, Pallas kernels, edge_projections(): call(functools.partial(edge_kernel, len(pieces)), [array((2 * TILE, out))...  2.49 us
  transfers between devices with their start and end apart: 14, of which 4 were waited for; matrix products, arithmetic and copies ran while one was open for 0% of the time, Pallas kernels for 22%

profile of v1, /device:TPU:9, one launch (start us, length us, event | category | flops | bytes accessed | tf_op | source)
XLA Modules:
  0.0 53.8 jit_solution(15535775772603327650)
XLA Ops:
  0.0 1.7 %shard_map.127 = (f32[8,512]{1,0:T(8,128)S(1)}, f32[1,2048]{1,0:T(1,128)S(1)}) custom-call(bf16[2048]{0:T(1024)(128)(2,1)} %refs_0_.2, bf16[2048]{0:T(1024)(128)(2,1)} %refs_1_.2, bf16[512,512]{1,0:T(8,128)(2,1)} %refs_2_.2, bf16[512,512]{1,0:T(8,128)(2,1)} %refs_3_.1, bf16[512,512]{1,0:T(8,128)(2,1)} %refs_4_.1, bf16[2048]{0:T(1024)(128)(2,1)} %refs_5_.1), custom_call_target="tpu_custom_call" | custom-call | tf_op jit(solution)/shard_map/pallas_call | solution.py:115
  1.7 0.0 copy-start
  1.7 0.0 copy-start.1
  1.7 1.4 %collective-permute-start.2 = (f32[8,512]{1,0:T(8,128)S(1)}, f32[8,512]{1,0:T(8,128)S(1)}, u32[]{:S(2)}, u32[]{:S(2)}) collective-permute-start(f32[8,512]{1,0:T(8,128)S(1)} %get-tuple-element.32.token_ref.refs_0_), channel_id=1, source_target_pairs={{0,12},{4,8},{8,4},{12,0},{1,13},{5,9},{9,5},{13,1},{2,14},{6,10},... | collective-permute-start | bytes 49160 | tf_op jit(solution)/shard_map/ppermute | solution.py:43
  3.1 1.1 %collective-permute-start.1 = (f32[8,512]{1,0:T(8,128)S(1)}, f32[8,512]{1,0:T(8,128)S(1)}, u32[]{:S(2)}, u32[]{:S(2)}) collective-permute-start(f32[8,512]{1,0:T(8,128)S(1)} %get-tuple-element.32.token_ref.refs_0_), channel_id=1, source_target_pairs={{0,8},{4,12},{8,0},{12,4},{1,9},{5,13},{9,1},{13,5},{2,10},{6,14},... | collective-permute-start | bytes 49160 | tf_op jit(solution)/shard_map/ppermute | solution.py:43
  4.2 1.1 %collective-permute-start = (f32[8,512]{1,0:T(8,128)S(1)}, f32[8,512]{1,0:T(8,128)S(1)}, u32[]{:S(2)}, u32[]{:S(2)}) collective-permute-start(f32[8,512]{1,0:T(8,128)S(1)} %get-tuple-element.32.token_ref.refs_0_), channel_id=1, source_target_pairs={{0,4},{4,0},{8,12},{12,8},{1,5},{5,1},{9,13},{13,9},{2,6},{6,2},{1... | collective-permute-start | bytes 49160 | tf_op jit(solution)/shard_map/ppermute | solution.py:43
  5.3 1.9 %shard_map.128 = (bf16[2048,256]{1,0:T(8,128)(2,1)S(1)}, bf16[2048,256]{1,0:T(8,128)(2,1)S(1)}, bf16[2048,256]{1,0:T(8,128)(2,1)S(1)}, f32[256,1024]{1,0:T(8,128)S(1)}) custom-call(f32[8,512]{1,0:T(8,128)S(1)} %get-tuple-element.32.token_ref.refs_0_, f32[15,4,31]{2,1,0:T(4,128)} %bitcast.1, bf16[2048,256]{1,0:T(8,128)(2,1)} %refs_0_.3, ...), custom_call_target="tpu_custom_call" | custom-call | flops 500000000 | tf_op jit(solution)/shard_map/pallas_call | solution.py:178
  7.2 0.0 collective-permute-done.2.refs_3_
  7.2 0.0 collective-permute-done.refs_1_
  7.2 2.9 %collective-permute-start.5 = (f32[8,512]{1,0:T(8,128)S(1)}, f32[8,512]{1,0:T(8,128)S(1)}, u32[]{:S(2)}, u32[]{:S(2)}) collective-permute-start(f32[8,512]{1,0:T(8,128)S(1)} %shard_map.129.rest_0_.token_ref.rest_4_), channel_id=1, source_target_pairs={{0,3},{1,2},{2,1},{3,0},{4,7},{5,6},{6,5},{7,4},{8,11},{9,10},{10,... | collective-permute-start | bytes 49160 | tf_op jit(solution)/shard_map/ppermute | solution.py:43
  10.1 0.1 collective-permute-start.4
  10.2 0.3 collective-permute-start.3
  10.6 0.3 shard_map.132.t_ref
  10.9 0.7 %collective-permute-done.5.rest_3_.rest_7_ = f32[8,512]{1,0:T(8,128)S(1)} collective-permute-done((f32[8,512]{1,0:T(8,128)S(1)}, f32[8,512]{1,0:T(8,128)S(1)}, u32[]{:S(2)}, u32[]{:S(2)}) %collective-permute-start.5) | collective-permute-done | bytes 16416 | tf_op jit(solution)/shard_map/ppermute | solution.py:43
  11.7 1.0 %collective-permute-done.4.rest_2_.rest_6_ = f32[8,512]{1,0:T(8,128)S(1)} collective-permute-done((f32[8,512]{1,0:T(8,128)S(1)}, f32[8,512]{1,0:T(8,128)S(1)}, u32[]{:S(2)}, u32[]{:S(2)}) %collective-permute-start.4) | collective-permute-done | bytes 16416 | tf_op jit(solution)/shard_map/ppermute | solution.py:43
  12.7 0.0 collective-permute-done.3.rest_1_.rest_5_
  12.7 2.5 %shard_map.130 = (bf16[512,256]{1,0:T(8,128)(2,1)S(1)}, bf16[2,256,256]{2,1,0:T(8,128)(2,1)S(1)}, bf16[2,256,256]{2,1,0:T(8,128)(2,1)S(1)}, bf16[2,256,256]{2,1,...) custom-call(bf16[1536,2048]{1,0:T(8,128)(2,1)S(1)} %copy-done, ...), custom_call_target="tpu_custom_call" | custom-call | flops 2000000000 | tf_op jit(solution)/shard_map/pallas_call | solution.py:259
  15.2 2.5 %collective-permute-start.8 = (bf16[2,64,256]{2,1,0:T(8,128)(2,1)S(1)}, bf16[2,64,256]{2,1,0:T(8,128)(2,1)S(1)}, u32[]{:S(2)}, u32[]{:S(2)}) collective-permute-start(bf16[2,64,256]{2,1,0:T(8,128)(2,1)S(1)} %get-tuple-element.45.rest_0_), channel_id=1, source_target_pairs={{0,12},{4,8},{8,4},{12,0},{1,13},{5,9},{9,5},{13,1},{2,14},{6,10},... | collective-permute-start | bytes 196616 | tf_op jit(solution)/shard_map/ppermute | solution.py:43
  17.7 1.6 %collective-permute-start.7 = (bf16[2,64,256]{2,1,0:T(8,128)(2,1)S(1)}, bf16[2,64,256]{2,1,0:T(8,128)(2,1)S(1)}, u32[]{:S(2)}, u32[]{:S(2)}) collective-permute-start(bf16[2,64,256]{2,1,0:T(8,128)(2,1)S(1)} %get-tuple-element.45.rest_0_), channel_id=1, source_target_pairs={{0,8},{4,12},{8,0},{12,4},{1,9},{5,13},{9,1},{13,5},{2,10},{6,14},... | collective-permute-start | bytes 196616 | tf_op jit(solution)/shard_map/ppermute | solution.py:43
  19.3 0.0 collective-permute-start.6
  19.3 1.5 %collective-permute-start.9 = (bf16[2,256,256]{2,1,0:T(8,128)(2,1)S(1)}, bf16[2,256,256]{2,1,0:T(8,128)(2,1)S(1)}, u32[]{:S(2)}, u32[]{:S(2)}) collective-permute-start(bf16[2,256,256]{2,1,0:T(8,128)(2,1)S(1)} %get-tuple-element.49), channel_id=1, source_target_pairs={{0,4},{4,0},{8,12},{12,8},{1,5},{5,1},{9,13},{13,9},{2,6},{6,2},{1... | collective-permute-start | bytes 786440 | tf_op jit(solution)/shard_map/ppermute | solution.py:601
  20.8 2.6 %collective-permute-start.10 = (bf16[2,256,256]{2,1,0:T(8,128)(2,1)S(1)}, bf16[2,256,256]{2,1,0:T(8,128)(2,1)S(1)}, u32[]{:S(2)}, u32[]{:S(2)}) collective-permute-start(bf16[2,256,256]{2,1,0:T(8,128)(2,1)S(1)} %get-tuple-element.50), channel_id=1, source_target_pairs={{4,8},{8,4},{5,9},{9,5},{6,10},{10,6},{7,11},{11,7},{20,24},{24,20... | collective-permute-start | bytes 786440 | tf_op jit(solution)/shard_map/ppermute | solution.py:603
  23.4 4.3 %shard_map.131 = (bf16[1536,256]{1,0:T(8,128)(2,1)S(1)}, bf16[1536,256]{1,0:T(8,128)(2,1)S(1)}, bf16[2,272,1536]{2,1,0:T(8,128)(2,1)S(1)}) custom-call(bf16[1536,2048]{1,0:T(8,128)(2,1)S(1)} %copy-done, f32[1,2048]{1,0:T(1,128)S(1)} %get-tuple-element.37.a_ref, f32[1,2048]{1,0:T(1,128)S(1)} %get-tuple-element.38.b_ref, ...), custom_call_target="tpu_custom_call" | custom-call | flops 5000000000 | tf_op jit(solution)/shard_map/pallas_call | solution.py:326
  27.7 0.0 collective-permute-done.7.rest_2_
  27.7 5.2 %shard_map.133 = (bf16[256,1536]{1,0:T(8,128)(2,1)S(1)}, bf16[256,256]{1,0:T(8,128)(2,1)S(1)}, bf16[272,256]{1,0:T(8,128)(2,1)S(1)}) custom-call(bf16[1536,256]{1,0:T(8,128)(2,1)S(1)} %get-tuple-element.42.q_ref, bf16[1536,256]{1,0:T(8,128)(2,1)S(1)} %get-tuple-element.43.k_ref, bf16[2,272,1536]{2,1,0:T(8,128)(2,1)S(1)} %get-tuple-element.44.v_ref, ...), custom_call_target="tpu_custom_call" | custom-call | flops 6000000000 | tf_op jit(solution)/shard_map/pallas_call | solution.py:489
  33.0 5.4 %shard_map.134 = (bf16[256,1536]{1,0:T(8,128)(2,1)S(1)}, bf16[384,2048]{1,0:T(8,128)(2,1)S(1)}, bf16[1024,2048]{1,0:T(8,128)(2,1)S(1)}, bf16[256,384]{1,0:T(8,12...) custom-call(bf16[256,1536]{1,0:T(8,128)(2,1)S(1)} %get-tuple-element, ...), custom_call_target="tpu_custom_call", output_to_operand_aliasing={{0}: (0, {})} | custom-call | flops 3000000000 | tf_op jit(solution)/shard_map/pallas_call | solution.py:505
  38.4 1.6 %collective-permute-start.11 = (bf16[256,384]{1,0:T(8,128)(2,1)S(1)}, bf16[256,384]{1,0:T(8,128)(2,1)S(1)}, u32[]{:S(2)}, u32[]{:S(2)}) collective-permute-start(bf16[256,384]{1,0:T(8,128)(2,1)S(1)} %get-tuple-element.54), channel_id=1, source_target_pairs={{0,1},{1,0},{2,3},{3,2},{4,5},{5,4},{6,7},{7,6},{8,9},{9,8},{10,11... | collective-permute-start | bytes 589832 | tf_op jit(solution)/shard_map/ppermute | solution.py:43
  40.0 1.2 %collective-permute-start.12 = (bf16[256,384]{1,0:T(8,128)(2,1)S(1)}, bf16[256,384]{1,0:T(8,128)(2,1)S(1)}, u32[]{:S(2)}, u32[]{:S(2)}) collective-permute-start(bf16[256,384]{1,0:T(8,128)(2,1)S(1)} %get-tuple-element.55), channel_id=1, source_target_pairs={{0,2},{1,3},{2,0},{3,1},{4,6},{5,7},{6,4},{7,5},{8,10},{9,11},{10,... | collective-permute-start | bytes 589832 | tf_op jit(solution)/shard_map/ppermute | solution.py:43
  41.2 0.5 collective-permute-start.13
  41.7 4.7 %collective-permute-done.12.rest_2_ = bf16[256,384]{1,0:T(8,128)(2,1)S(1)} collective-permute-done((bf16[256,384]{1,0:T(8,128)(2,1)S(1)}, bf16[256,384]{1,0:T(8,128)(2,1)S(1)}, u32[]{:S(2)}, u32[]{:S(2)}) %collective-permute-start.12) | collective-permute-done | bytes 196640 | tf_op jit(solution)/shard_map/ppermute | solution.py:43
  46.4 4.5 %collective-permute-done.13.rest_3_ = bf16[256,384]{1,0:T(8,128)(2,1)S(1)} collective-permute-done((bf16[256,384]{1,0:T(8,128)(2,1)S(1)}, bf16[256,384]{1,0:T(8,128)(2,1)S(1)}, u32[]{:S(2)}, u32[]{:S(2)}) %collective-permute-start.13) | collective-permute-done | bytes 196640 | tf_op jit(solution)/shard_map/ppermute | solution.py:43
  50.8 3.0 %shard_map.135 = bf16[384,2048]{1,0:T(8,128)(2,1)} custom-call(bf16[384,2048]{1,0:T(8,128)(2,1)S(1)} %get-tuple-element.51.x_ref, bf16[1024,2048]{1,0:T(8,128)(2,1)S(1)} %get-tuple-element.52.w_ref, bf16[256,384]{1,0:T(8,128)(2,1)S(1)} %get-tuple-element.53.rest_0_, bf16[256,384]{1,0:T(8,128)(2,1)S(1)} %collective-permute-done.11.rest_1_, ...), custom_call_target="tpu_custom_call" | custom-call | flops 2000000000 | tf_op jit(solution)/shard_map/pallas_call | solution.py:558
  (9 shorter events, 0.0 us)
Async XLA Ops:
  1.7 11.0 %copy-start = (bf16[1536,2048]{1,0:T(8,128)(2,1)S(1)}, bf16[1536,2048]{1,0:T(8,128)(2,1)}, u32[]{:S(2)}) copy-start(bf16[1536,2048]{1,0:T(8,128)(2,1)} %latent_ref.1) | copy-start | bytes 18874372
  1.7 11.0 %copy-start.1 = (bf16[64,2048]{1,0:T(8,128)(2,1)S(1)}, bf16[64,2048]{1,0:T(8,128)(2,1)}, u32[]{:S(2)}) copy-start(bf16[64,2048]{1,0:T(8,128)(2,1)} %context_ref.1) | copy-start | bytes 786436
  1.7 5.5 %collective-permute-start.2 = (f32[8,512]{1,0:T(8,128)S(1)}, f32[8,512]{1,0:T(8,128)S(1)}, u32[]{:S(2)}, u32[]{:S(2)}) collective-permute-start(f32[8,512]{1,0:T(8,128)S(1)} %get-tuple-element.32.token_ref.refs_0_), channel_id=1, source_target_pairs={{0,12},{4,8},{8,4},{12,0},{1,13},{5,9},{9,5},{13,1},{2,14},{6,10},... | collective-permute-start | bytes 49160 | tf_op jit(solution)/shard_map/ppermute | solution.py:43
  3.1 4.1 %collective-permute-start.1 = (f32[8,512]{1,0:T(8,128)S(1)}, f32[8,512]{1,0:T(8,128)S(1)}, u32[]{:S(2)}, u32[]{:S(2)}) collective-permute-start(f32[8,512]{1,0:T(8,128)S(1)} %get-tuple-element.32.token_ref.refs_0_), channel_id=1, source_target_pairs={{0,8},{4,12},{8,0},{12,4},{1,9},{5,13},{9,1},{13,5},{2,10},{6,14},... | collective-permute-start | bytes 49160 | tf_op jit(solution)/shard_map/ppermute | solution.py:43
  4.2 3.0 %collective-permute-start = (f32[8,512]{1,0:T(8,128)S(1)}, f32[8,512]{1,0:T(8,128)S(1)}, u32[]{:S(2)}, u32[]{:S(2)}) collective-permute-start(f32[8,512]{1,0:T(8,128)S(1)} %get-tuple-element.32.token_ref.refs_0_), channel_id=1, source_target_pairs={{0,4},{4,0},{8,12},{12,8},{1,5},{5,1},{9,13},{13,9},{2,6},{6,2},{1... | collective-permute-start | bytes 49160 | tf_op jit(solution)/shard_map/ppermute | solution.py:43
  7.2 4.4 %collective-permute-start.5 = (f32[8,512]{1,0:T(8,128)S(1)}, f32[8,512]{1,0:T(8,128)S(1)}, u32[]{:S(2)}, u32[]{:S(2)}) collective-permute-start(f32[8,512]{1,0:T(8,128)S(1)} %shard_map.129.rest_0_.token_ref.rest_4_), channel_id=1, source_target_pairs={{0,3},{1,2},{2,1},{3,0},{4,7},{5,6},{6,5},{7,4},{8,11},{9,10},{10,... | collective-permute-start | bytes 49160 | tf_op jit(solution)/shard_map/ppermute | solution.py:43
  10.1 2.6 %collective-permute-start.4 = (f32[8,512]{1,0:T(8,128)S(1)}, f32[8,512]{1,0:T(8,128)S(1)}, u32[]{:S(2)}, u32[]{:S(2)}) collective-permute-start(f32[8,512]{1,0:T(8,128)S(1)} %shard_map.129.rest_0_.token_ref.rest_4_), channel_id=1, source_target_pairs={{0,2},{1,3},{2,0},{3,1},{4,6},{5,7},{6,4},{7,5},{8,10},{9,11},{10,... | collective-permute-start | bytes 49160 | tf_op jit(solution)/shard_map/ppermute | solution.py:43
  10.2 2.5 %collective-permute-start.3 = (f32[8,512]{1,0:T(8,128)S(1)}, f32[8,512]{1,0:T(8,128)S(1)}, u32[]{:S(2)}, u32[]{:S(2)}) collective-permute-start(f32[8,512]{1,0:T(8,128)S(1)} %shard_map.129.rest_0_.token_ref.rest_4_), channel_id=1, source_target_pairs={{0,1},{1,0},{2,3},{3,2},{4,5},{5,4},{6,7},{7,6},{8,9},{9,8},{10,11... | collective-permute-start | bytes 49160 | tf_op jit(solution)/shard_map/ppermute | solution.py:43
  15.2 12.5 %collective-permute-start.8 = (bf16[2,64,256]{2,1,0:T(8,128)(2,1)S(1)}, bf16[2,64,256]{2,1,0:T(8,128)(2,1)S(1)}, u32[]{:S(2)}, u32[]{:S(2)}) collective-permute-start(bf16[2,64,256]{2,1,0:T(8,128)(2,1)S(1)} %get-tuple-element.45.rest_0_), channel_id=1, source_target_pairs={{0,12},{4,8},{8,4},{12,0},{1,13},{5,9},{9,5},{13,1},{2,14},{6,10},... | collective-permute-start | bytes 196616 | tf_op jit(solution)/shard_map/ppermute | solution.py:43
  17.7 10.0 %collective-permute-start.7 = (bf16[2,64,256]{2,1,0:T(8,128)(2,1)S(1)}, bf16[2,64,256]{2,1,0:T(8,128)(2,1)S(1)}, u32[]{:S(2)}, u32[]{:S(2)}) collective-permute-start(bf16[2,64,256]{2,1,0:T(8,128)(2,1)S(1)} %get-tuple-element.45.rest_0_), channel_id=1, source_target_pairs={{0,8},{4,12},{8,0},{12,4},{1,9},{5,13},{9,1},{13,5},{2,10},{6,14},... | collective-permute-start | bytes 196616 | tf_op jit(solution)/shard_map/ppermute | solution.py:43
  19.3 8.4 %collective-permute-start.6 = (bf16[2,64,256]{2,1,0:T(8,128)(2,1)S(1)}, bf16[2,64,256]{2,1,0:T(8,128)(2,1)S(1)}, u32[]{:S(2)}, u32[]{:S(2)}) collective-permute-start(bf16[2,64,256]{2,1,0:T(8,128)(2,1)S(1)} %get-tuple-element.45.rest_0_), channel_id=1, source_target_pairs={{0,4},{4,0},{8,12},{12,8},{1,5},{5,1},{9,13},{13,9},{2,6},{6,2},{1... | collective-permute-start | bytes 196616 | tf_op jit(solution)/shard_map/ppermute | solution.py:43
  19.3 13.6 %collective-permute-start.9 = (bf16[2,256,256]{2,1,0:T(8,128)(2,1)S(1)}, bf16[2,256,256]{2,1,0:T(8,128)(2,1)S(1)}, u32[]{:S(2)}, u32[]{:S(2)}) collective-permute-start(bf16[2,256,256]{2,1,0:T(8,128)(2,1)S(1)} %get-tuple-element.49), channel_id=1, source_target_pairs={{0,4},{4,0},{8,12},{12,8},{1,5},{5,1},{9,13},{13,9},{2,6},{6,2},{1... | collective-permute-start | bytes 786440 | tf_op jit(solution)/shard_map/ppermute | solution.py:601
  20.8 12.2 %collective-permute-start.10 = (bf16[2,256,256]{2,1,0:T(8,128)(2,1)S(1)}, bf16[2,256,256]{2,1,0:T(8,128)(2,1)S(1)}, u32[]{:S(2)}, u32[]{:S(2)}) collective-permute-start(bf16[2,256,256]{2,1,0:T(8,128)(2,1)S(1)} %get-tuple-element.50), channel_id=1, source_target_pairs={{4,8},{8,4},{5,9},{9,5},{6,10},{10,6},{7,11},{11,7},{20,24},{24,20... | collective-permute-start | bytes 786440 | tf_op jit(solution)/shard_map/ppermute | solution.py:603
  38.4 3.3 %collective-permute-start.11 = (bf16[256,384]{1,0:T(8,128)(2,1)S(1)}, bf16[256,384]{1,0:T(8,128)(2,1)S(1)}, u32[]{:S(2)}, u32[]{:S(2)}) collective-permute-start(bf16[256,384]{1,0:T(8,128)(2,1)S(1)} %get-tuple-element.54), channel_id=1, source_target_pairs={{0,1},{1,0},{2,3},{3,2},{4,5},{5,4},{6,7},{7,6},{8,9},{9,8},{10,11... | collective-permute-start | bytes 589832 | tf_op jit(solution)/shard_map/ppermute | solution.py:43
  40.0 6.4 %collective-permute-start.12 = (bf16[256,384]{1,0:T(8,128)(2,1)S(1)}, bf16[256,384]{1,0:T(8,128)(2,1)S(1)}, u32[]{:S(2)}, u32[]{:S(2)}) collective-permute-start(bf16[256,384]{1,0:T(8,128)(2,1)S(1)} %get-tuple-element.55), channel_id=1, source_target_pairs={{0,2},{1,3},{2,0},{3,1},{4,6},{5,7},{6,4},{7,5},{8,10},{9,11},{10,... | collective-permute-start | bytes 589832 | tf_op jit(solution)/shard_map/ppermute | solution.py:43
  41.2 9.7 %collective-permute-start.13 = (bf16[256,384]{1,0:T(8,128)(2,1)S(1)}, bf16[256,384]{1,0:T(8,128)(2,1)S(1)}, u32[]{:S(2)}, u32[]{:S(2)}) collective-permute-start(bf16[256,384]{1,0:T(8,128)(2,1)S(1)} %get-tuple-element.56), channel_id=1, source_target_pairs={{0,3},{1,2},{2,1},{3,0},{4,7},{5,6},{6,5},{7,4},{8,11},{9,10},{10,... | collective-permute-start | bytes 589832 | tf_op jit(solution)/shard_map/ppermute | solution.py:43

commit v2 on v1

--- a/solution.py
+++ b/solution.py
@@ -417,21 +417,10 @@
     attend_rows(rows, q_ref, kc_ref, vc_ref, t_ref, out_ref, scratch[0:2], scratch[2:4])
 
 
-def outer_kernel(sp_count, done_ref, latent_ref, weight_ref, q_ref, k_ref, v_ref, kc_ref, vc_ref, t_ref, first_ref, second_ref, out_ref, own_ref, held_ref, *rest):
-    share, tp_count = own_ref.shape[0], q_ref.shape[0] // own_ref.shape[0]
-    aligned = share % LANES == 0
-    block_refs, rest = (rest[:tp_count], rest[tp_count:]) if aligned else ((), rest)
-    sems, *scratch = rest
-    copies = [
-        pltpu.make_async_copy(weight_ref, held_ref, sems.at[0]),
-        pltpu.make_async_copy(
-            latent_ref.at[part(lax.axis_index("tp") * share, GRID_W, share)], own_ref, sems.at[1]
-        ),
-    ]
-    for copy in copies:
-        copy.start()
+def outer_kernel(sp_count, done_ref, q_ref, k_ref, v_ref, kc_ref, vc_ref, t_ref, first_ref, second_ref, out_ref, *rest):
     tokens, width = q_ref.shape
     grid_rows = tokens // GRID_W
+    block_refs, scratch = rest[:-8], rest[-8:]
     kl_ref, kh_ref, vl_ref, vh_ref = scratch[0:4]
     strip = 3 * TILE
     ones = jnp.ones((ONES, strip), bf16)
@@ -474,9 +463,8 @@
             rows.append((row, kh_ref, vh_ref, first - own - (grid_rows - WIN_ROWS), offset))
     attend_rows(rows, q_ref, kc_ref, vc_ref, t_ref, out_ref, scratch[4:6], scratch[6:8])
     for step, block_ref in enumerate(block_refs):
+        share = block_ref.shape[1]
         block_ref[...] = out_ref[:, part(target("tp", step) * share, LANES, share)]
-    for copy in copies:
-        copy.wait()
 
 
 def attention_scratch(total, width):
@@ -496,71 +484,70 @@
     )(queries, keys, values, table, *contexts)
 
 
-def outer_attention(latent, weight, done, queries, keys, values, far_keys, far_values, table, low, high):
+def outer_attention(done, queries, keys, values, far_keys, far_values, table, first, second):
     tokens, width = queries.shape
     strip = 3 * TILE
     tp_count = lax.axis_size("tp")
     share = tokens // tp_count
     blocks = [array((width, share))] * (tp_count if share % LANES == 0 else 0)
-    attended, own, held, *blocks = call(
+    attended, *blocks = call(
         functools.partial(outer_kernel, lax.axis_size("sp")),
-        [array((width, tokens)), array((share, latent.shape[1])), array(weight.shape), *blocks],
-        in_specs=[whole()] + [whole(HBM)] * 2 + [whole()] * 8,
-        out_specs=[whole()] * (3 + len(blocks)),
+        [array((width, tokens)), *blocks],
+        in_specs=[whole()] * 9,
+        out_specs=[whole()] * (1 + len(blocks)),
         input_output_aliases={0: 0},
-        scratch_shapes=[pltpu.SemaphoreType.DMA((2,))]
-        + [VMEM((strip, width), bf16)] * 2
+        scratch_shapes=[VMEM((strip, width), bf16)] * 2
         + [VMEM((2, width + ONES, strip), bf16)] * 2
         + attention_scratch(NEAR + far_keys.shape[0], width),
         flops=3_000_000_000,
-    )(
-        done,
-        *in_hbm((latent, weight)),
-        queries,
-        keys,
-        values,
-        far_keys,
-        far_values,
-        table,
-        low,
-        high,
-    )
+    )(done, queries, keys, values, far_keys, far_values, table, first, second)
     if not blocks:
         for step in range(tp_count):
             start = target("tp", step) * share
             blocks.append(lax.dynamic_slice_in_dim(attended, start, share, 1))
-    return own, held, blocks
+    return blocks
 
 
 def output_kernel(count, x_ref, w_ref, *rest):
     blocks, pieces = rest[:count], rest[count : 2 * count]
-    out_ref, gate_ref = rest[2 * count :]
-    height, _ = blocks[0].shape
+    out_ref, gate_ref, held_ref, block_ref, sems = rest[2 * count :]
+    height, share = blocks[0].shape
     dims = (((0,), (0,)), ((), ()))
     tile = w_ref.shape[1] // count
-    for index, piece in enumerate(pieces):
-        owner = origin("tp", index)
-        gate_ref[:, part(owner * tile, LANES, tile)] = piece[4:5, :]
+    for index in range(count):
+        gate_ref[:, part(origin("tp", index) * tile, LANES, tile)] = pieces[index][4:5, :]
+        rows = part(origin("tp", index) * height, LANES, height)
+        block_ref[rows, :] = blocks[index][...]
+    mine = part(lax.axis_index("tp") * share, GRID_W, share)
+    copies = []
     for step in range(count):
         cols = slice(step * tile, (step + 1) * tile)
-        total = None
-        for index, block in enumerate(blocks):
-            owner = origin("tp", index)
-            weight = w_ref[part(owner * height, LANES, height), cols]
-            term = lax.dot_general(block[...], weight, dims, preferred_element_type=f32)
-            total = term if total is None else total + term
-        out_ref[:, cols] = (x_ref[:, cols].astype(f32) + gate_ref[:, cols] * total).astype(bf16)
+        total = lax.dot_general(block_ref[...], w_ref[:, cols], dims, preferred_element_type=f32)
+        held_ref[:, cols] = (
+            x_ref[mine, cols].astype(f32) + gate_ref[:, cols] * total
+        ).astype(bf16)
+        copies.append(
+            pltpu.make_async_copy(held_ref.at[:, cols], out_ref.at[:, cols], sems.at[step])
+        )
+        copies[-1].start()
+    for copy in copies:
+        copy.wait()
 
 
 def output(x, weight, blocks, pieces):
     count = len(blocks)
-    share = x.shape[0]
+    share = x.shape[0] // count
     return call(
         functools.partial(output_kernel, count),
         array((share, x.shape[1])),
         in_specs=[whole()] * (2 + 2 * count),
-        out_specs=whole(),
-        scratch_shapes=[VMEM((1, x.shape[1]), f32)],
+        out_specs=whole(HBM),
+        scratch_shapes=[
+            VMEM((1, x.shape[1]), f32),
+            VMEM((share, x.shape[1]), bf16),
+            VMEM((weight.shape[0], share), bf16),
+            pltpu.SemaphoreType.DMA((count,)),
+        ],
         flops=2_000_000_000,
     )(x, weight, *blocks, *pieces)
 
@@ -603,13 +590,11 @@
     second = lax.ppermute(edges[4], "sp", pairs)
     fields = main_projections(latent, a, b, weights, edges[:3])
     inner, *fars = inner_attention(*fields, table, contexts)
-    own, wo, blocks = outer_attention(
-        latent, out_weight, inner, *fields, *fars, table, first, second
-    )
+    blocks = outer_attention(inner, *fields, *fars, table, first, second)
     received = blocks[:1] + [
         exchange(block, "tp", step) for step, block in enumerate(blocks) if step
     ]
-    return output(own, wo, received, pieces)
+    return output(latent, out_weight, received, pieces)
 
 
 def solution(mesh):

time: 54 us -> 51.1 us (0.946)
  Pallas kernels: 24.4 us -> 21.3 us
    pallas_call x1, Pallas kernels: 5.42 us -> 2.9 us  [outer_attention(): call(functools.partial(outer_kernel, lax.axis_size('sp')), [array((width,...]
  transfers between devices with their start and end apart: 14 -> 14, of which waited for: 4 -> 4; matrix products, arithmetic and copies ran while one was open for 0% -> 0% of each run, Pallas kernels for 22% -> 23%
where the time goes in v2:
time: 51.1 us; the launch traced here: 50.9 us
  Pallas kernels  21.3 us (42%)
  starting transfers between devices  18.4 us (36%)
  waiting for transfers between devices  10.9 us (21%)
    ppermute x12, starting transfers between devices, exchange(): return lax.ppermute(block, axis, [(i, i ^ step) for i in range(count)])  14.3 us
    ppermute x12, waiting for transfers between devices, exchange(): return lax.ppermute(block, axis, [(i, i ^ step) for i in range(count)])  10.9 us
    pallas_call x1, Pallas kernels, inner_attention(): call(functools.partial(inner_kernel, len(contexts)), [array((width, token...  4.97 us
    pallas_call x1, Pallas kernels, main_projections(): call(main_kernel, [array((tokens, out)), array((tokens, out)), array((2,...  4.31 us
    pallas_call x1, Pallas kernels, outer_attention(): call(functools.partial(outer_kernel, lax.axis_size('sp')), [array((width,...  2.9 us
    pallas_call x1, Pallas kernels, output(): call(functools.partial(output_kernel, count), array((share, x.shape[1])),...  2.69 us
    ppermute x1, starting transfers between devices, local(): second = lax.ppermute(edges[4], 'sp', pairs)  2.6 us
    pallas_call x1, Pallas kernels, edge_projections(): call(functools.partial(edge_kernel, len(pieces)), [array((2 * TILE, out))...  2.49 us
  transfers between devices with their start and end apart: 14, of which 4 were waited for; matrix products, arithmetic and copies ran while one was open for 0% of the time, Pallas kernels for 23%

profile of v2, /device:TPU:9, one launch (start us, length us, event | category | flops | bytes accessed | tf_op | source)
XLA Modules:
  0.0 50.9 jit_solution(4236433226585557481)
XLA Ops:
  0.0 1.7 %shard_map.127 = (f32[8,512]{1,0:T(8,128)S(1)}, f32[1,2048]{1,0:T(1,128)S(1)}) custom-call(bf16[2048]{0:T(1024)(128)(2,1)} %refs_0_.2, bf16[2048]{0:T(1024)(128)(2,1)} %refs_1_.2, bf16[512,512]{1,0:T(8,128)(2,1)} %refs_2_.2, bf16[512,512]{1,0:T(8,128)(2,1)} %refs_3_.1, bf16[512,512]{1,0:T(8,128)(2,1)} %refs_4_.1, bf16[2048]{0:T(1024)(128)(2,1)} %refs_5_.1), custom_call_target="tpu_custom_call" | custom-call | tf_op jit(solution)/shard_map/pallas_call | solution.py:115
  1.7 0.0 copy-start
  1.7 0.0 copy-start.2
  1.7 1.4 %collective-permute-start.2 = (f32[8,512]{1,0:T(8,128)S(1)}, f32[8,512]{1,0:T(8,128)S(1)}, u32[]{:S(2)}, u32[]{:S(2)}) collective-permute-start(f32[8,512]{1,0:T(8,128)S(1)} %get-tuple-element.30.token_ref.refs_0_), channel_id=1, source_target_pairs={{0,12},{4,8},{8,4},{12,0},{1,13},{5,9},{9,5},{13,1},{2,14},{6,10},... | collective-permute-start | bytes 49160 | tf_op jit(solution)/shard_map/ppermute | solution.py:43
  3.1 1.1 %collective-permute-start.1 = (f32[8,512]{1,0:T(8,128)S(1)}, f32[8,512]{1,0:T(8,128)S(1)}, u32[]{:S(2)}, u32[]{:S(2)}) collective-permute-start(f32[8,512]{1,0:T(8,128)S(1)} %get-tuple-element.30.token_ref.refs_0_), channel_id=1, source_target_pairs={{0,8},{4,12},{8,0},{12,4},{1,9},{5,13},{9,1},{13,5},{2,10},{6,14},... | collective-permute-start | bytes 49160 | tf_op jit(solution)/shard_map/ppermute | solution.py:43
  4.2 1.1 %collective-permute-start = (f32[8,512]{1,0:T(8,128)S(1)}, f32[8,512]{1,0:T(8,128)S(1)}, u32[]{:S(2)}, u32[]{:S(2)}) collective-permute-start(f32[8,512]{1,0:T(8,128)S(1)} %get-tuple-element.30.token_ref.refs_0_), channel_id=1, source_target_pairs={{0,4},{4,0},{8,12},{12,8},{1,5},{5,1},{9,13},{13,9},{2,6},{6,2},{1... | collective-permute-start | bytes 49160 | tf_op jit(solution)/shard_map/ppermute | solution.py:43
  5.3 1.9 %shard_map.128 = (bf16[2048,256]{1,0:T(8,128)(2,1)S(1)}, bf16[2048,256]{1,0:T(8,128)(2,1)S(1)}, bf16[2048,256]{1,0:T(8,128)(2,1)S(1)}, f32[256,1024]{1,0:T(8,128)S(1)}) custom-call(f32[8,512]{1,0:T(8,128)S(1)} %get-tuple-element.30.token_ref.refs_0_, f32[15,4,31]{2,1,0:T(4,128)} %bitcast.1, bf16[2048,256]{1,0:T(8,128)(2,1)} %refs_0_.3, ...), custom_call_target="tpu_custom_call" | custom-call | flops 500000000 | tf_op jit(solution)/shard_map/pallas_call | solution.py:178
  7.2 0.0 collective-permute-done.2.refs_3_
  7.2 0.0 collective-permute-done.refs_1_
  7.2 2.9 %collective-permute-start.5 = (f32[8,512]{1,0:T(8,128)S(1)}, f32[8,512]{1,0:T(8,128)S(1)}, u32[]{:S(2)}, u32[]{:S(2)}) collective-permute-start(f32[8,512]{1,0:T(8,128)S(1)} %shard_map.129.rest_0_.token_ref.rest_4_), channel_id=1, source_target_pairs={{0,3},{1,2},{2,1},{3,0},{4,7},{5,6},{6,5},{7,4},{8,11},{9,10},{10,... | collective-permute-start | bytes 49160 | tf_op jit(solution)/shard_map/ppermute | solution.py:43
  10.1 0.1 collective-permute-start.4
  10.2 0.3 collective-permute-start.3
  10.6 0.3 shard_map.132.t_ref
  10.9 0.7 %collective-permute-done.5.rest_3_.rest_7_ = f32[8,512]{1,0:T(8,128)S(1)} collective-permute-done((f32[8,512]{1,0:T(8,128)S(1)}, f32[8,512]{1,0:T(8,128)S(1)}, u32[]{:S(2)}, u32[]{:S(2)}) %collective-permute-start.5) | collective-permute-done | bytes 16416 | tf_op jit(solution)/shard_map/ppermute | solution.py:43
  11.7 1.0 %collective-permute-done.4.rest_2_.rest_6_ = f32[8,512]{1,0:T(8,128)S(1)} collective-permute-done((f32[8,512]{1,0:T(8,128)S(1)}, f32[8,512]{1,0:T(8,128)S(1)}, u32[]{:S(2)}, u32[]{:S(2)}) %collective-permute-start.4) | collective-permute-done | bytes 16416 | tf_op jit(solution)/shard_map/ppermute | solution.py:43
  12.7 0.0 collective-permute-done.3.rest_1_.rest_5_
  12.7 2.5 %shard_map.130 = (bf16[512,256]{1,0:T(8,128)(2,1)S(1)}, bf16[2,256,256]{2,1,0:T(8,128)(2,1)S(1)}, bf16[2,256,256]{2,1,0:T(8,128)(2,1)S(1)}, bf16[2,256,256]{2,1,...) custom-call(bf16[1536,2048]{1,0:T(8,128)(2,1)S(1)} %copy-done, ...), custom_call_target="tpu_custom_call" | custom-call | flops 2000000000 | tf_op jit(solution)/shard_map/pallas_call | solution.py:259
  15.2 2.5 %collective-permute-start.8 = (bf16[2,64,256]{2,1,0:T(8,128)(2,1)S(1)}, bf16[2,64,256]{2,1,0:T(8,128)(2,1)S(1)}, u32[]{:S(2)}, u32[]{:S(2)}) collective-permute-start(bf16[2,64,256]{2,1,0:T(8,128)(2,1)S(1)} %get-tuple-element.43.rest_0_), channel_id=1, source_target_pairs={{0,12},{4,8},{8,4},{12,0},{1,13},{5,9},{9,5},{13,1},{2,14},{6,10},... | collective-permute-start | bytes 196616 | tf_op jit(solution)/shard_map/ppermute | solution.py:43
  17.7 1.6 %collective-permute-start.7 = (bf16[2,64,256]{2,1,0:T(8,128)(2,1)S(1)}, bf16[2,64,256]{2,1,0:T(8,128)(2,1)S(1)}, u32[]{:S(2)}, u32[]{:S(2)}) collective-permute-start(bf16[2,64,256]{2,1,0:T(8,128)(2,1)S(1)} %get-tuple-element.43.rest_0_), channel_id=1, source_target_pairs={{0,8},{4,12},{8,0},{12,4},{1,9},{5,13},{9,1},{13,5},{2,10},{6,14},... | collective-permute-start | bytes 196616 | tf_op jit(solution)/shard_map/ppermute | solution.py:43
  19.3 0.0 collective-permute-start.6
  19.3 1.5 %collective-permute-start.9 = (bf16[2,256,256]{2,1,0:T(8,128)(2,1)S(1)}, bf16[2,256,256]{2,1,0:T(8,128)(2,1)S(1)}, u32[]{:S(2)}, u32[]{:S(2)}) collective-permute-start(bf16[2,256,256]{2,1,0:T(8,128)(2,1)S(1)} %get-tuple-element.47), channel_id=1, source_target_pairs={{0,4},{4,0},{8,12},{12,8},{1,5},{5,1},{9,13},{13,9},{2,6},{6,2},{1... | collective-permute-start | bytes 786440 | tf_op jit(solution)/shard_map/ppermute | solution.py:588
  20.8 2.6 %collective-permute-start.10 = (bf16[2,256,256]{2,1,0:T(8,128)(2,1)S(1)}, bf16[2,256,256]{2,1,0:T(8,128)(2,1)S(1)}, u32[]{:S(2)}, u32[]{:S(2)}) collective-permute-start(bf16[2,256,256]{2,1,0:T(8,128)(2,1)S(1)} %get-tuple-element.48), channel_id=1, source_target_pairs={{4,8},{8,4},{5,9},{9,5},{6,10},{10,6},{7,11},{11,7},{20,24},{24,20... | collective-permute-start | bytes 786440 | tf_op jit(solution)/shard_map/ppermute | solution.py:590
  23.4 4.3 %shard_map.131 = (bf16[1536,256]{1,0:T(8,128)(2,1)S(1)}, bf16[1536,256]{1,0:T(8,128)(2,1)S(1)}, bf16[2,272,1536]{2,1,0:T(8,128)(2,1)S(1)}) custom-call(bf16[1536,2048]{1,0:T(8,128)(2,1)S(1)} %copy-done, f32[1,2048]{1,0:T(1,128)S(1)} %get-tuple-element.35.a_ref, f32[1,2048]{1,0:T(1,128)S(1)} %get-tuple-element.36.b_ref, ...), custom_call_target="tpu_custom_call" | custom-call | flops 5000000000 | tf_op jit(solution)/shard_map/pallas_call | solution.py:326
  27.7 5.0 %shard_map.133 = (bf16[256,1536]{1,0:T(8,128)(2,1)S(1)}, bf16[256,256]{1,0:T(8,128)(2,1)S(1)}, bf16[272,256]{1,0:T(8,128)(2,1)S(1)}) custom-call(bf16[1536,256]{1,0:T(8,128)(2,1)S(1)} %get-tuple-element.40.q_ref, bf16[1536,256]{1,0:T(8,128)(2,1)S(1)} %get-tuple-element.41.k_ref, bf16[2,272,1536]{2,1,0:T(8,128)(2,1)S(1)} %get-tuple-element.42.v_ref, ...), custom_call_target="tpu_custom_call" | custom-call | flops 6000000000 | tf_op jit(solution)/shard_map/pallas_call | solution.py:477
  32.7 0.0 copy-start.1
  32.7 2.9 %shard_map.134 = (bf16[256,1536]{1,0:T(8,128)(2,1)S(1)}, bf16[256,384]{1,0:T(8,128)(2,1)S(1)}, bf16[256,384]{1,0:T(8,128)(2,1)S(1)}, bf16[256,384]{1,0:T(8,128)(2,1)S(1)}, bf16[256,384]{1,0:T(8,128)(2,1)S(1)}) custom-call(bf16[256,1536]{1,0:T(8,128)(2,1)S(1)} %get-tuple-element.44.done_ref, ...), custom_call_target="tpu_custom_call", output_to_operand_aliasing={{0}: (0, {})} | custom-call | flops 3000000000 | tf_op jit(solution)/shard_map/pallas_call | solution.py:493
  35.6 1.6 %collective-permute-start.11 = (bf16[256,384]{1,0:T(8,128)(2,1)S(1)}, bf16[256,384]{1,0:T(8,128)(2,1)S(1)}, u32[]{:S(2)}, u32[]{:S(2)}) collective-permute-start(bf16[256,384]{1,0:T(8,128)(2,1)S(1)} %get-tuple-element.50), channel_id=1, source_target_pairs={{0,1},{1,0},{2,3},{3,2},{4,5},{5,4},{6,7},{7,6},{8,9},{9,8},{10,11... | collective-permute-start | bytes 589832 | tf_op jit(solution)/shard_map/ppermute | solution.py:43
  37.3 1.2 %collective-permute-start.12 = (bf16[256,384]{1,0:T(8,128)(2,1)S(1)}, bf16[256,384]{1,0:T(8,128)(2,1)S(1)}, u32[]{:S(2)}, u32[]{:S(2)}) collective-permute-start(bf16[256,384]{1,0:T(8,128)(2,1)S(1)} %get-tuple-element.51), channel_id=1, source_target_pairs={{0,2},{1,3},{2,0},{3,1},{4,6},{5,7},{6,4},{7,5},{8,10},{9,11},{10,... | collective-permute-start | bytes 589832 | tf_op jit(solution)/shard_map/ppermute | solution.py:43
  38.4 0.5 %collective-permute-start.13 = (bf16[256,384]{1,0:T(8,128)(2,1)S(1)}, bf16[256,384]{1,0:T(8,128)(2,1)S(1)}, u32[]{:S(2)}, u32[]{:S(2)}) collective-permute-start(bf16[256,384]{1,0:T(8,128)(2,1)S(1)} %get-tuple-element.52), channel_id=1, source_target_pairs={{0,3},{1,2},{2,1},{3,0},{4,7},{5,6},{6,5},{7,4},{8,11},{9,10},{10,... | collective-permute-start | bytes 589832 | tf_op jit(solution)/shard_map/ppermute | solution.py:43
  39.0 4.7 %collective-permute-done.12.rest_2_ = bf16[256,384]{1,0:T(8,128)(2,1)S(1)} collective-permute-done((bf16[256,384]{1,0:T(8,128)(2,1)S(1)}, bf16[256,384]{1,0:T(8,128)(2,1)S(1)}, u32[]{:S(2)}, u32[]{:S(2)}) %collective-permute-start.12) | collective-permute-done | bytes 196640 | tf_op jit(solution)/shard_map/ppermute | solution.py:43
  43.6 4.5 %collective-permute-done.13.rest_3_ = bf16[256,384]{1,0:T(8,128)(2,1)S(1)} collective-permute-done((bf16[256,384]{1,0:T(8,128)(2,1)S(1)}, bf16[256,384]{1,0:T(8,128)(2,1)S(1)}, u32[]{:S(2)}, u32[]{:S(2)}) %collective-permute-start.13) | collective-permute-done | bytes 196640 | tf_op jit(solution)/shard_map/ppermute | solution.py:43
  48.1 2.7 %shard_map.135 = bf16[384,2048]{1,0:T(8,128)(2,1)} custom-call(bf16[1536,2048]{1,0:T(8,128)(2,1)S(1)} %copy-done, bf16[1024,2048]{1,0:T(8,128)(2,1)S(1)} %copy-done.1, bf16[256,384]{1,0:T(8,128)(2,1)S(1)} %get-tuple-element.49.rest_0_, bf16[256,384]{1,0:T(8,128)(2,1)S(1)} %collective-permute-done.11.rest_1_, ...), custom_call_target="tpu_custom_call" | custom-call | flops 2000000000 | tf_op jit(solution)/shard_map/pallas_call | solution.py:540
  (11 shorter events, 0.0 us)
Async XLA Ops:
  1.7 11.0 %copy-start = (bf16[1536,2048]{1,0:T(8,128)(2,1)S(1)}, bf16[1536,2048]{1,0:T(8,128)(2,1)}, u32[]{:S(2)}) copy-start(bf16[1536,2048]{1,0:T(8,128)(2,1)} %x_ref.5) | copy-start | bytes 18874372
  1.7 11.0 %copy-start.2 = (bf16[64,2048]{1,0:T(8,128)(2,1)S(1)}, bf16[64,2048]{1,0:T(8,128)(2,1)}, u32[]{:S(2)}) copy-start(bf16[64,2048]{1,0:T(8,128)(2,1)} %context_ref.1) | copy-start | bytes 786436
  1.7 5.5 %collective-permute-start.2 = (f32[8,512]{1,0:T(8,128)S(1)}, f32[8,512]{1,0:T(8,128)S(1)}, u32[]{:S(2)}, u32[]{:S(2)}) collective-permute-start(f32[8,512]{1,0:T(8,128)S(1)} %get-tuple-element.30.token_ref.refs_0_), channel_id=1, source_target_pairs={{0,12},{4,8},{8,4},{12,0},{1,13},{5,9},{9,5},{13,1},{2,14},{6,10},... | collective-permute-start | bytes 49160 | tf_op jit(solution)/shard_map/ppermute | solution.py:43
  3.1 4.1 %collective-permute-start.1 = (f32[8,512]{1,0:T(8,128)S(1)}, f32[8,512]{1,0:T(8,128)S(1)}, u32[]{:S(2)}, u32[]{:S(2)}) collective-permute-start(f32[8,512]{1,0:T(8,128)S(1)} %get-tuple-element.30.token_ref.refs_0_), channel_id=1, source_target_pairs={{0,8},{4,12},{8,0},{12,4},{1,9},{5,13},{9,1},{13,5},{2,10},{6,14},... | collective-permute-start | bytes 49160 | tf_op jit(solution)/shard_map/ppermute | solution.py:43
  4.2 3.0 %collective-permute-start = (f32[8,512]{1,0:T(8,128)S(1)}, f32[8,512]{1,0:T(8,128)S(1)}, u32[]{:S(2)}, u32[]{:S(2)}) collective-permute-start(f32[8,512]{1,0:T(8,128)S(1)} %get-tuple-element.30.token_ref.refs_0_), channel_id=1, source_target_pairs={{0,4},{4,0},{8,12},{12,8},{1,5},{5,1},{9,13},{13,9},{2,6},{6,2},{1... | collective-permute-start | bytes 49160 | tf_op jit(solution)/shard_map/ppermute | solution.py:43
  7.2 4.4 %collective-permute-start.5 = (f32[8,512]{1,0:T(8,128)S(1)}, f32[8,512]{1,0:T(8,128)S(1)}, u32[]{:S(2)}, u32[]{:S(2)}) collective-permute-start(f32[8,512]{1,0:T(8,128)S(1)} %shard_map.129.rest_0_.token_ref.rest_4_), channel_id=1, source_target_pairs={{0,3},{1,2},{2,1},{3,0},{4,7},{5,6},{6,5},{7,4},{8,11},{9,10},{10,... | collective-permute-start | bytes 49160 | tf_op jit(solution)/shard_map/ppermute | solution.py:43
  10.1 2.6 %collective-permute-start.4 = (f32[8,512]{1,0:T(8,128)S(1)}, f32[8,512]{1,0:T(8,128)S(1)}, u32[]{:S(2)}, u32[]{:S(2)}) collective-permute-start(f32[8,512]{1,0:T(8,128)S(1)} %shard_map.129.rest_0_.token_ref.rest_4_), channel_id=1, source_target_pairs={{0,2},{1,3},{2,0},{3,1},{4,6},{5,7},{6,4},{7,5},{8,10},{9,11},{10,... | collective-permute-start | bytes 49160 | tf_op jit(solution)/shard_map/ppermute | solution.py:43
  10.2 2.5 %collective-permute-start.3 = (f32[8,512]{1,0:T(8,128)S(1)}, f32[8,512]{1,0:T(8,128)S(1)}, u32[]{:S(2)}, u32[]{:S(2)}) collective-permute-start(f32[8,512]{1,0:T(8,128)S(1)} %shard_map.129.rest_0_.token_ref.rest_4_), channel_id=1, source_target_pairs={{0,1},{1,0},{2,3},{3,2},{4,5},{5,4},{6,7},{7,6},{8,9},{9,8},{10,11... | collective-permute-start | bytes 49160 | tf_op jit(solution)/shard_map/ppermute | solution.py:43
  15.2 12.5 %collective-permute-start.8 = (bf16[2,64,256]{2,1,0:T(8,128)(2,1)S(1)}, bf16[2,64,256]{2,1,0:T(8,128)(2,1)S(1)}, u32[]{:S(2)}, u32[]{:S(2)}) collective-permute-start(bf16[2,64,256]{2,1,0:T(8,128)(2,1)S(1)} %get-tuple-element.43.rest_0_), channel_id=1, source_target_pairs={{0,12},{4,8},{8,4},{12,0},{1,13},{5,9},{9,5},{13,1},{2,14},{6,10},... | collective-permute-start | bytes 196616 | tf_op jit(solution)/shard_map/ppermute | solution.py:43
  17.7 10.0 %collective-permute-start.7 = (bf16[2,64,256]{2,1,0:T(8,128)(2,1)S(1)}, bf16[2,64,256]{2,1,0:T(8,128)(2,1)S(1)}, u32[]{:S(2)}, u32[]{:S(2)}) collective-permute-start(bf16[2,64,256]{2,1,0:T(8,128)(2,1)S(1)} %get-tuple-element.43.rest_0_), channel_id=1, source_target_pairs={{0,8},{4,12},{8,0},{12,4},{1,9},{5,13},{9,1},{13,5},{2,10},{6,14},... | collective-permute-start | bytes 196616 | tf_op jit(solution)/shard_map/ppermute | solution.py:43
  19.3 8.4 %collective-permute-start.6 = (bf16[2,64,256]{2,1,0:T(8,128)(2,1)S(1)}, bf16[2,64,256]{2,1,0:T(8,128)(2,1)S(1)}, u32[]{:S(2)}, u32[]{:S(2)}) collective-permute-start(bf16[2,64,256]{2,1,0:T(8,128)(2,1)S(1)} %get-tuple-element.43.rest_0_), channel_id=1, source_target_pairs={{0,4},{4,0},{8,12},{12,8},{1,5},{5,1},{9,13},{13,9},{2,6},{6,2},{1... | collective-permute-start | bytes 196616 | tf_op jit(solution)/shard_map/ppermute | solution.py:43
  19.3 13.4 %collective-permute-start.9 = (bf16[2,256,256]{2,1,0:T(8,128)(2,1)S(1)}, bf16[2,256,256]{2,1,0:T(8,128)(2,1)S(1)}, u32[]{:S(2)}, u32[]{:S(2)}) collective-permute-start(bf16[2,256,256]{2,1,0:T(8,128)(2,1)S(1)} %get-tuple-element.47), channel_id=1, source_target_pairs={{0,4},{4,0},{8,12},{12,8},{1,5},{5,1},{9,13},{13,9},{2,6},{6,2},{1... | collective-permute-start | bytes 786440 | tf_op jit(solution)/shard_map/ppermute | solution.py:588
  20.8 11.9 %collective-permute-start.10 = (bf16[2,256,256]{2,1,0:T(8,128)(2,1)S(1)}, bf16[2,256,256]{2,1,0:T(8,128)(2,1)S(1)}, u32[]{:S(2)}, u32[]{:S(2)}) collective-permute-start(bf16[2,256,256]{2,1,0:T(8,128)(2,1)S(1)} %get-tuple-element.48), channel_id=1, source_target_pairs={{4,8},{8,4},{5,9},{9,5},{6,10},{10,6},{7,11},{11,7},{20,24},{24,20... | collective-permute-start | bytes 786440 | tf_op jit(solution)/shard_map/ppermute | solution.py:590
  32.7 15.4 %copy-start.1 = (bf16[1024,2048]{1,0:T(8,128)(2,1)S(1)}, bf16[1024,2048]{1,0:T(8,128)(2,1)}, u32[]{:S(2)}) copy-start(bf16[1024,2048]{1,0:T(8,128)(2,1)} %w_ref.1) | copy-start | bytes 12582916
  35.6 3.3 %collective-permute-start.11 = (bf16[256,384]{1,0:T(8,128)(2,1)S(1)}, bf16[256,384]{1,0:T(8,128)(2,1)S(1)}, u32[]{:S(2)}, u32[]{:S(2)}) collective-permute-start(bf16[256,384]{1,0:T(8,128)(2,1)S(1)} %get-tuple-element.50), channel_id=1, source_target_pairs={{0,1},{1,0},{2,3},{3,2},{4,5},{5,4},{6,7},{7,6},{8,9},{9,8},{10,11... | collective-permute-start | bytes 589832 | tf_op jit(solution)/shard_map/ppermute | solution.py:43
  37.3 6.4 %collective-permute-start.12 = (bf16[256,384]{1,0:T(8,128)(2,1)S(1)}, bf16[256,384]{1,0:T(8,128)(2,1)S(1)}, u32[]{:S(2)}, u32[]{:S(2)}) collective-permute-start(bf16[256,384]{1,0:T(8,128)(2,1)S(1)} %get-tuple-element.51), channel_id=1, source_target_pairs={{0,2},{1,3},{2,0},{3,1},{4,6},{5,7},{6,4},{7,5},{8,10},{9,11},{10,... | collective-permute-start | bytes 589832 | tf_op jit(solution)/shard_map/ppermute | solution.py:43
  38.4 9.7 %collective-permute-start.13 = (bf16[256,384]{1,0:T(8,128)(2,1)S(1)}, bf16[256,384]{1,0:T(8,128)(2,1)S(1)}, u32[]{:S(2)}, u32[]{:S(2)}) collective-permute-start(bf16[256,384]{1,0:T(8,128)(2,1)S(1)} %get-tuple-element.52), channel_id=1, source_target_pairs={{0,3},{1,2},{2,1},{3,0},{4,7},{5,6},{6,5},{7,4},{8,11},{9,10},{10,... | collective-permute-start | bytes 589832 | tf_op jit(solution)/shard_map/ppermute | solution.py:43

commit v3 on v2

--- a/solution.py
+++ b/solution.py
@@ -7,6 +7,7 @@
 from jax.experimental import pallas as pl
 from jax.experimental.pallas import tpu as pltpu
 from jax.sharding import PartitionSpec as P
+
 
 HEAD_DIM = 64
 GRID_W = 64
@@ -125,6 +126,7 @@
             VMEM((3, rows, width), bf16),
             pltpu.SemaphoreType.DMA((6,)),
         ],
+        flops=3_000_000_000,
     )(*in_hbm((condition, context_condition, *rest)))
 
 
@@ -189,7 +191,9 @@
     )(token, *in_hbm((jnp.transpose(offset_bias, (1, 0, 2)), *weights)))
 
 
-def flip_kernel(token_ref, table_ref, out_ref):
+def flip_kernel(token_ref, table_ref, weight_ref, held_ref, out_ref, sem):
+    copy = pltpu.make_async_copy(weight_ref, held_ref, sem)
+    copy.start()
     width = table_ref.shape[0]
     key = lax.broadcasted_iota(jnp.int32, (LANES, LANES), 0) % GRID_W
     query = lax.broadcasted_iota(jnp.int32, (LANES, LANES), 1) % GRID_W
@@ -199,16 +203,18 @@
         for col in range(width // LANES):
             rows, cols = slice(row * LANES, (row + 1) * LANES), slice(col * LANES, (col + 1) * LANES)
             out_ref[rows, cols] = jnp.where(inside, table_ref[cols, rows].T, masked_score)
-
-
-def bias_table(token, rows):
+    copy.wait()
+
+
+def bias_table(token, rows, weight):
     return call(
         flip_kernel,
-        array(rows.shape[::-1], f32),
-        in_specs=[whole()] * 2,
-        out_specs=whole(),
+        [array(weight.shape), array(rows.shape[::-1], f32)],
+        in_specs=[whole()] * 2 + [whole(HBM)],
+        out_specs=[whole()] * 2,
+        scratch_shapes=[pltpu.SemaphoreType.DMA],
         flops=1_000_000_000,
-    )(token, rows)
+    )(token, rows, *in_hbm([weight]))
 
 
 def modulators(pieces, gain_ref, scale_row, shift_row, a_ref, b_ref):
@@ -400,28 +406,59 @@
     return pl.ds(pl.multiple_of(start, unit), size)
 
 
-def inner_kernel(count, q_ref, k_ref, v_ref, t_ref, *rest):
-    contexts, (out_ref, kc_ref, vc_ref, *scratch) = rest[:count], rest[count:]
-    width = q_ref.shape[1]
-    grid_rows = q_ref.shape[0] // GRID_W
+def is_free(row, grid_rows):
+    return HALO_ROWS <= row < grid_rows - HALO_ROWS
+
+
+def phases(tokens):
+    count = lax.axis_size("tp")
+    share = tokens // count
+    rows = range(tokens // GRID_W)
+    if share % LANES or share < 2 * LANES:
+        return rows, range(0)
+    each = share // GRID_W
+    late = [r for r in rows if (r < 2 if r < each else r % each >= each - 2)]
+    return [r for r in rows if r not in late], late
+
+
+def far_refs(contexts, kc_ref, vc_ref):
+    width = kc_ref.shape[1]
     height = contexts[0].shape[1]
     for index, context in enumerate(contexts):
         kc_ref[index * height : (index + 1) * height] = context[0]
     far_values = jnp.concatenate([context[1] for context in contexts], axis=0)
     vc_ref[0:width, :] = far_values.astype(f32).T.astype(bf16)
     vc_ref[width:, :] = jnp.ones((ONES, vc_ref.shape[1]), bf16)
-    rows = [
-        (row, k_ref, v_ref, row - HALO_ROWS, WIN_ROWS - 1 - HALO_ROWS)
-        for row in range(HALO_ROWS, grid_rows - HALO_ROWS)
-    ]
-    attend_rows(rows, q_ref, kc_ref, vc_ref, t_ref, out_ref, scratch[0:2], scratch[2:4])
-
-
-def outer_kernel(sp_count, done_ref, q_ref, k_ref, v_ref, kc_ref, vc_ref, t_ref, first_ref, second_ref, out_ref, *rest):
-    tokens, width = q_ref.shape
-    grid_rows = tokens // GRID_W
-    block_refs, scratch = rest[:-8], rest[-8:]
-    kl_ref, kh_ref, vl_ref, vh_ref = scratch[0:4]
+
+
+def row_plan(rows, grid_rows, sp_count, k_ref, v_ref, strips):
+    own = lax.axis_index("sp") * grid_rows
+    total = grid_rows * sp_count
+    plan = []
+    for row in rows:
+        if is_free(row, grid_rows):
+            plan.append((row, k_ref, v_ref, row - HALO_ROWS, WIN_ROWS - 1 - HALO_ROWS))
+            continue
+        kl_ref, kh_ref, vl_ref, vh_ref = strips
+        first = jnp.clip(own + row - HALO_ROWS, 0, total - WIN_ROWS)
+        offset = first - (own + row) + WIN_ROWS - 1
+        if row < HALO_ROWS:
+            plan.append((row, kl_ref, vl_ref, first - own + HALO_ROWS, offset))
+        else:
+            plan.append((row, kh_ref, vh_ref, first - own - (grid_rows - WIN_ROWS), offset))
+    return plan
+
+
+def inner_kernel(count, rows, q_ref, k_ref, v_ref, t_ref, *rest):
+    contexts, (out_ref, kc_ref, vc_ref, *scratch) = rest[:count], rest[count:]
+    far_refs(contexts, kc_ref, vc_ref)
+    plan = row_plan(rows, q_ref.shape[0] // GRID_W, 0, k_ref, v_ref, None)
+    attend_rows(plan, q_ref, kc_ref, vc_ref, t_ref, out_ref, scratch[0:2], scratch[2:4])
+
+
+def fill_strips(k_ref, v_ref, first_ref, second_ref, strips):
+    tokens, width = k_ref.shape
+    kl_ref, kh_ref, vl_ref, vh_ref = strips
     strip = 3 * TILE
     ones = jnp.ones((ONES, strip), bf16)
     even = lax.axis_index("sp") % 2 == 0
@@ -450,21 +487,37 @@
     vh_ref[1, 0:width, 2 * TILE - GRID_W : 2 * TILE] = rolled[:, TILE - GRID_W :]
     vh_ref[1, 0:width, 2 * TILE : strip - GRID_W] = rolled[:, 0 : TILE - GRID_W]
     vh_ref[1, 0:width, strip - GRID_W :] = jnp.zeros((width, GRID_W), bf16)
-    sp = lax.axis_index("sp")
-    total = grid_rows * sp_count
-    rows = []
-    for row in (*range(HALO_ROWS), *range(grid_rows - HALO_ROWS, grid_rows)):
-        own = sp * grid_rows
-        first = jnp.clip(own + row - HALO_ROWS, 0, total - WIN_ROWS)
-        offset = first - (own + row) + WIN_ROWS - 1
-        if row < HALO_ROWS:
-            rows.append((row, kl_ref, vl_ref, first - own + HALO_ROWS, offset))
-        else:
-            rows.append((row, kh_ref, vh_ref, first - own - (grid_rows - WIN_ROWS), offset))
-    attend_rows(rows, q_ref, kc_ref, vc_ref, t_ref, out_ref, scratch[4:6], scratch[6:8])
+
+
+def split_blocks(out_ref, block_refs, late):
     for step, block_ref in enumerate(block_refs):
-        share = block_ref.shape[1]
-        block_ref[...] = out_ref[:, part(target("tp", step) * share, LANES, share)]
+        size = block_ref.shape[1]
+        owner = target("tp", step)
+        share = out_ref.shape[1] // len(block_refs)
+        inside = jnp.where(owner == 0, 0, share - size)
+        inside = inside if late else share - size - inside
+        start = owner * share + inside
+        block_ref[...] = out_ref[:, part(start, LANES, size)]
+
+
+def middle_kernel(rows, sp_count, done_ref, latent_ref, q_ref, k_ref, v_ref, kc_ref, vc_ref, t_ref, first_ref, second_ref, out_ref, own_ref, *rest):
+    strips, block_refs, (sem, *scratch) = rest[:4], rest[4:-5], rest[-5:]
+    share = own_ref.shape[0]
+    mine = part(lax.axis_index("tp") * share, GRID_W, share)
+    copy = pltpu.make_async_copy(latent_ref.at[mine], own_ref, sem)
+    copy.start()
+    fill_strips(k_ref, v_ref, first_ref, second_ref, strips)
+    plan = row_plan(rows, q_ref.shape[0] // GRID_W, sp_count, k_ref, v_ref, strips)
+    attend_rows(plan, q_ref, kc_ref, vc_ref, t_ref, out_ref, scratch[0:2], scratch[2:4])
+    split_blocks(out_ref, block_refs, False)
+    copy.wait()
+
+
+def late_kernel(rows, sp_count, q_ref, k_ref, v_ref, kc_ref, vc_ref, t_ref, *rest):
+    strips, block_refs, (out_ref, *scratch) = rest[:4], rest[4:-5], rest[-5:]
+    plan = row_plan(rows, q_ref.shape[0] // GRID_W, sp_count, k_ref, v_ref, strips)
+    attend_rows(plan, q_ref, kc_ref, vc_ref, t_ref, out_ref, scratch[0:2], scratch[2:4])
+    split_blocks(out_ref, block_refs, True)
 
 
 def attention_scratch(total, width):
@@ -474,86 +527,128 @@
 def inner_attention(queries, keys, values, table, contexts):
     tokens, width = queries.shape
     far = len(contexts) * contexts[0].shape[1]
+    rows = [r for r in phases(tokens)[0] if is_free(r, tokens // GRID_W)]
+    rows = [r for r in rows if r ^ 1 in rows]
     return call(
-        functools.partial(inner_kernel, len(contexts)),
+        functools.partial(inner_kernel, len(contexts), rows),
         [array((width, tokens)), array((far, width)), array((width + ONES, far))],
         in_specs=[whole()] * (4 + len(contexts)),
         out_specs=[whole()] * 3,
         scratch_shapes=attention_scratch(NEAR + far, width),
-        flops=6_000_000_000,
+        flops=4_000_000_000,
     )(queries, keys, values, table, *contexts)
 
 
-def outer_attention(done, queries, keys, values, far_keys, far_values, table, first, second):
+def middle_attention(done, latent, queries, keys, values, far_keys, far_values, table, first, second):
     tokens, width = queries.shape
     strip = 3 * TILE
-    tp_count = lax.axis_size("tp")
-    share = tokens // tp_count
-    blocks = [array((width, share))] * (tp_count if share % LANES == 0 else 0)
-    attended, *blocks = call(
-        functools.partial(outer_kernel, lax.axis_size("sp")),
-        [array((width, tokens)), *blocks],
-        in_specs=[whole()] * 9,
-        out_specs=[whole()] * (1 + len(blocks)),
+    count = lax.axis_size("tp")
+    early, late = phases(tokens)
+    rows = [
+        r for r in early if not (is_free(r, tokens // GRID_W) and is_free(r ^ 1, tokens // GRID_W))
+    ]
+    block = array((width, len(early) * GRID_W // count))
+    attended, own, *rest = call(
+        functools.partial(middle_kernel, rows, lax.axis_size("sp")),
+        [
+            array((width, tokens)),
+            array((tokens // count, latent.shape[1])),
+            *[array((strip, width))] * 2,
+            *[array((2, width + ONES, strip))] * 2,
+            *[block] * (count if late else 0),
+        ],
+        in_specs=[whole(), whole(HBM)] + [whole()] * 8,
+        out_specs=[whole()] * (6 + (count if late else 0)),
         input_output_aliases={0: 0},
-        scratch_shapes=[VMEM((strip, width), bf16)] * 2
-        + [VMEM((2, width + ONES, strip), bf16)] * 2
+        scratch_shapes=[pltpu.SemaphoreType.DMA]
         + attention_scratch(NEAR + far_keys.shape[0], width),
-        flops=3_000_000_000,
-    )(done, queries, keys, values, far_keys, far_values, table, first, second)
-    if not blocks:
-        for step in range(tp_count):
-            start = target("tp", step) * share
-            blocks.append(lax.dynamic_slice_in_dim(attended, start, share, 1))
-    return blocks
-
-
-def output_kernel(count, x_ref, w_ref, *rest):
-    blocks, pieces = rest[:count], rest[count : 2 * count]
-    out_ref, gate_ref, held_ref, block_ref, sems = rest[2 * count :]
-    height, share = blocks[0].shape
-    dims = (((0,), (0,)), ((), ()))
+        flops=2_000_000_000,
+    )(done, *in_hbm([latent]), queries, keys, values, far_keys, far_values, table, first, second)
+    strips, blocks = rest[:4], rest[4:]
+    if not late:
+        share = tokens // count
+        blocks = [
+            lax.dynamic_slice_in_dim(attended, target("tp", step) * share, share, 1)
+            for step in range(count)
+        ]
+    return own, strips, list(blocks)
+
+
+def late_attention(queries, keys, values, far_keys, far_values, table, strips):
+    tokens, width = queries.shape
+    count = lax.axis_size("tp")
+    late = phases(tokens)[1]
+    if not late:
+        return []
+    return list(
+        call(
+            functools.partial(late_kernel, late, lax.axis_size("sp")),
+            [array((width, len(late) * GRID_W // count))] * count,
+            in_specs=[whole()] * 10,
+            out_specs=[whole()] * count,
+            scratch_shapes=[VMEM((width, tokens), bf16)]
+            + attention_scratch(NEAR + far_keys.shape[0], width),
+            flops=3_000_000_000,
+        )(queries, keys, values, far_keys, far_values, table, *strips)
+    )
+
+
+def output_kernel(count, late, *refs):
+    x_ref, w_ref, *arrays, out_ref, gate_ref, held_ref, block_ref, sems = refs[late:]
+    pieces, blocks = arrays[:count], arrays[count:]
+    height, size = blocks[0].shape
+    share = out_ref.shape[0]
     tile = w_ref.shape[1] // count
+    tp = lax.axis_index("tp")
     for index in range(count):
         gate_ref[:, part(origin("tp", index) * tile, LANES, tile)] = pieces[index][4:5, :]
         rows = part(origin("tp", index) * height, LANES, height)
-        block_ref[rows, :] = blocks[index][...]
-    mine = part(lax.axis_index("tp") * share, GRID_W, share)
+        block_ref[:, rows] = blocks[index][...].astype(f32).T.astype(bf16)
+    inside = jnp.where(tp == 0, 0, share - size)
+    inside = inside if late else share - size - inside
+    mine = part(inside, GRID_W, size)
     copies = []
     for step in range(count):
         cols = slice(step * tile, (step + 1) * tile)
-        total = lax.dot_general(block_ref[...], w_ref[:, cols], dims, preferred_element_type=f32)
+        total = jnp.dot(block_ref[...], w_ref[:, cols], preferred_element_type=f32)
         held_ref[:, cols] = (
             x_ref[mine, cols].astype(f32) + gate_ref[:, cols] * total
         ).astype(bf16)
         copies.append(
-            pltpu.make_async_copy(held_ref.at[:, cols], out_ref.at[:, cols], sems.at[step])
+            pltpu.make_async_copy(held_ref.at[:, cols], out_ref.at[mine, cols], sems.at[step])
         )
         copies[-1].start()
     for copy in copies:
         copy.wait()
 
 
-def output(x, weight, blocks, pieces):
+def output(x, weight, blocks, pieces, done=None):
     count = len(blocks)
-    share = x.shape[0] // count
+    share, width = x.shape
+    size = blocks[0].shape[1]
+    late = done is not None
     return call(
-        functools.partial(output_kernel, count),
-        array((share, x.shape[1])),
-        in_specs=[whole()] * (2 + 2 * count),
+        functools.partial(output_kernel, count, late),
+        array((share, width)),
+        in_specs=[whole(HBM)] * late + [whole()] * (2 + len(pieces) + len(blocks)),
         out_specs=whole(HBM),
+        input_output_aliases={0: 0} if late else {},
         scratch_shapes=[
-            VMEM((1, x.shape[1]), f32),
-            VMEM((share, x.shape[1]), bf16),
-            VMEM((weight.shape[0], share), bf16),
+            VMEM((1, width), f32),
+            VMEM((size, width), bf16),
+            VMEM((size, weight.shape[0]), bf16),
             pltpu.SemaphoreType.DMA((count,)),
         ],
         flops=2_000_000_000,
-    )(x, weight, *blocks, *pieces)
+    )(*([done] if late else []), x, weight, *pieces, *blocks)
 
 
 def gathered(block, axis):
     return [block] + [exchange(block, axis, step) for step in range(1, lax.axis_size(axis))]
+
+
+def sent(blocks):
+    return blocks[:1] + [exchange(blocks[step], "tp", step) for step in range(1, len(blocks))]
 
 
 def local(
@@ -575,10 +670,11 @@
         condition, context_condition, shift_weight, scale_weight, gate_weight, norm_gain
     )
     partials = gathered(terms, "sp")
-    *weights, rows = bias_rows(terms, offset_bias, query_weight, key_weight, value_weight)
+    wk, wv, rows = bias_rows(terms, offset_bias, key_weight, value_weight)
     summed = summed_terms(rows, partials)
     pieces = gathered(summed, "tp")
-    table = bias_table(summed, rows)
+    wq, table = bias_table(summed, rows, query_weight)
+    weights = (wq, wk, wv)
     *edges, far, a, b = edge_projections(
         latent, context_tokens, gain, weights, pieces
     )
@@ -590,11 +686,14 @@
     second = lax.ppermute(edges[4], "sp", pairs)
     fields = main_projections(latent, a, b, weights, edges[:3])
     inner, *fars = inner_attention(*fields, table, contexts)
-    blocks = outer_attention(inner, *fields, *fars, table, first, second)
-    received = blocks[:1] + [
-        exchange(block, "tp", step) for step, block in enumerate(blocks) if step
-    ]
-    return output(latent, out_weight, received, pieces)
+    own, strips, early = middle_attention(inner, latent, *fields, *fars, table, first, second)
+    early = sent(early)
+    late = late_attention(*fields, *fars, table, strips)
+    late = sent(late)
+    done = output(own, out_weight, early, pieces)
+    if not late:
+        return done
+    return output(own, out_weight, late, pieces, done)
 
 
 def solution(mesh):

time: 51.1 us -> 48.4 us (0.947)
  waiting for transfers between devices: 10.9 us -> 2.79 us
  Pallas kernels: 21.3 us -> 24.5 us
  starting transfers between devices: 18.4 us -> 20.6 us
    ppermute x12 -> x15, waiting for transfers between devices: 10.9 us -> 2.79 us  [exchange(): return lax.ppermute(block, axis, [(i, i ^ step) for i in range(count)])]
    pallas_call x4 -> x6, Pallas kernels: 10.9 us -> 14.2 us  [the longest x2 3.82 us: output(): call(functools.partial(output_kernel, count, late), array((share, width))...]
    ppermute x12 -> x15, starting transfers between devices: 14.3 us -> 16.7 us  [exchange(): return lax.ppermute(block, axis, [(i, i ^ step) for i in range(count)])]
  transfers between devices with their start and end apart: 14 -> 17, of which waited for: 4 -> 2; matrix products, arithmetic and copies ran while one was open for 0% -> 0% of each run, Pallas kernels for 23% -> 33%
where the time goes in v3:
time: 48.4 us; the launch traced here: 48.2 us
  Pallas kernels  24.5 us (51%)
  starting transfers between devices  20.6 us (43%)
  waiting for transfers between devices  2.79 us (6%)
    ppermute x15, starting transfers between devices, exchange(): return lax.ppermute(block, axis, [(i, i ^ step) for i in range(count)])  16.7 us
    pallas_call x1, Pallas kernels, main_projections(): call(main_kernel, [array((tokens, out)), array((tokens, out)), array((2,...  4.33 us
    pallas_call x2, Pallas kernels, output(): call(functools.partial(output_kernel, count, late), array((share, width))...  3.82 us
    pallas_call x1, Pallas kernels, inner_attention(): call(functools.partial(inner_kernel, len(contexts), rows), [array((width,...  3.76 us
    ppermute x15, waiting for transfers between devices, exchange(): return lax.ppermute(block, axis, [(i, i ^ step) for i in range(count)])  2.79 us
    pallas_call x1, Pallas kernels, late_attention(): call(functools.partial(late_kernel, late, lax.axis_size('sp')), [array((w...  2.76 us
    pallas_call x1, Pallas kernels, middle_attention(): call(functools.partial(middle_kernel, rows, lax.axis_size('sp')), [array(...  2.67 us
    pallas_call x1, Pallas kernels, edge_projections(): call(functools.partial(edge_kernel, len(pieces)), [array((2 * TILE, out))...  2.49 us
  transfers between devices with their start and end apart: 17, of which 2 were waited for; matrix products, arithmetic and copies ran while one was open for 0% of the time, Pallas kernels for 33%

profile of v3, /device:TPU:9, one launch (start us, length us, event | category | flops | bytes accessed | tf_op | source)
XLA Modules:
  0.0 48.2 jit_solution(8042402295612051068)
XLA Ops:
  0.0 1.7 %shard_map.127 = (f32[8,512]{1,0:T(8,128)S(1)}, f32[1,2048]{1,0:T(1,128)S(1)}) custom-call(bf16[2048]{0:T(1024)(128)(2,1)} %refs_0_.2, bf16[2048]{0:T(1024)(128)(2,1)} %refs_1_.3, bf16[512,512]{1,0:T(8,128)(2,1)} %refs_2_.2, bf16[512,512]{1,0:T(8,128)(2,1)} %refs_3_.1, bf16[512,512]{1,0:T(8,128)(2,1)} %refs_4_.1, bf16[2048]{0:T(1024)(128)(2,1)} %refs_5_.1), custom_call_target="tpu_custom_call" | custom-call | flops 3000000000 | tf_op jit(solution)/shard_map/pallas_call | solution.py:116
  1.7 1.4 %collective-permute-start.2 = (f32[8,512]{1,0:T(8,128)S(1)}, f32[8,512]{1,0:T(8,128)S(1)}, u32[]{:S(2)}, u32[]{:S(2)}) collective-permute-start(f32[8,512]{1,0:T(8,128)S(1)} %get-tuple-element.40.token_ref.refs_0_), channel_id=1, source_target_pairs={{0,12},{4,8},{8,4},{12,0},{1,13},{5,9},{9,5},{13,1},{2,14},{6,10},... | collective-permute-start | bytes 49160 | tf_op jit(solution)/shard_map/ppermute | solution.py:44
  3.1 1.1 %collective-permute-start.1 = (f32[8,512]{1,0:T(8,128)S(1)}, f32[8,512]{1,0:T(8,128)S(1)}, u32[]{:S(2)}, u32[]{:S(2)}) collective-permute-start(f32[8,512]{1,0:T(8,128)S(1)} %get-tuple-element.40.token_ref.refs_0_), channel_id=1, source_target_pairs={{0,8},{4,12},{8,0},{12,4},{1,9},{5,13},{9,1},{13,5},{2,10},{6,14},... | collective-permute-start | bytes 49160 | tf_op jit(solution)/shard_map/ppermute | solution.py:44
  4.2 1.1 %collective-permute-start = (f32[8,512]{1,0:T(8,128)S(1)}, f32[8,512]{1,0:T(8,128)S(1)}, u32[]{:S(2)}, u32[]{:S(2)}) collective-permute-start(f32[8,512]{1,0:T(8,128)S(1)} %get-tuple-element.40.token_ref.refs_0_), channel_id=1, source_target_pairs={{0,4},{4,0},{8,12},{12,8},{1,5},{5,1},{9,13},{13,9},{2,6},{6,2},{1... | collective-permute-start | bytes 49160 | tf_op jit(solution)/shard_map/ppermute | solution.py:44
  5.3 1.7 %shard_map.128 = (bf16[2048,256]{1,0:T(8,128)(2,1)S(1)}, bf16[2048,256]{1,0:T(8,128)(2,1)S(1)}, f32[256,1024]{1,0:T(8,128)S(1)}) custom-call(f32[8,512]{1,0:T(8,128)S(1)} %get-tuple-element.40.token_ref.refs_0_, f32[15,4,31]{2,1,0:T(4,128)} %bitcast.1, bf16[2048,256]{1,0:T(8,128)(2,1)} %refs_0_.3, bf16[2048,256]{1,0:T(8,128)(2,1)} %refs_1_.4), custom_call_target="tpu_custom_call" | custom-call | flops 500000000 | tf_op jit(solution)/shard_map/pallas_call | solution.py:180
  7.0 0.0 collective-permute-done.refs_1_
  7.1 0.0 copy-start.2
  7.1 3.1 %collective-permute-start.5 = (f32[8,512]{1,0:T(8,128)S(1)}, f32[8,512]{1,0:T(8,128)S(1)}, u32[]{:S(2)}, u32[]{:S(2)}) collective-permute-start(f32[8,512]{1,0:T(8,128)S(1)} %shard_map.129.token_ref.rest_0_.refs_2_.refs_3_), channel_id=1, source_target_pairs={{0,3},{1,2},{2,1},{3,0},{4,7},{5,6},{6,5},{7,4},{8,11},{9,10},{10,... | collective-permute-start | bytes 49160 | tf_op jit(solution)/shard_map/ppermute | solution.py:44
  10.2 0.1 collective-permute-start.4
  10.3 0.4 collective-permute-start.3
  10.6 1.2 %shard_map.130 = (bf16[2048,256]{1,0:T(8,128)(2,1)S(1)}, f32[1024,256]{1,0:T(8,128)S(1)}) custom-call(f32[8,512]{1,0:T(8,128)S(1)} %shard_map.129.token_ref.rest_0_.refs_2_.refs_3_, f32[256,1024]{1,0:T(8,128)S(1)} %get-tuple-element.41.token_ref.table_ref, bf16[2048,256]{1,0:T(8,128)(2,1)} %weight_ref.1), custom_call_target="tpu_custom_call" | custom-call | flops 1000000000 | tf_op jit(solution)/shard_map/pallas_call | solution.py:210
  11.9 0.0 collective-permute-done.5.rest_3_.refs_5_.refs_6_
  11.9 0.9 %collective-permute-done.4.rest_2_.refs_4_.refs_5_ = f32[8,512]{1,0:T(8,128)S(1)} collective-permute-done((f32[8,512]{1,0:T(8,128)S(1)}, f32[8,512]{1,0:T(8,128)S(1)}, u32[]{:S(2)}, u32[]{:S(2)}) %collective-permute-start.4) | collective-permute-done | bytes 16416 | tf_op jit(solution)/shard_map/ppermute | solution.py:44
  12.8 2.5 %shard_map.131 = (bf16[512,256]{1,0:T(8,128)(2,1)S(1)}, bf16[2,256,256]{2,1,0:T(8,128)(2,1)S(1)}, bf16[2,256,256]{2,1,0:T(8,128)(2,1)S(1)}, bf16[2,256,256]{2,1,...) custom-call(bf16[1536,2048]{1,0:T(8,128)(2,1)S(1)} %copy-done, ...), custom_call_target="tpu_custom_call" | custom-call | flops 2000000000 | tf_op jit(solution)/shard_map/pallas_call | solution.py:265
  15.3 2.5 %collective-permute-start.8 = (bf16[2,64,256]{2,1,0:T(8,128)(2,1)S(1)}, bf16[2,64,256]{2,1,0:T(8,128)(2,1)S(1)}, u32[]{:S(2)}, u32[]{:S(2)}) collective-permute-start(bf16[2,64,256]{2,1,0:T(8,128)(2,1)S(1)} %get-tuple-element.54.rest_0_), channel_id=1, source_target_pairs={{0,12},{4,8},{8,4},{12,0},{1,13},{5,9},{9,5},{13,1},{2,14},{6,10},... | collective-permute-start | bytes 196616 | tf_op jit(solution)/shard_map/ppermute | solution.py:44
  17.8 1.5 %collective-permute-start.7 = (bf16[2,64,256]{2,1,0:T(8,128)(2,1)S(1)}, bf16[2,64,256]{2,1,0:T(8,128)(2,1)S(1)}, u32[]{:S(2)}, u32[]{:S(2)}) collective-permute-start(bf16[2,64,256]{2,1,0:T(8,128)(2,1)S(1)} %get-tuple-element.54.rest_0_), channel_id=1, source_target_pairs={{0,8},{4,12},{8,0},{12,4},{1,9},{5,13},{9,1},{13,5},{2,10},{6,14},... | collective-permute-start | bytes 196616 | tf_op jit(solution)/shard_map/ppermute | solution.py:44
  19.3 1.5 %collective-permute-start.9 = (bf16[2,256,256]{2,1,0:T(8,128)(2,1)S(1)}, bf16[2,256,256]{2,1,0:T(8,128)(2,1)S(1)}, u32[]{:S(2)}, u32[]{:S(2)}) collective-permute-start(bf16[2,256,256]{2,1,0:T(8,128)(2,1)S(1)} %get-tuple-element.58), channel_id=1, source_target_pairs={{0,4},{4,0},{8,12},{12,8},{1,5},{5,1},{9,13},{13,9},{2,6},{6,2},{1... | collective-permute-start | bytes 786440 | tf_op jit(solution)/shard_map/ppermute | solution.py:684
  20.8 2.4 %collective-permute-start.10 = (bf16[2,256,256]{2,1,0:T(8,128)(2,1)S(1)}, bf16[2,256,256]{2,1,0:T(8,128)(2,1)S(1)}, u32[]{:S(2)}, u32[]{:S(2)}) collective-permute-start(bf16[2,256,256]{2,1,0:T(8,128)(2,1)S(1)} %get-tuple-element.59), channel_id=1, source_target_pairs={{4,8},{8,4},{5,9},{9,5},{6,10},{10,6},{7,11},{11,7},{20,24},{24,20... | collective-permute-start | bytes 786440 | tf_op jit(solution)/shard_map/ppermute | solution.py:686
  23.2 4.3 %shard_map.132 = (bf16[1536,256]{1,0:T(8,128)(2,1)S(1)}, bf16[1536,256]{1,0:T(8,128)(2,1)S(1)}, bf16[2,272,1536]{2,1,0:T(8,128)(2,1)S(1)}) custom-call(bf16[1536,2048]{1,0:T(8,128)(2,1)S(1)} %copy-done, f32[1,2048]{1,0:T(1,128)S(1)} %get-tuple-element.45.a_ref, f32[1,2048]{1,0:T(1,128)S(1)} %get-tuple-element.46.b_ref, ...), custom_call_target="tpu_custom_call" | custom-call | flops 5000000000 | tf_op jit(solution)/shard_map/pallas_call | solution.py:332
  27.5 3.8 %shard_map.133 = (bf16[256,1536]{1,0:T(8,128)(2,1)S(1)}, bf16[256,256]{1,0:T(8,128)(2,1)S(1)}, bf16[272,256]{1,0:T(8,128)(2,1)S(1)}) custom-call(bf16[1536,256]{1,0:T(8,128)(2,1)S(1)} %get-tuple-element.50.q_ref, bf16[1536,256]{1,0:T(8,128)(2,1)S(1)} %get-tuple-element.51.k_ref, bf16[2,272,1536]{2,1,0:T(8,128)(2,1)S(1)} %get-tuple-element.52.v_ref, ...), custom_call_target="tpu_custom_call" | custom-call | flops 4000000000 | tf_op jit(solution)/shard_map/pallas_call | solution.py:532
  31.3 2.7 %shard_map.134 = (bf16[256,1536]{1,0:T(8,128)(2,1)S(1)}, bf16[384,2048]{1,0:T(8,128)(2,1)S(1)}, bf16[768,256]{1,0:T(8,128)(2,1)S(1)}, bf16[768,256]{1,0:T(8,128)...) custom-call(bf16[256,1536]{1,0:T(8,128)(2,1)S(1)} %get-tuple-element, ...), custom_call_target="tpu_custom_call", output_to_operand_aliasing={{0}: (0, {})} | custom-call | flops 2000000000 | tf_op jit(solution)/shard_map/pallas_call | solution.py:551
  34.0 1.6 %collective-permute-start.11 = (bf16[256,256]{1,0:T(8,128)(2,1)S(1)}, bf16[256,256]{1,0:T(8,128)(2,1)S(1)}, u32[]{:S(2)}, u32[]{:S(2)}) collective-permute-start(bf16[256,256]{1,0:T(8,128)(2,1)S(1)} %get-tuple-element.62), channel_id=1, source_target_pairs={{0,1},{1,0},{2,3},{3,2},{4,5},{5,4},{6,7},{7,6},{8,9},{9,8},{10,11... | collective-permute-start | bytes 393224 | tf_op jit(solution)/shard_map/ppermute | solution.py:44
  35.6 1.2 %collective-permute-start.12 = (bf16[256,256]{1,0:T(8,128)(2,1)S(1)}, bf16[256,256]{1,0:T(8,128)(2,1)S(1)}, u32[]{:S(2)}, u32[]{:S(2)}) collective-permute-start(bf16[256,256]{1,0:T(8,128)(2,1)S(1)} %get-tuple-element.63), channel_id=1, source_target_pairs={{0,2},{1,3},{2,0},{3,1},{4,6},{5,7},{6,4},{7,5},{8,10},{9,11},{10,... | collective-permute-start | bytes 393224 | tf_op jit(solution)/shard_map/ppermute | solution.py:44
  36.8 0.5 %collective-permute-start.13 = (bf16[256,256]{1,0:T(8,128)(2,1)S(1)}, bf16[256,256]{1,0:T(8,128)(2,1)S(1)}, u32[]{:S(2)}, u32[]{:S(2)}) collective-permute-start(bf16[256,256]{1,0:T(8,128)(2,1)S(1)} %get-tuple-element.64), channel_id=1, source_target_pairs={{0,3},{1,2},{2,1},{3,0},{4,7},{5,6},{6,5},{7,4},{8,11},{9,10},{10,... | collective-permute-start | bytes 393224 | tf_op jit(solution)/shard_map/ppermute | solution.py:44
  37.3 2.8 %shard_map.136 = (bf16[256,128]{1,0:T(8,128)(2,1)S(1)}, bf16[256,128]{1,0:T(8,128)(2,1)S(1)}, bf16[256,128]{1,0:T(8,128)(2,1)S(1)}, bf16[256,128]{1,0:T(8,128)(2,1)S(1)}) custom-call(bf16[1536,256]{1,0:T(8,128)(2,1)S(1)} %get-tuple-element.50.q_ref, bf16[1536,256]{1,0:T(8,128)(2,1)S(1)} %get-tuple-element.51.k_ref, ...), custom_call_target="tpu_custom_call" | custom-call | flops 3000000000 | tf_op jit(solution)/shard_map/pallas_call | solution.py:584
  40.1 0.2 collective-permute-start.14
  40.3 1.2 %collective-permute-start.15 = (bf16[256,128]{1,0:T(8,128)(2,1)S(1)}, bf16[256,128]{1,0:T(8,128)(2,1)S(1)}, u32[]{:S(2)}, u32[]{:S(2)}) collective-permute-start(bf16[256,128]{1,0:T(8,128)(2,1)S(1)} %get-tuple-element.71), channel_id=1, source_target_pairs={{0,2},{1,3},{2,0},{3,1},{4,6},{5,7},{6,4},{7,5},{8,10},{9,11},{10,... | collective-permute-start | bytes 196616 | tf_op jit(solution)/shard_map/ppermute | solution.py:44
  41.5 0.8 %collective-permute-start.16 = (bf16[256,128]{1,0:T(8,128)(2,1)S(1)}, bf16[256,128]{1,0:T(8,128)(2,1)S(1)}, u32[]{:S(2)}, u32[]{:S(2)}) collective-permute-start(bf16[256,128]{1,0:T(8,128)(2,1)S(1)} %get-tuple-element.72), channel_id=1, source_target_pairs={{0,3},{1,2},{2,1},{3,0},{4,7},{5,6},{6,5},{7,4},{8,11},{9,10},{10,... | collective-permute-start | bytes 196616 | tf_op jit(solution)/shard_map/ppermute | solution.py:44
  42.3 1.9 %collective-permute-done.13.refs_9_ = bf16[256,256]{1,0:T(8,128)(2,1)S(1)} collective-permute-done((bf16[256,256]{1,0:T(8,128)(2,1)S(1)}, bf16[256,256]{1,0:T(8,128)(2,1)S(1)}, u32[]{:S(2)}, u32[]{:S(2)}) %collective-permute-start.13) | collective-permute-done | bytes 131104 | tf_op jit(solution)/shard_map/ppermute | solution.py:44
  44.2 2.2 %shard_map.135.refs_0_ = bf16[384,2048]{1,0:T(8,128)(2,1)} custom-call(bf16[384,2048]{1,0:T(8,128)(2,1)S(1)} %get-tuple-element.60.refs_0_.refs_1_, bf16[1024,2048]{1,0:T(8,128)(2,1)S(1)} %copy-done.1, f32[8,512]{1,0:T(8,128)S(1)} %shard_map.129.token_ref.rest_0_.refs_2_.refs_3_, f32[8,512]{1,0:T(8,128)S(1)} %collective-permute-done.3.rest_1_.refs_3_.refs_4_, ...), custom_call_target="tpu_custom_call" | custom-call | flops 2000000000 | tf_op jit(solution)/shard_map/pallas_call | solution.py:630
  46.4 0.0 collective-permute-done.16.refs_10_
  46.5 1.6 %shard_map.137 = bf16[384,2048]{1,0:T(8,128)(2,1)} custom-call(bf16[384,2048]{1,0:T(8,128)(2,1)} %shard_map.135.refs_0_, bf16[384,2048]{1,0:T(8,128)(2,1)S(1)} %get-tuple-element.60.refs_0_.refs_1_, bf16[1024,2048]{1,0:T(8,128)(2,1)S(1)} %copy-done.1, f32[8,512]{1,0:T(8,128)S(1)} %shard_map.129.token_ref.rest_0_.refs_2_.refs_3_, ...), custom_call_target="tpu_custom_call", output_to_operand_aliasing={{}: (0, {})} | custom-call | flops 2000000000 | tf_op jit(solution)/shard_map/pallas_call | solution.py:630
  (19 shorter events, 0.1 us)
Async XLA Ops:
  1.7 5.3 %collective-permute-start.2 = (f32[8,512]{1,0:T(8,128)S(1)}, f32[8,512]{1,0:T(8,128)S(1)}, u32[]{:S(2)}, u32[]{:S(2)}) collective-permute-start(f32[8,512]{1,0:T(8,128)S(1)} %get-tuple-element.40.token_ref.refs_0_), channel_id=1, source_target_pairs={{0,12},{4,8},{8,4},{12,0},{1,13},{5,9},{9,5},{13,1},{2,14},{6,10},... | collective-permute-start | bytes 49160 | tf_op jit(solution)/shard_map/ppermute | solution.py:44
  3.1 4.0 %collective-permute-start.1 = (f32[8,512]{1,0:T(8,128)S(1)}, f32[8,512]{1,0:T(8,128)S(1)}, u32[]{:S(2)}, u32[]{:S(2)}) collective-permute-start(f32[8,512]{1,0:T(8,128)S(1)} %get-tuple-element.40.token_ref.refs_0_), channel_id=1, source_target_pairs={{0,8},{4,12},{8,0},{12,4},{1,9},{5,13},{9,1},{13,5},{2,10},{6,14},... | collective-permute-start | bytes 49160 | tf_op jit(solution)/shard_map/ppermute | solution.py:44
  4.2 2.9 %collective-permute-start = (f32[8,512]{1,0:T(8,128)S(1)}, f32[8,512]{1,0:T(8,128)S(1)}, u32[]{:S(2)}, u32[]{:S(2)}) collective-permute-start(f32[8,512]{1,0:T(8,128)S(1)} %get-tuple-element.40.token_ref.refs_0_), channel_id=1, source_target_pairs={{0,4},{4,0},{8,12},{12,8},{1,5},{5,1},{9,13},{13,9},{2,6},{6,2},{1... | collective-permute-start | bytes 49160 | tf_op jit(solution)/shard_map/ppermute | solution.py:44
  5.3 7.5 %copy-start = (bf16[1536,2048]{1,0:T(8,128)(2,1)S(1)}, bf16[1536,2048]{1,0:T(8,128)(2,1)}, u32[]{:S(2)}) copy-start(bf16[1536,2048]{1,0:T(8,128)(2,1)} %latent_ref.1) | copy-start | bytes 18874372
  7.1 5.7 %copy-start.2 = (bf16[64,2048]{1,0:T(8,128)(2,1)S(1)}, bf16[64,2048]{1,0:T(8,128)(2,1)}, u32[]{:S(2)}) copy-start(bf16[64,2048]{1,0:T(8,128)(2,1)} %context_ref.1) | copy-start | bytes 786436
  7.1 4.8 %collective-permute-start.5 = (f32[8,512]{1,0:T(8,128)S(1)}, f32[8,512]{1,0:T(8,128)S(1)}, u32[]{:S(2)}, u32[]{:S(2)}) collective-permute-start(f32[8,512]{1,0:T(8,128)S(1)} %shard_map.129.token_ref.rest_0_.refs_2_.refs_3_), channel_id=1, source_target_pairs={{0,3},{1,2},{2,1},{3,0},{4,7},{5,6},{6,5},{7,4},{8,11},{9,10},{10,... | collective-permute-start | bytes 49160 | tf_op jit(solution)/shard_map/ppermute | solution.py:44
  10.2 2.6 %collective-permute-start.4 = (f32[8,512]{1,0:T(8,128)S(1)}, f32[8,512]{1,0:T(8,128)S(1)}, u32[]{:S(2)}, u32[]{:S(2)}) collective-permute-start(f32[8,512]{1,0:T(8,128)S(1)} %shard_map.129.token_ref.rest_0_.refs_2_.refs_3_), channel_id=1, source_target_pairs={{0,2},{1,3},{2,0},{3,1},{4,6},{5,7},{6,4},{7,5},{8,10},{9,11},{10,... | collective-permute-start | bytes 49160 | tf_op jit(solution)/shard_map/ppermute | solution.py:44
  10.3 2.5 %collective-permute-start.3 = (f32[8,512]{1,0:T(8,128)S(1)}, f32[8,512]{1,0:T(8,128)S(1)}, u32[]{:S(2)}, u32[]{:S(2)}) collective-permute-start(f32[8,512]{1,0:T(8,128)S(1)} %shard_map.129.token_ref.rest_0_.refs_2_.refs_3_), channel_id=1, source_target_pairs={{0,1},{1,0},{2,3},{3,2},{4,5},{5,4},{6,7},{7,6},{8,9},{9,8},{10,11... | collective-permute-start | bytes 49160 | tf_op jit(solution)/shard_map/ppermute | solution.py:44
  15.3 12.3 %collective-permute-start.8 = (bf16[2,64,256]{2,1,0:T(8,128)(2,1)S(1)}, bf16[2,64,256]{2,1,0:T(8,128)(2,1)S(1)}, u32[]{:S(2)}, u32[]{:S(2)}) collective-permute-start(bf16[2,64,256]{2,1,0:T(8,128)(2,1)S(1)} %get-tuple-element.54.rest_0_), channel_id=1, source_target_pairs={{0,12},{4,8},{8,4},{12,0},{1,13},{5,9},{9,5},{13,1},{2,14},{6,10},... | collective-permute-start | bytes 196616 | tf_op jit(solution)/shard_map/ppermute | solution.py:44
  17.8 9.8 %collective-permute-start.7 = (bf16[2,64,256]{2,1,0:T(8,128)(2,1)S(1)}, bf16[2,64,256]{2,1,0:T(8,128)(2,1)S(1)}, u32[]{:S(2)}, u32[]{:S(2)}) collective-permute-start(bf16[2,64,256]{2,1,0:T(8,128)(2,1)S(1)} %get-tuple-element.54.rest_0_), channel_id=1, source_target_pairs={{0,8},{4,12},{8,0},{12,4},{1,9},{5,13},{9,1},{13,5},{2,10},{6,14},... | collective-permute-start | bytes 196616 | tf_op jit(solution)/shard_map/ppermute | solution.py:44
  19.3 8.3 %collective-permute-start.6 = (bf16[2,64,256]{2,1,0:T(8,128)(2,1)S(1)}, bf16[2,64,256]{2,1,0:T(8,128)(2,1)S(1)}, u32[]{:S(2)}, u32[]{:S(2)}) collective-permute-start(bf16[2,64,256]{2,1,0:T(8,128)(2,1)S(1)} %get-tuple-element.54.rest_0_), channel_id=1, source_target_pairs={{0,4},{4,0},{8,12},{12,8},{1,5},{5,1},{9,13},{13,9},{2,6},{6,2},{1... | collective-permute-start | bytes 196616 | tf_op jit(solution)/shard_map/ppermute | solution.py:44
  19.3 12.0 %collective-permute-start.9 = (bf16[2,256,256]{2,1,0:T(8,128)(2,1)S(1)}, bf16[2,256,256]{2,1,0:T(8,128)(2,1)S(1)}, u32[]{:S(2)}, u32[]{:S(2)}) collective-permute-start(bf16[2,256,256]{2,1,0:T(8,128)(2,1)S(1)} %get-tuple-element.58), channel_id=1, source_target_pairs={{0,4},{4,0},{8,12},{12,8},{1,5},{5,1},{9,13},{13,9},{2,6},{6,2},{1... | collective-permute-start | bytes 786440 | tf_op jit(solution)/shard_map/ppermute | solution.py:684
  20.8 10.6 %collective-permute-start.10 = (bf16[2,256,256]{2,1,0:T(8,128)(2,1)S(1)}, bf16[2,256,256]{2,1,0:T(8,128)(2,1)S(1)}, u32[]{:S(2)}, u32[]{:S(2)}) collective-permute-start(bf16[2,256,256]{2,1,0:T(8,128)(2,1)S(1)} %get-tuple-element.59), channel_id=1, source_target_pairs={{4,8},{8,4},{5,9},{9,5},{6,10},{10,6},{7,11},{11,7},{20,24},{24,20... | collective-permute-start | bytes 786440 | tf_op jit(solution)/shard_map/ppermute | solution.py:686
  34.0 7.5 %collective-permute-start.11 = (bf16[256,256]{1,0:T(8,128)(2,1)S(1)}, bf16[256,256]{1,0:T(8,128)(2,1)S(1)}, u32[]{:S(2)}, u32[]{:S(2)}) collective-permute-start(bf16[256,256]{1,0:T(8,128)(2,1)S(1)} %get-tuple-element.62), channel_id=1, source_target_pairs={{0,1},{1,0},{2,3},{3,2},{4,5},{5,4},{6,7},{7,6},{8,9},{9,8},{10,11... | collective-permute-start | bytes 393224 | tf_op jit(solution)/shard_map/ppermute | solution.py:44
  35.6 6.7 %collective-permute-start.12 = (bf16[256,256]{1,0:T(8,128)(2,1)S(1)}, bf16[256,256]{1,0:T(8,128)(2,1)S(1)}, u32[]{:S(2)}, u32[]{:S(2)}) collective-permute-start(bf16[256,256]{1,0:T(8,128)(2,1)S(1)} %get-tuple-element.63), channel_id=1, source_target_pairs={{0,2},{1,3},{2,0},{3,1},{4,6},{5,7},{6,4},{7,5},{8,10},{9,11},{10,... | collective-permute-start | bytes 393224 | tf_op jit(solution)/shard_map/ppermute | solution.py:44
  36.8 7.4 %collective-permute-start.13 = (bf16[256,256]{1,0:T(8,128)(2,1)S(1)}, bf16[256,256]{1,0:T(8,128)(2,1)S(1)}, u32[]{:S(2)}, u32[]{:S(2)}) collective-permute-start(bf16[256,256]{1,0:T(8,128)(2,1)S(1)} %get-tuple-element.64), channel_id=1, source_target_pairs={{0,3},{1,2},{2,1},{3,0},{4,7},{5,6},{6,5},{7,4},{8,11},{9,10},{10,... | collective-permute-start | bytes 393224 | tf_op jit(solution)/shard_map/ppermute | solution.py:44
  37.3 6.9 %copy-start.1 = (bf16[1024,2048]{1,0:T(8,128)(2,1)S(1)}, bf16[1024,2048]{1,0:T(8,128)(2,1)}, u32[]{:S(2)}) copy-start(bf16[1024,2048]{1,0:T(8,128)(2,1)} %refs_2_.3) | copy-start | bytes 12582916
  40.1 6.3 %collective-permute-start.14 = (bf16[256,128]{1,0:T(8,128)(2,1)S(1)}, bf16[256,128]{1,0:T(8,128)(2,1)S(1)}, u32[]{:S(2)}, u32[]{:S(2)}) collective-permute-start(bf16[256,128]{1,0:T(8,128)(2,1)S(1)} %get-tuple-element.70), channel_id=1, source_target_pairs={{0,1},{1,0},{2,3},{3,2},{4,5},{5,4},{6,7},{7,6},{8,9},{9,8},{10,11... | collective-permute-start | bytes 196616 | tf_op jit(solution)/shard_map/ppermute | solution.py:44
  40.3 6.1 %collective-permute-start.15 = (bf16[256,128]{1,0:T(8,128)(2,1)S(1)}, bf16[256,128]{1,0:T(8,128)(2,1)S(1)}, u32[]{:S(2)}, u32[]{:S(2)}) collective-permute-start(bf16[256,128]{1,0:T(8,128)(2,1)S(1)} %get-tuple-element.71), channel_id=1, source_target_pairs={{0,2},{1,3},{2,0},{3,1},{4,6},{5,7},{6,4},{7,5},{8,10},{9,11},{10,... | collective-permute-start | bytes 196616 | tf_op jit(solution)/shard_map/ppermute | solution.py:44
  41.5 4.9 %collective-permute-start.16 = (bf16[256,128]{1,0:T(8,128)(2,1)S(1)}, bf16[256,128]{1,0:T(8,128)(2,1)S(1)}, u32[]{:S(2)}, u32[]{:S(2)}) collective-permute-start(bf16[256,128]{1,0:T(8,128)(2,1)S(1)} %get-tuple-element.72), channel_id=1, source_target_pairs={{0,3},{1,2},{2,1},{3,0},{4,7},{5,6},{6,5},{7,4},{8,11},{9,10},{10,... | collective-permute-start | bytes 196616 | tf_op jit(solution)/shard_map/ppermute | solution.py:44

commit v4 on v3

--- a/solution.py
+++ b/solution.py
@@ -191,9 +191,15 @@
     )(token, *in_hbm((jnp.transpose(offset_bias, (1, 0, 2)), *weights)))
 
 
-def flip_kernel(token_ref, table_ref, weight_ref, held_ref, out_ref, sem):
-    copy = pltpu.make_async_copy(weight_ref, held_ref, sem)
-    copy.start()
+def flip_kernel(token_ref, table_ref, *refs):
+    *refs, out_ref, sems = refs
+    count = len(refs) // 2
+    copies = [
+        pltpu.make_async_copy(refs[index], refs[count + index], sems.at[index])
+        for index in range(count)
+    ]
+    for copy in copies:
+        copy.start()
     width = table_ref.shape[0]
     key = lax.broadcasted_iota(jnp.int32, (LANES, LANES), 0) % GRID_W
     query = lax.broadcasted_iota(jnp.int32, (LANES, LANES), 1) % GRID_W
@@ -203,18 +209,19 @@
         for col in range(width // LANES):
             rows, cols = slice(row * LANES, (row + 1) * LANES), slice(col * LANES, (col + 1) * LANES)
             out_ref[rows, cols] = jnp.where(inside, table_ref[cols, rows].T, masked_score)
-    copy.wait()
-
-
-def bias_table(token, rows, weight):
+    for copy in copies:
+        copy.wait()
+
+
+def bias_table(token, rows, *weights):
     return call(
         flip_kernel,
-        [array(weight.shape), array(rows.shape[::-1], f32)],
-        in_specs=[whole()] * 2 + [whole(HBM)],
-        out_specs=[whole()] * 2,
-        scratch_shapes=[pltpu.SemaphoreType.DMA],
+        [*(array(weight.shape) for weight in weights), array(rows.shape[::-1], f32)],
+        in_specs=[whole()] * 2 + [whole(HBM)] * len(weights),
+        out_specs=[whole()] * (1 + len(weights)),
+        scratch_shapes=[pltpu.SemaphoreType.DMA((len(weights),))],
         flops=1_000_000_000,
-    )(token, rows, *in_hbm([weight]))
+    )(token, rows, *in_hbm(weights))
 
 
 def modulators(pieces, gain_ref, scale_row, shift_row, a_ref, b_ref):
@@ -235,9 +242,10 @@
 query_factor = log2e * HEAD_DIM ** (-0.5)
 
 
-def edge_kernel(count, x_ref, context_ref, gain_ref, wq_ref, wk_ref, wv_ref, *rest):
+def edge_kernel(count, x_ref, context_ref, gain_ref, wk_ref, wv_ref, *rest):
     pieces = rest[:count]
-    q_ref, low_ref, high_ref, even_ref, odd_ref, far_ref, a_ref, b_ref, ac_ref, bc_ref, first_ref, second_ref = rest[count:]
+    first_ref, second_ref, low_ref, high_ref, even_ref, odd_ref, far_ref, *rest = rest[count:]
+    a_ref, b_ref, ac_ref, bc_ref = rest
     modulators(pieces, gain_ref, 3, 1, ac_ref, bc_ref)
     hidden = modulated(context_ref[...], ac_ref[...], bc_ref[...])
     far_ref[0] = jnp.dot(hidden, wk_ref[...], preferred_element_type=f32).astype(bf16)
@@ -254,9 +262,6 @@
     even = lax.axis_index("sp") % 2 == 0
     even_ref[...] = jnp.where(even, high_ref[...], low_ref[...])
     odd_ref[...] = jnp.where(even, low_ref[...], high_ref[...])
-    for index, ref in enumerate(scratch):
-        queries = jnp.dot(ref[...], wq_ref[...], preferred_element_type=f32)
-        q_ref[index * TILE : (index + 1) * TILE] = (queries * query_factor).astype(bf16)
 
 
 def edge_projections(latent, context, gain, weights, pieces):
@@ -265,27 +270,22 @@
     return call(
         functools.partial(edge_kernel, len(pieces)),
         [
-            array((2 * TILE, out)),
+            *[array((TILE, width))] * 2,
             *[array((2, TILE, out))] * 4,
             array((2, context.shape[0], out)),
             array((1, width), f32),
             array((1, width), f32),
         ],
-        in_specs=[whole()] * (6 + len(pieces)),
-        out_specs=[whole()] * 8,
-        scratch_shapes=[
-            VMEM((1, width), f32),
-            VMEM((1, width), f32),
-            VMEM((TILE, width), bf16),
-            VMEM((TILE, width), bf16),
-        ],
+        in_specs=[whole()] * (5 + len(pieces)),
+        out_specs=[whole()] * 9,
+        scratch_shapes=[VMEM((1, width), f32)] * 2,
         flops=2_000_000_000,
-    )(latent, context, gain, *weights, *pieces)
-
-
-def main_kernel(x_ref, a_ref, b_ref, wq_ref, wk_ref, wv_ref, qe_ref, low_ref, high_ref, *rest):
+    )(latent, context, gain, *weights[1:], *pieces)
+
+
+def main_kernel(pad, x_ref, a_ref, b_ref, wq_ref, wk_ref, wv_ref, one_ref, two_ref, low_ref, high_ref, *rest):
     q_ref, k_ref, v_ref, *scratch = rest
-    tokens, width = k_ref.shape
+    tokens, width = q_ref.shape
     tiles = tokens // TILE
 
     def load(index):
@@ -294,6 +294,7 @@
 
     def values_at(start, values):
         turned = values.T
+        start += pad
         v_ref[0, 0:width, start : start + TILE] = turned.astype(bf16)
         rolled = pltpu.roll(turned, TILE - GRID_W, 1).astype(bf16)
         v_ref[1, 0:width, start : start + TILE - GRID_W] = rolled[:, 0 : TILE - GRID_W]
@@ -307,39 +308,45 @@
         rows = slice(index * TILE, (index + 1) * TILE)
         queries = jnp.dot(hidden, wq_ref[...], preferred_element_type=f32)
         q_ref[rows] = (queries * query_factor).astype(bf16)
-        k_ref[rows] = keys
+        k_ref[pad + index * TILE : pad + (index + 1) * TILE] = keys
         values_at(index * TILE, values)
 
     load(1)
-    q_ref[0:TILE] = qe_ref[0:TILE]
-    q_ref[tokens - TILE :] = qe_ref[TILE:]
-    k_ref[0:TILE] = low_ref[0]
-    k_ref[tokens - TILE :] = high_ref[0]
-    v_ref[0, width:, :] = jnp.ones((ONES, tokens), bf16)
-    v_ref[1, width:, :] = jnp.ones((ONES, tokens), bf16)
+    for start, ref in ((0, one_ref), (tokens - TILE, two_ref)):
+        queries = jnp.dot(ref[...], wq_ref[...], preferred_element_type=f32)
+        q_ref[start : start + TILE] = (queries * query_factor).astype(bf16)
+    k_ref[pad : pad + TILE] = low_ref[0]
+    k_ref[pad + tokens - TILE : pad + tokens] = high_ref[0]
+    for index in range(2):
+        v_ref[index, width:, :] = jnp.ones((ONES, tokens + 2 * pad), bf16)
     values_at(0, low_ref[1].astype(f32))
     for index in range(1, tiles - 1):
         if index + 2 < tiles:
             load(index + 1)
         multiply(index)
     values_at(tokens - TILE, high_ref[1].astype(f32))
-    v_ref[1, 0:width, tokens - GRID_W :] = jnp.zeros((width, GRID_W), bf16)
-
-
-def main_projections(latent, a, b, weights, edges):
+    if not pad:
+        v_ref[1, 0:width, tokens - GRID_W :] = jnp.zeros((width, GRID_W), bf16)
+
+
+def main_projections(latent, a, b, weights, edges, pad):
     tokens, width = latent.shape
     out = weights[0].shape[1]
     return call(
-        main_kernel,
-        [array((tokens, out)), array((tokens, out)), array((2, out + ONES, tokens))],
-        in_specs=[whole()] * 9,
+        functools.partial(main_kernel, pad),
+        [
+            array((tokens, out)),
+            array((tokens + 2 * pad, out)),
+            array((2, out + ONES, tokens + 2 * pad)),
+        ],
+        in_specs=[whole()] * 10,
         out_specs=[whole()] * 3,
         scratch_shapes=[VMEM((TILE, width), bf16), VMEM((TILE, width), bf16)],
         flops=5_000_000_000,
     )(latent, a, b, *weights, *edges)
 
 
-def attend_rows(rows, q_ref, kc_ref, vc_ref, t_ref, out_ref, scores, probs):
+def attend_rows(rows, q_ref, kc_ref, vc_ref, t_ref, out_ref, scores, probs, whole_rows=True):
     width = q_ref.shape[1]
     heads = width // HEAD_DIM
     lane_head = lax.broadcasted_iota(jnp.int32, (1, width), 1) // HEAD_DIM
@@ -348,9 +355,9 @@
     dims = (((1,), (1,)), ((), ()))
 
     def score(index):
-        row, k_ref, _, start, offset = rows[index]
+        row, k_ref, _, start, offset, _ = rows[index]
         s_ref = scores[index % len(scores)]
-        q = q_ref[row * GRID_W : (row + 1) * GRID_W, :]
+        q = q_ref[part(row * GRID_W, GRID_W, GRID_W), :]
         big = jnp.concatenate([q * mask for mask in head_mask], axis=0)
         keys = k_ref[part(start * GRID_W, GRID_W, NEAR), :]
         near = lax.dot_general(keys, big, dims, preferred_element_type=f32)
@@ -367,15 +374,16 @@
         p_ref[...] = jnp.exp2(s_ref[...] - peak).astype(bf16)
 
     def gather(index):
-        _, _, v_ref, start, _ = rows[index]
+        _, _, v_ref, start, _, parity = rows[index]
         p_ref = probs[index % len(probs)]
-        values = v_ref[start % 2, :, part(start // 2 * LANES, LANES, NEAR)]
+        parity = start % 2 if parity is None else parity
+        values = v_ref[parity, :, part(start // 2 * LANES, LANES, NEAR)]
         out = jnp.dot(values, p_ref[0:NEAR, :], preferred_element_type=f32)
         out += jnp.dot(vc_ref[...], p_ref[NEAR:, :], preferred_element_type=f32)
         return out[0:width] * (1.0 / out[width : width + 1])
 
     def store(index, left, right):
-        row = rows[index][0]
+        row = rows[index][0] if whole_rows else index
         lanes = slice(row * GRID_W, row * GRID_W + LANES)
         for pair in range(heads // 2):
             cols = slice(pair * LANES, (pair + 1) * LANES)
@@ -437,15 +445,15 @@
     plan = []
     for row in rows:
         if is_free(row, grid_rows):
-            plan.append((row, k_ref, v_ref, row - HALO_ROWS, WIN_ROWS - 1 - HALO_ROWS))
+            plan.append((row, k_ref, v_ref, row - HALO_ROWS, WIN_ROWS - 1 - HALO_ROWS, None))
             continue
         kl_ref, kh_ref, vl_ref, vh_ref = strips
         first = jnp.clip(own + row - HALO_ROWS, 0, total - WIN_ROWS)
         offset = first - (own + row) + WIN_ROWS - 1
         if row < HALO_ROWS:
-            plan.append((row, kl_ref, vl_ref, first - own + HALO_ROWS, offset))
+            plan.append((row, kl_ref, vl_ref, first - own + HALO_ROWS, offset, None))
         else:
-            plan.append((row, kh_ref, vh_ref, first - own - (grid_rows - WIN_ROWS), offset))
+            plan.append((row, kh_ref, vh_ref, first - own - (grid_rows - WIN_ROWS), offset, None))
     return plan
 
 
@@ -593,6 +601,174 @@
     )
 
 
+def by_destination(tokens):
+    each = tokens // GRID_W // 4
+    return lax.axis_size("tp") == 4 and each % 2 == 0 and HALO_ROWS <= each
+
+
+def free_target():
+    return jnp.where(lax.axis_index("tp") < 2, 2, 1)
+
+
+def halo_target():
+    return jnp.where(lax.axis_index("tp") < 2, 3, 0)
+
+
+def destination_plan(owner, tokens, sp_count, k_ref, v_ref, free):
+    grid_rows = tokens // GRID_W
+    each = grid_rows // 4
+    own = lax.axis_index("sp") * grid_rows
+    plan = []
+    for index in range(each):
+        row = owner * each + index
+        if free:
+            plan.append((row, k_ref, v_ref, row, WIN_ROWS - 1 - HALO_ROWS, index % 2))
+            continue
+        first = jnp.clip(own + row - HALO_ROWS, 0, grid_rows * sp_count - WIN_ROWS)
+        offset = first - (own + row) + WIN_ROWS - 1
+        plan.append((row, k_ref, v_ref, first - own + HALO_ROWS, offset, None))
+    return plan
+
+
+def first_kernel(count, k_in, v_in, q_ref, t_ref, *rest):
+    contexts, (k_ref, v_ref, kc_ref, vc_ref, out_ref, *scratch) = rest[:count], rest[count:]
+    far_refs(contexts, kc_ref, vc_ref)
+    plan = destination_plan(free_target(), q_ref.shape[0], 0, k_ref, v_ref, True)
+    attend_rows(
+        plan, q_ref, kc_ref, vc_ref, t_ref, out_ref, scratch[0:2], scratch[2:4], whole_rows=False
+    )
+
+
+def second_kernel(sp_count, k_in, v_in, latent_ref, q_ref, kc_ref, vc_ref, t_ref, one_ref, two_ref, k_ref, v_ref, own_ref, out_ref, sem, *scratch):
+    share = own_ref.shape[0]
+    mine = part(lax.axis_index("tp") * share, GRID_W, share)
+    copy = pltpu.make_async_copy(latent_ref.at[mine], own_ref, sem)
+    copy.start()
+    tokens, width = q_ref.shape
+    even = lax.axis_index("sp") % 2 == 0
+    low = jnp.where(even, two_ref[...], one_ref[...])
+    high = jnp.where(even, one_ref[...], two_ref[...])
+    end = TILE + tokens
+    k_ref[0:TILE] = low[0]
+    k_ref[end:] = high[0]
+    turned = low[1].astype(f32).T
+    rolled = pltpu.roll(turned, TILE - GRID_W, 1).astype(bf16)
+    v_ref[0, 0:width, 0:TILE] = turned.astype(bf16)
+    v_ref[1, 0:width, 0 : TILE - GRID_W] = rolled[:, 0 : TILE - GRID_W]
+    turned = high[1].astype(f32).T
+    rolled = pltpu.roll(turned, TILE - GRID_W, 1).astype(bf16)
+    v_ref[0, 0:width, end:] = turned.astype(bf16)
+    v_ref[1, 0:width, end - GRID_W : end] = rolled[:, TILE - GRID_W :]
+    v_ref[1, 0:width, end : end + TILE - GRID_W] = rolled[:, 0 : TILE - GRID_W]
+    v_ref[1, 0:width, end + TILE - GRID_W :] = jnp.zeros((width, GRID_W), bf16)
+    plan = destination_plan(halo_target(), tokens, sp_count, k_ref, v_ref, False)
+    attend_rows(
+        plan, q_ref, kc_ref, vc_ref, t_ref, out_ref, scratch[0:2], scratch[2:4], whole_rows=False
+    )
+    copy.wait()
+
+
+def near_kernel(step, sp_count, k_ref, v_ref, q_ref, kc_ref, vc_ref, t_ref, out_ref, *scratch):
+    owner = target("tp", step)
+    plan = destination_plan(owner, q_ref.shape[0], sp_count, k_ref, v_ref, False)
+    attend_rows(
+        plan, q_ref, kc_ref, vc_ref, t_ref, out_ref, scratch[0:2], scratch[2:4], whole_rows=False
+    )
+
+
+def destination_attention(latent, queries, keys, values, table, contexts, one, two):
+    tokens, width = queries.shape
+    far = len(contexts) * contexts[0].shape[1]
+    sp_count = lax.axis_size("sp")
+    share = tokens // 4
+    scratch = attention_scratch(NEAR + far, width)
+    padded = [array(keys.shape), array(values.shape)]
+    keys, values, far_keys, far_values, block = call(
+        functools.partial(first_kernel, len(contexts)),
+        [*padded, array((far, width)), array((width + ONES, far)), array((width, share))],
+        in_specs=[whole()] * (4 + len(contexts)),
+        out_specs=[whole()] * 5,
+        input_output_aliases={0: 0, 1: 1},
+        scratch_shapes=scratch,
+        flops=3_000_000_000,
+    )(keys, values, queries, table, *contexts)
+    x1 = exchange(block, "tp", 2)
+    keys, values, own, block = call(
+        functools.partial(second_kernel, sp_count),
+        [*padded, array((share, latent.shape[1])), array((width, share))],
+        in_specs=[whole()] * 2 + [whole(HBM)] + [whole()] * 6,
+        out_specs=[whole()] * 4,
+        input_output_aliases={0: 0, 1: 1},
+        scratch_shapes=[pltpu.SemaphoreType.DMA] + scratch,
+        flops=3_000_000_000,
+    )(keys, values, *in_hbm([latent]), queries, far_keys, far_values, table, one, two)
+    x2 = exchange(block, "tp", 2)
+    blocks = []
+    for step in (1, 0):
+        blocks.append(
+            call(
+                functools.partial(near_kernel, step, sp_count),
+                array((width, share)),
+                in_specs=[whole()] * 6,
+                out_specs=whole(),
+                scratch_shapes=scratch,
+                flops=3_000_000_000,
+            )(keys, values, queries, far_keys, far_values, table)
+        )
+    neighbour = exchange(blocks[0], "tp", 1)
+    passed1 = exchange(x1, "tp", 1)
+    passed2 = exchange(x2, "tp", 1)
+    return own, (blocks[1], neighbour, x1, x2, passed1, passed2)
+
+
+def gather_kernel(x_ref, w_ref, *rest):
+    pieces, blocks, (out_ref, gate_ref, held_ref, block_ref, sems) = rest[:4], rest[4:10], rest[10:]
+    mine_ref, neighbour_ref, x1_ref, x2_ref, passed1_ref, passed2_ref = blocks
+    height = mine_ref.shape[0]
+    tile = w_ref.shape[1] // 4
+    tp = lax.axis_index("tp")
+    free = (tp == 1) | (tp == 2)
+    for index in range(4):
+        gate_ref[:, part(origin("tp", index) * tile, LANES, tile)] = pieces[index][4:5, :]
+    values = (
+        mine_ref[...],
+        neighbour_ref[...],
+        jnp.where(free, x1_ref[...], x2_ref[...]),
+        jnp.where(free, passed1_ref[...], passed2_ref[...]),
+    )
+    for index, value in enumerate(values):
+        rows = part(origin("tp", index) * height, LANES, height)
+        block_ref[:, rows] = value.astype(f32).T.astype(bf16)
+    copies = []
+    for step in range(4):
+        cols = slice(step * tile, (step + 1) * tile)
+        total = jnp.dot(block_ref[...], w_ref[:, cols], preferred_element_type=f32)
+        held_ref[:, cols] = (x_ref[:, cols].astype(f32) + gate_ref[:, cols] * total).astype(bf16)
+        copies.append(
+            pltpu.make_async_copy(held_ref.at[:, cols], out_ref.at[:, cols], sems.at[step])
+        )
+        copies[-1].start()
+    for copy in copies:
+        copy.wait()
+
+
+def gathered_output(x, weight, blocks, pieces):
+    share, width = x.shape
+    return call(
+        gather_kernel,
+        array((share, width)),
+        in_specs=[whole()] * 12,
+        out_specs=whole(HBM),
+        scratch_shapes=[
+            VMEM((1, width), f32),
+            VMEM((share, width), bf16),
+            VMEM((share, weight.shape[0]), bf16),
+            pltpu.SemaphoreType.DMA((4,)),
+        ],
+        flops=2_000_000_000,
+    )(x, weight, *pieces, *blocks)
+
+
 def output_kernel(count, late, *refs):
     x_ref, w_ref, *arrays, out_ref, gate_ref, held_ref, block_ref, sems = refs[late:]
     pieces, blocks = arrays[:count], arrays[count:]
@@ -644,7 +820,10 @@
 
 
 def gathered(block, axis):
-    return [block] + [exchange(block, axis, step) for step in range(1, lax.axis_size(axis))]
+    blocks = [block]
+    for step in range(1, lax.axis_size(axis)):
+        blocks.append(exchange(block, axis, step))
+    return blocks
 
 
 def sent(blocks):
@@ -670,10 +849,10 @@
         condition, context_condition, shift_weight, scale_weight, gate_weight, norm_gain
     )
     partials = gathered(terms, "sp")
-    wk, wv, rows = bias_rows(terms, offset_bias, key_weight, value_weight)
+    wk, rows = bias_rows(terms, offset_bias, key_weight)
     summed = summed_terms(rows, partials)
     pieces = gathered(summed, "tp")
-    wq, table = bias_table(summed, rows, query_weight)
+    wv, wq, table = bias_table(summed, rows, value_weight, query_weight)
     weights = (wq, wk, wv)
     *edges, far, a, b = edge_projections(
         latent, context_tokens, gain, weights, pieces
@@ -681,10 +860,14 @@
     count = lax.axis_size("sp")
     contexts = gathered(far, "sp")
     pairs = [(i, i ^ 1) for i in range(count) if i ^ 1 < count]
-    first = lax.ppermute(edges[3], "sp", pairs)
+    first = lax.ppermute(edges[4], "sp", pairs)
     pairs = [(i, j) for i in range(count) for j in [((i + 1) ^ 1) - 1] if 0 <= j < count]
-    second = lax.ppermute(edges[4], "sp", pairs)
-    fields = main_projections(latent, a, b, weights, edges[:3])
+    second = lax.ppermute(edges[5], "sp", pairs)
+    special = by_destination(latent.shape[0])
+    fields = main_projections(latent, a, b, weights, edges[:4], TILE if special else 0)
+    if special:
+        own, blocks = destination_attention(latent, *fields, table, contexts, first, second)
+        return gathered_output(own, out_weight, blocks, pieces)
     inner, *fars = inner_attention(*fields, table, contexts)
     own, strips, early = middle_attention(inner, latent, *fields, *fars, table, first, second)
     early = sent(early)

time: 48.4 us -> 47.8 us (0.988); the launches traced: 48.2 us -> 47.1 us
  waiting for transfers between devices: 2.79 us -> 0.52 us
  starting transfers between devices: 20.6 us -> 21.8 us
    ppermute x15 -> x14, waiting for transfers between devices: 2.79 us -> 0.51 us  [exchange(): return lax.ppermute(block, axis, [(i, i ^ step) for i in range(count)])]
    ppermute x15 -> x14, starting transfers between devices: 16.7 us -> 18 us  [exchange(): return lax.ppermute(block, axis, [(i, i ^ step) for i in range(count)])]
  transfers between devices with their start and end apart: 17 -> 16, of which waited for: 2 -> 1; matrix products, arithmetic and copies ran while one was open for 0% -> 0% of each run, Pallas kernels for 33% -> 38%
where the time goes in v4:
time: 47.8 us; the launch traced here: 47.1 us
  Pallas kernels  24.4 us (51%)
  starting transfers between devices  21.8 us (46%)
  waiting for transfers between devices  0.52 us (1%)
    ppermute x14, starting transfers between devices, exchange(): return lax.ppermute(block, axis, [(i, i ^ step) for i in range(count)])  18 us
    pallas_call x1, Pallas kernels, main_projections(): call(functools.partial(main_kernel, pad), [array((tokens, out)), array((t...  4.76 us
    pallas_call x2, Pallas kernels, destination_attention(): call(functools.partial(near_kernel, step, sp_count), array((width, share)...  4.37 us
    pallas_call x1, Pallas kernels, destination_attention(): call(functools.partial(second_kernel, sp_count), [*padded, array((share,...  3.43 us
    pallas_call x1, Pallas kernels, gathered_output(): call(gather_kernel, array((share, width)), in_specs=[whole()] * 12, out_s...  2.84 us
    ppermute x1, starting transfers between devices, local(): second = lax.ppermute(edges[5], 'sp', pairs)  2.36 us
    pallas_call x1, Pallas kernels, destination_attention(): call(functools.partial(first_kernel, len(contexts)), [*padded, array((far...  2.18 us
    pallas_call x1, Pallas kernels, edge_projections(): call(functools.partial(edge_kernel, len(pieces)), [*[array((TILE, width))...  1.98 us
  transfers between devices with their start and end apart: 16, of which 1 were waited for; matrix products, arithmetic and copies ran while one was open for 0% of the time, Pallas kernels for 38%

profile of v4, /device:TPU:9, one launch (start us, length us, event | category | flops | bytes accessed | tf_op | source)
XLA Modules:
  0.0 47.1 jit_solution(22969702275534507)
XLA Ops:
  0.0 1.7 %shard_map.127 = (f32[8,512]{1,0:T(8,128)S(1)}, f32[1,2048]{1,0:T(1,128)S(1)}) custom-call(bf16[2048]{0:T(1024)(128)(2,1)} %refs_0_.3, bf16[2048]{0:T(1024)(128)(2,1)} %refs_1_.2, bf16[512,512]{1,0:T(8,128)(2,1)} %refs_2_.1, bf16[512,512]{1,0:T(8,128)(2,1)} %refs_3_.1, bf16[512,512]{1,0:T(8,128)(2,1)} %refs_4_.1, bf16[2048]{0:T(1024)(128)(2,1)} %refs_5_.1), custom_call_target="tpu_custom_call" | custom-call | flops 3000000000 | tf_op jit(solution)/shard_map/pallas_call | solution.py:116
  1.7 1.4 %collective-permute-start.2 = (f32[8,512]{1,0:T(8,128)S(1)}, f32[8,512]{1,0:T(8,128)S(1)}, u32[]{:S(2)}, u32[]{:S(2)}) collective-permute-start(f32[8,512]{1,0:T(8,128)S(1)} %get-tuple-element.34.token_ref.refs_0_), channel_id=1, source_target_pairs={{0,12},{4,8},{8,4},{12,0},{1,13},{5,9},{9,5},{13,1},{2,14},{6,10},... | collective-permute-start | bytes 49160 | tf_op jit(solution)/shard_map/ppermute | solution.py:44
  3.1 1.1 %collective-permute-start.1 = (f32[8,512]{1,0:T(8,128)S(1)}, f32[8,512]{1,0:T(8,128)S(1)}, u32[]{:S(2)}, u32[]{:S(2)}) collective-permute-start(f32[8,512]{1,0:T(8,128)S(1)} %get-tuple-element.34.token_ref.refs_0_), channel_id=1, source_target_pairs={{0,8},{4,12},{8,0},{12,4},{1,9},{5,13},{9,1},{13,5},{2,10},{6,14},... | collective-permute-start | bytes 49160 | tf_op jit(solution)/shard_map/ppermute | solution.py:44
  4.2 1.1 %collective-permute-start = (f32[8,512]{1,0:T(8,128)S(1)}, f32[8,512]{1,0:T(8,128)S(1)}, u32[]{:S(2)}, u32[]{:S(2)}) collective-permute-start(f32[8,512]{1,0:T(8,128)S(1)} %get-tuple-element.34.token_ref.refs_0_), channel_id=1, source_target_pairs={{0,4},{4,0},{8,12},{12,8},{1,5},{5,1},{9,13},{13,9},{2,6},{6,2},{1... | collective-permute-start | bytes 49160 | tf_op jit(solution)/shard_map/ppermute | solution.py:44
  5.3 1.5 %shard_map.128 = (bf16[2048,256]{1,0:T(8,128)(2,1)S(1)}, f32[256,1024]{1,0:T(8,128)S(1)}) custom-call(f32[8,512]{1,0:T(8,128)S(1)} %get-tuple-element.34.token_ref.refs_0_, f32[15,4,31]{2,1,0:T(4,128)} %bitcast.1, bf16[2048,256]{1,0:T(8,128)(2,1)} %refs_0_.4), custom_call_target="tpu_custom_call" | custom-call | flops 500000000 | tf_op jit(solution)/shard_map/pallas_call | solution.py:180
  6.8 0.0 collective-permute-done.2.refs_3_
  6.8 0.0 collective-permute-done.1.refs_2_
  6.8 0.0 copy-start.2
  6.8 3.3 %collective-permute-start.5 = (f32[8,512]{1,0:T(8,128)S(1)}, f32[8,512]{1,0:T(8,128)S(1)}, u32[]{:S(2)}, u32[]{:S(2)}) collective-permute-start(f32[8,512]{1,0:T(8,128)S(1)} %shard_map.129.token_ref.rest_0_), channel_id=1, source_target_pairs={{0,3},{1,2},{2,1},{3,0},{4,7},{5,6},{6,5},{7,4},{8,11},{9,10},{10,... | collective-permute-start | bytes 49160 | tf_op jit(solution)/shard_map/ppermute | solution.py:44
  10.2 0.1 collective-permute-start.4
  10.3 0.4 collective-permute-start.3
  10.6 1.6 %shard_map.130 = (bf16[2048,256]{1,0:T(8,128)(2,1)S(1)}, bf16[2048,256]{1,0:T(8,128)(2,1)S(1)}, f32[1024,256]{1,0:T(8,128)S(1)}) custom-call(f32[8,512]{1,0:T(8,128)S(1)} %shard_map.129.token_ref.rest_0_, f32[256,1024]{1,0:T(8,128)S(1)} %get-tuple-element.36.token_ref.table_ref, bf16[2048,256]{1,0:T(8,128)(2,1)} %refs_0_.5, bf16[2048,256]{1,0:T(8,128)(2,1)} %refs_1_.3), custom_call_target="tpu_custom_call" | custom-call | flops 1000000000 | tf_op jit(solution)/shard_map/pallas_call | solution.py:217
  12.3 0.5 %collective-permute-done.4.rest_2_ = f32[8,512]{1,0:T(8,128)S(1)} collective-permute-done((f32[8,512]{1,0:T(8,128)S(1)}, f32[8,512]{1,0:T(8,128)S(1)}, u32[]{:S(2)}, u32[]{:S(2)}) %collective-permute-start.4) | collective-permute-done | bytes 16416 | tf_op jit(solution)/shard_map/ppermute | solution.py:44
  12.8 2.0 %shard_map.131 = (bf16[256,2048]{1,0:T(8,128)(2,1)S(1)}, bf16[256,2048]{1,0:T(8,128)(2,1)S(1)}, bf16[2,256,256]{2,1,0:T(8,128)(2,1)S(1)}, bf16[2,256,256]{2,1,0:...) custom-call(bf16[1536,2048]{1,0:T(8,128)(2,1)S(1)} %copy-done, ...), custom_call_target="tpu_custom_call" | custom-call | flops 2000000000 | tf_op jit(solution)/shard_map/pallas_call | solution.py:270
  14.8 2.5 %collective-permute-start.8 = (bf16[2,64,256]{2,1,0:T(8,128)(2,1)S(1)}, bf16[2,64,256]{2,1,0:T(8,128)(2,1)S(1)}, u32[]{:S(2)}, u32[]{:S(2)}) collective-permute-start(bf16[2,64,256]{2,1,0:T(8,128)(2,1)S(1)} %get-tuple-element.49.rest_0_), channel_id=1, source_target_pairs={{0,12},{4,8},{8,4},{12,0},{1,13},{5,9},{9,5},{13,1},{2,14},{6,10},... | collective-permute-start | bytes 196616 | tf_op jit(solution)/shard_map/ppermute | solution.py:44
  17.2 1.5 %collective-permute-start.7 = (bf16[2,64,256]{2,1,0:T(8,128)(2,1)S(1)}, bf16[2,64,256]{2,1,0:T(8,128)(2,1)S(1)}, u32[]{:S(2)}, u32[]{:S(2)}) collective-permute-start(bf16[2,64,256]{2,1,0:T(8,128)(2,1)S(1)} %get-tuple-element.49.rest_0_), channel_id=1, source_target_pairs={{0,8},{4,12},{8,0},{12,4},{1,9},{5,13},{9,1},{13,5},{2,10},{6,14},... | collective-permute-start | bytes 196616 | tf_op jit(solution)/shard_map/ppermute | solution.py:44
  18.8 0.0 collective-permute-start.6
  18.8 1.5 %collective-permute-start.9 = (bf16[2,256,256]{2,1,0:T(8,128)(2,1)S(1)}, bf16[2,256,256]{2,1,0:T(8,128)(2,1)S(1)}, u32[]{:S(2)}, u32[]{:S(2)}) collective-permute-start(bf16[2,256,256]{2,1,0:T(8,128)(2,1)S(1)} %get-tuple-element.54), channel_id=1, source_target_pairs={{0,4},{4,0},{8,12},{12,8},{1,5},{5,1},{9,13},{13,9},{2,6},{6,2},{1... | collective-permute-start | bytes 786440 | tf_op jit(solution)/shard_map/ppermute | solution.py:863
  20.2 2.4 %collective-permute-start.10 = (bf16[2,256,256]{2,1,0:T(8,128)(2,1)S(1)}, bf16[2,256,256]{2,1,0:T(8,128)(2,1)S(1)}, u32[]{:S(2)}, u32[]{:S(2)}) collective-permute-start(bf16[2,256,256]{2,1,0:T(8,128)(2,1)S(1)} %get-tuple-element.55), channel_id=1, source_target_pairs={{4,8},{8,4},{5,9},{9,5},{6,10},{10,6},{7,11},{11,7},{20,24},{24,20... | collective-permute-start | bytes 786440 | tf_op jit(solution)/shard_map/ppermute | solution.py:865
  22.6 4.8 %shard_map.132 = (bf16[1536,256]{1,0:T(8,128)(2,1)S(1)}, bf16[2048,256]{1,0:T(8,128)(2,1)S(1)}, bf16[2,272,2048]{2,1,0:T(8,128)(2,1)S(1)}) custom-call(bf16[1536,2048]{1,0:T(8,128)(2,1)S(1)} %copy-done, f32[1,2048]{1,0:T(1,128)S(1)} %get-tuple-element.38.a_ref, f32[1,2048]{1,0:T(1,128)S(1)} %get-tuple-element.39.b_ref, ...), custom_call_target="tpu_custom_call" | custom-call | flops 5000000000 | tf_op jit(solution)/shard_map/pallas_call | solution.py:335
  27.4 0.0 collective-permute-done.8.rest_3_
  27.4 2.2 %shard_map.133 = (bf16[2048,256]{1,0:T(8,128)(2,1)S(1)}, bf16[2,272,2048]{2,1,0:T(8,128)(2,1)S(1)}, bf16[256,256]{1,0:T(8,128)(2,1)S(1)}, bf16[272,256]{1,0:T(8,128)(2,1)S(1)}, bf16[256,384]{1,0:T(8,128)(2,1)S(1)}) custom-call(bf16[2048,256]{1,0:T(8,128)(2,1)S(1)} %get-tuple-element.45.k_in, ...), custom_call_target="tpu_custom_call", output_to_operand_aliasing={{0}: (0, {}), {1}: (1, {})} | custom-call | flops 3000000000 | tf_op jit(solution)/shard_map/pallas_call | solution.py:686
  29.6 0.6 %collective-permute-start.12 = (bf16[256,384]{1,0:T(8,128)(2,1)S(1)}, bf16[256,384]{1,0:T(8,128)(2,1)S(1)}, u32[]{:S(2)}, u32[]{:S(2)}) collective-permute-start(bf16[256,384]{1,0:T(8,128)(2,1)S(1)} %get-tuple-element.59), channel_id=1, source_target_pairs={{0,2},{1,3},{2,0},{3,1},{4,6},{5,7},{6,4},{7,5},{8,10},{9,11},{10,... | collective-permute-start | bytes 589832 | tf_op jit(solution)/shard_map/ppermute | solution.py:44
  30.2 3.4 %shard_map.134 = (bf16[2048,256]{1,0:T(8,128)(2,1)S(1)}, bf16[2,272,2048]{2,1,0:T(8,128)(2,1)S(1)}, bf16[384,2048]{1,0:T(8,128)(2,1)S(1)}, bf16[256,384]{1,0:T(8,128)(2,1)S(1)}) custom-call(bf16[2048,256]{1,0:T(8,128)(2,1)S(1)} %get-tuple-element.50.k_in, ...), custom_call_target="tpu_custom_call", output_to_operand_aliasing={{0}: (0, {}), {1}: (1, {})} | custom-call | flops 3000000000 | tf_op jit(solution)/shard_map/pallas_call | solution.py:696
  33.7 0.9 %collective-permute-start.13 = (bf16[256,384]{1,0:T(8,128)(2,1)S(1)}, bf16[256,384]{1,0:T(8,128)(2,1)S(1)}, u32[]{:S(2)}, u32[]{:S(2)}) collective-permute-start(bf16[256,384]{1,0:T(8,128)(2,1)S(1)} %get-tuple-element.60), channel_id=1, source_target_pairs={{0,2},{1,3},{2,0},{3,1},{4,6},{5,7},{6,4},{7,5},{8,10},{9,11},{10,... | collective-permute-start | bytes 589832 | tf_op jit(solution)/shard_map/ppermute | solution.py:44
  34.6 2.2 %shard_map.136 = bf16[256,384]{1,0:T(8,128)(2,1)S(1)} custom-call(bf16[2048,256]{1,0:T(8,128)(2,1)S(1)} %get-tuple-element.57.k_ref, bf16[2,272,2048]{2,1,0:T(8,128)(2,1)S(1)} %get-tuple-element.58.v_ref, bf16[1536,256]{1,0:T(8,128)(2,1)S(1)} %get-tuple-element.47.q_ref, bf16[256,256]{1,0:T(8,128)(2,1)S(1)} %get-tuple-element.52.kc_ref, ...), custom_call_target="tpu_custom_call" | custom-call | flops 3000000000 | tf_op jit(solution)/shard_map/pallas_call | solution.py:709
  36.8 0.0 copy-start.1
  36.8 2.2 %collective-permute-start.11 = (bf16[256,384]{1,0:T(8,128)(2,1)S(1)}, bf16[256,384]{1,0:T(8,128)(2,1)S(1)}, u32[]{:S(2)}, u32[]{:S(2)}) collective-permute-start(bf16[256,384]{1,0:T(8,128)(2,1)S(1)} %shard_map.136), channel_id=1, source_target_pairs={{0,1},{1,0},{2,3},{3,2},{4,5},{5,4},{6,7},{7,6},{8,9},{9,8},{10,11... | collective-permute-start | bytes 589832 | tf_op jit(solution)/shard_map/ppermute | solution.py:44
  39.0 0.1 collective-permute-start.14
  39.1 2.8 %collective-permute-start.15 = (bf16[256,384]{1,0:T(8,128)(2,1)S(1)}, bf16[256,384]{1,0:T(8,128)(2,1)S(1)}, u32[]{:S(2)}, u32[]{:S(2)}) collective-permute-start(bf16[256,384]{1,0:T(8,128)(2,1)S(1)} %collective-permute-done.13.rest_7_), channel_id=1, source_target_pairs={{0,1},{1,0},{2,3},{3,2},{4,5},{5,4},{6,7},{7,6},{8,9},{9,8},{10,11... | collective-permute-start | bytes 589832 | tf_op jit(solution)/shard_map/ppermute | solution.py:44
  41.8 2.2 %shard_map.135.rest_4_ = bf16[256,384]{1,0:T(8,128)(2,1)S(1)} custom-call(bf16[2048,256]{1,0:T(8,128)(2,1)S(1)} %get-tuple-element.57.k_ref, bf16[2,272,2048]{2,1,0:T(8,128)(2,1)S(1)} %get-tuple-element.58.v_ref, bf16[1536,256]{1,0:T(8,128)(2,1)S(1)} %get-tuple-element.47.q_ref, bf16[256,256]{1,0:T(8,128)(2,1)S(1)} %get-tuple-element.52.kc_ref, ...), custom_call_target="tpu_custom_call" | custom-call | flops 3000000000 | tf_op jit(solution)/shard_map/pallas_call | solution.py:709
  44.1 2.8 %shard_map.137 = bf16[384,2048]{1,0:T(8,128)(2,1)} custom-call(bf16[384,2048]{1,0:T(8,128)(2,1)S(1)} %get-tuple-element.56.x_ref, bf16[1024,2048]{1,0:T(8,128)(2,1)S(1)} %copy-done.1, f32[8,512]{1,0:T(8,128)S(1)} %shard_map.129.token_ref.rest_0_, f32[8,512]{1,0:T(8,128)S(1)} %collective-permute-done.3.rest_1_, f32[8,512]{1,0:T(8,128)S(1)} %collective-permute-done.4.rest_2_, ...), custom_call_target="tpu_custom_call" | custom-call | flops 2000000000 | tf_op jit(solution)/shard_map/pallas_call | solution.py:757
  (17 shorter events, 0.0 us)
Async XLA Ops:
  1.7 5.1 %collective-permute-start.2 = (f32[8,512]{1,0:T(8,128)S(1)}, f32[8,512]{1,0:T(8,128)S(1)}, u32[]{:S(2)}, u32[]{:S(2)}) collective-permute-start(f32[8,512]{1,0:T(8,128)S(1)} %get-tuple-element.34.token_ref.refs_0_), channel_id=1, source_target_pairs={{0,12},{4,8},{8,4},{12,0},{1,13},{5,9},{9,5},{13,1},{2,14},{6,10},... | collective-permute-start | bytes 49160 | tf_op jit(solution)/shard_map/ppermute | solution.py:44
  3.1 3.7 %collective-permute-start.1 = (f32[8,512]{1,0:T(8,128)S(1)}, f32[8,512]{1,0:T(8,128)S(1)}, u32[]{:S(2)}, u32[]{:S(2)}) collective-permute-start(f32[8,512]{1,0:T(8,128)S(1)} %get-tuple-element.34.token_ref.refs_0_), channel_id=1, source_target_pairs={{0,8},{4,12},{8,0},{12,4},{1,9},{5,13},{9,1},{13,5},{2,10},{6,14},... | collective-permute-start | bytes 49160 | tf_op jit(solution)/shard_map/ppermute | solution.py:44
  4.2 2.6 %collective-permute-start = (f32[8,512]{1,0:T(8,128)S(1)}, f32[8,512]{1,0:T(8,128)S(1)}, u32[]{:S(2)}, u32[]{:S(2)}) collective-permute-start(f32[8,512]{1,0:T(8,128)S(1)} %get-tuple-element.34.token_ref.refs_0_), channel_id=1, source_target_pairs={{0,4},{4,0},{8,12},{12,8},{1,5},{5,1},{9,13},{13,9},{2,6},{6,2},{1... | collective-permute-start | bytes 49160 | tf_op jit(solution)/shard_map/ppermute | solution.py:44
  5.3 7.5 %copy-start = (bf16[1536,2048]{1,0:T(8,128)(2,1)S(1)}, bf16[1536,2048]{1,0:T(8,128)(2,1)}, u32[]{:S(2)}) copy-start(bf16[1536,2048]{1,0:T(8,128)(2,1)} %latent_ref.1) | copy-start | bytes 18874372
  6.8 6.0 %copy-start.2 = (bf16[64,2048]{1,0:T(8,128)(2,1)S(1)}, bf16[64,2048]{1,0:T(8,128)(2,1)}, u32[]{:S(2)}) copy-start(bf16[64,2048]{1,0:T(8,128)(2,1)} %context_ref.1) | copy-start | bytes 786436
  6.8 5.5 %collective-permute-start.5 = (f32[8,512]{1,0:T(8,128)S(1)}, f32[8,512]{1,0:T(8,128)S(1)}, u32[]{:S(2)}, u32[]{:S(2)}) collective-permute-start(f32[8,512]{1,0:T(8,128)S(1)} %shard_map.129.token_ref.rest_0_), channel_id=1, source_target_pairs={{0,3},{1,2},{2,1},{3,0},{4,7},{5,6},{6,5},{7,4},{8,11},{9,10},{10,... | collective-permute-start | bytes 49160 | tf_op jit(solution)/shard_map/ppermute | solution.py:44
  10.2 2.6 %collective-permute-start.4 = (f32[8,512]{1,0:T(8,128)S(1)}, f32[8,512]{1,0:T(8,128)S(1)}, u32[]{:S(2)}, u32[]{:S(2)}) collective-permute-start(f32[8,512]{1,0:T(8,128)S(1)} %shard_map.129.token_ref.rest_0_), channel_id=1, source_target_pairs={{0,2},{1,3},{2,0},{3,1},{4,6},{5,7},{6,4},{7,5},{8,10},{9,11},{10,... | collective-permute-start | bytes 49160 | tf_op jit(solution)/shard_map/ppermute | solution.py:44
  10.3 2.5 %collective-permute-start.3 = (f32[8,512]{1,0:T(8,128)S(1)}, f32[8,512]{1,0:T(8,128)S(1)}, u32[]{:S(2)}, u32[]{:S(2)}) collective-permute-start(f32[8,512]{1,0:T(8,128)S(1)} %shard_map.129.token_ref.rest_0_), channel_id=1, source_target_pairs={{0,1},{1,0},{2,3},{3,2},{4,5},{5,4},{6,7},{7,6},{8,9},{9,8},{10,11... | collective-permute-start | bytes 49160 | tf_op jit(solution)/shard_map/ppermute | solution.py:44
  14.8 12.6 %collective-permute-start.8 = (bf16[2,64,256]{2,1,0:T(8,128)(2,1)S(1)}, bf16[2,64,256]{2,1,0:T(8,128)(2,1)S(1)}, u32[]{:S(2)}, u32[]{:S(2)}) collective-permute-start(bf16[2,64,256]{2,1,0:T(8,128)(2,1)S(1)} %get-tuple-element.49.rest_0_), channel_id=1, source_target_pairs={{0,12},{4,8},{8,4},{12,0},{1,13},{5,9},{9,5},{13,1},{2,14},{6,10},... | collective-permute-start | bytes 196616 | tf_op jit(solution)/shard_map/ppermute | solution.py:44
  17.2 10.1 %collective-permute-start.7 = (bf16[2,64,256]{2,1,0:T(8,128)(2,1)S(1)}, bf16[2,64,256]{2,1,0:T(8,128)(2,1)S(1)}, u32[]{:S(2)}, u32[]{:S(2)}) collective-permute-start(bf16[2,64,256]{2,1,0:T(8,128)(2,1)S(1)} %get-tuple-element.49.rest_0_), channel_id=1, source_target_pairs={{0,8},{4,12},{8,0},{12,4},{1,9},{5,13},{9,1},{13,5},{2,10},{6,14},... | collective-permute-start | bytes 196616 | tf_op jit(solution)/shard_map/ppermute | solution.py:44
  18.8 8.6 %collective-permute-start.6 = (bf16[2,64,256]{2,1,0:T(8,128)(2,1)S(1)}, bf16[2,64,256]{2,1,0:T(8,128)(2,1)S(1)}, u32[]{:S(2)}, u32[]{:S(2)}) collective-permute-start(bf16[2,64,256]{2,1,0:T(8,128)(2,1)S(1)} %get-tuple-element.49.rest_0_), channel_id=1, source_target_pairs={{0,4},{4,0},{8,12},{12,8},{1,5},{5,1},{9,13},{13,9},{2,6},{6,2},{1... | collective-permute-start | bytes 196616 | tf_op jit(solution)/shard_map/ppermute | solution.py:44
  18.8 11.5 %collective-permute-start.9 = (bf16[2,256,256]{2,1,0:T(8,128)(2,1)S(1)}, bf16[2,256,256]{2,1,0:T(8,128)(2,1)S(1)}, u32[]{:S(2)}, u32[]{:S(2)}) collective-permute-start(bf16[2,256,256]{2,1,0:T(8,128)(2,1)S(1)} %get-tuple-element.54), channel_id=1, source_target_pairs={{0,4},{4,0},{8,12},{12,8},{1,5},{5,1},{9,13},{13,9},{2,6},{6,2},{1... | collective-permute-start | bytes 786440 | tf_op jit(solution)/shard_map/ppermute | solution.py:863
  20.2 10.0 %collective-permute-start.10 = (bf16[2,256,256]{2,1,0:T(8,128)(2,1)S(1)}, bf16[2,256,256]{2,1,0:T(8,128)(2,1)S(1)}, u32[]{:S(2)}, u32[]{:S(2)}) collective-permute-start(bf16[2,256,256]{2,1,0:T(8,128)(2,1)S(1)} %get-tuple-element.55), channel_id=1, source_target_pairs={{4,8},{8,4},{5,9},{9,5},{6,10},{10,6},{7,11},{11,7},{20,24},{24,20... | collective-permute-start | bytes 786440 | tf_op jit(solution)/shard_map/ppermute | solution.py:865
  29.6 9.4 %collective-permute-start.12 = (bf16[256,384]{1,0:T(8,128)(2,1)S(1)}, bf16[256,384]{1,0:T(8,128)(2,1)S(1)}, u32[]{:S(2)}, u32[]{:S(2)}) collective-permute-start(bf16[256,384]{1,0:T(8,128)(2,1)S(1)} %get-tuple-element.59), channel_id=1, source_target_pairs={{0,2},{1,3},{2,0},{3,1},{4,6},{5,7},{6,4},{7,5},{8,10},{9,11},{10,... | collective-permute-start | bytes 589832 | tf_op jit(solution)/shard_map/ppermute | solution.py:44
  33.7 5.4 %collective-permute-start.13 = (bf16[256,384]{1,0:T(8,128)(2,1)S(1)}, bf16[256,384]{1,0:T(8,128)(2,1)S(1)}, u32[]{:S(2)}, u32[]{:S(2)}) collective-permute-start(bf16[256,384]{1,0:T(8,128)(2,1)S(1)} %get-tuple-element.60), channel_id=1, source_target_pairs={{0,2},{1,3},{2,0},{3,1},{4,6},{5,7},{6,4},{7,5},{8,10},{9,11},{10,... | collective-permute-start | bytes 589832 | tf_op jit(solution)/shard_map/ppermute | solution.py:44
  36.8 7.3 %copy-start.1 = (bf16[1024,2048]{1,0:T(8,128)(2,1)S(1)}, bf16[1024,2048]{1,0:T(8,128)(2,1)}, u32[]{:S(2)}) copy-start(bf16[1024,2048]{1,0:T(8,128)(2,1)} %w_ref.1) | copy-start | bytes 12582916
  36.8 7.3 %collective-permute-start.11 = (bf16[256,384]{1,0:T(8,128)(2,1)S(1)}, bf16[256,384]{1,0:T(8,128)(2,1)S(1)}, u32[]{:S(2)}, u32[]{:S(2)}) collective-permute-start(bf16[256,384]{1,0:T(8,128)(2,1)S(1)} %shard_map.136), channel_id=1, source_target_pairs={{0,1},{1,0},{2,3},{3,2},{4,5},{5,4},{6,7},{7,6},{8,9},{9,8},{10,11... | collective-permute-start | bytes 589832 | tf_op jit(solution)/shard_map/ppermute | solution.py:44
  39.0 5.1 %collective-permute-start.14 = (bf16[256,384]{1,0:T(8,128)(2,1)S(1)}, bf16[256,384]{1,0:T(8,128)(2,1)S(1)}, u32[]{:S(2)}, u32[]{:S(2)}) collective-permute-start(bf16[256,384]{1,0:T(8,128)(2,1)S(1)} %collective-permute-done.12.rest_6_), channel_id=1, source_target_pairs={{0,1},{1,0},{2,3},{3,2},{4,5},{5,4},{6,7},{7,6},{8,9},{9,8},{10,11... | collective-permute-start | bytes 589832 | tf_op jit(solution)/shard_map/ppermute | solution.py:44
  39.1 5.0 %collective-permute-start.15 = (bf16[256,384]{1,0:T(8,128)(2,1)S(1)}, bf16[256,384]{1,0:T(8,128)(2,1)S(1)}, u32[]{:S(2)}, u32[]{:S(2)}) collective-permute-start(bf16[256,384]{1,0:T(8,128)(2,1)S(1)} %collective-permute-done.13.rest_7_), channel_id=1, source_target_pairs={{0,1},{1,0},{2,3},{3,2},{4,5},{5,4},{6,7},{7,6},{8,9},{9,8},{10,11... | collective-permute-start | bytes 589832 | tf_op jit(solution)/shard_map/ppermute | solution.py:44

commit v5 on v4

--- a/solution.py
+++ b/solution.py
@@ -639,11 +639,7 @@
     )
 
 
-def second_kernel(sp_count, k_in, v_in, latent_ref, q_ref, kc_ref, vc_ref, t_ref, one_ref, two_ref, k_ref, v_ref, own_ref, out_ref, sem, *scratch):
-    share = own_ref.shape[0]
-    mine = part(lax.axis_index("tp") * share, GRID_W, share)
-    copy = pltpu.make_async_copy(latent_ref.at[mine], own_ref, sem)
-    copy.start()
+def second_kernel(sp_count, k_in, v_in, q_ref, kc_ref, vc_ref, t_ref, one_ref, two_ref, k_ref, v_ref, out_ref, *scratch):
     tokens, width = q_ref.shape
     even = lax.axis_index("sp") % 2 == 0
     low = jnp.where(even, two_ref[...], one_ref[...])
@@ -665,7 +661,6 @@
     attend_rows(
         plan, q_ref, kc_ref, vc_ref, t_ref, out_ref, scratch[0:2], scratch[2:4], whole_rows=False
     )
-    copy.wait()
 
 
 def near_kernel(step, sp_count, k_ref, v_ref, q_ref, kc_ref, vc_ref, t_ref, out_ref, *scratch):
@@ -676,7 +671,7 @@
     )
 
 
-def destination_attention(latent, queries, keys, values, table, contexts, one, two):
+def destination_attention(queries, keys, values, table, contexts, one, two):
     tokens, width = queries.shape
     far = len(contexts) * contexts[0].shape[1]
     sp_count = lax.axis_size("sp")
@@ -693,15 +688,15 @@
         flops=3_000_000_000,
     )(keys, values, queries, table, *contexts)
     x1 = exchange(block, "tp", 2)
-    keys, values, own, block = call(
+    keys, values, block = call(
         functools.partial(second_kernel, sp_count),
-        [*padded, array((share, latent.shape[1])), array((width, share))],
-        in_specs=[whole()] * 2 + [whole(HBM)] + [whole()] * 6,
-        out_specs=[whole()] * 4,
+        [*padded, array((width, share))],
+        in_specs=[whole()] * 8,
+        out_specs=[whole()] * 3,
         input_output_aliases={0: 0, 1: 1},
-        scratch_shapes=[pltpu.SemaphoreType.DMA] + scratch,
+        scratch_shapes=scratch,
         flops=3_000_000_000,
-    )(keys, values, *in_hbm([latent]), queries, far_keys, far_values, table, one, two)
+    )(keys, values, queries, far_keys, far_values, table, one, two)
     x2 = exchange(block, "tp", 2)
     blocks = []
     for step in (1, 0):
@@ -718,7 +713,7 @@
     neighbour = exchange(blocks[0], "tp", 1)
     passed1 = exchange(x1, "tp", 1)
     passed2 = exchange(x2, "tp", 1)
-    return own, (blocks[1], neighbour, x1, x2, passed1, passed2)
+    return blocks[1], neighbour, x1, x2, passed1, passed2
 
 
 def gather_kernel(x_ref, w_ref, *rest):
@@ -728,6 +723,7 @@
     tile = w_ref.shape[1] // 4
     tp = lax.axis_index("tp")
     free = (tp == 1) | (tp == 2)
+    mine = part(tp * held_ref.shape[0], GRID_W, held_ref.shape[0])
     for index in range(4):
         gate_ref[:, part(origin("tp", index) * tile, LANES, tile)] = pieces[index][4:5, :]
     values = (
@@ -743,7 +739,7 @@
     for step in range(4):
         cols = slice(step * tile, (step + 1) * tile)
         total = jnp.dot(block_ref[...], w_ref[:, cols], preferred_element_type=f32)
-        held_ref[:, cols] = (x_ref[:, cols].astype(f32) + gate_ref[:, cols] * total).astype(bf16)
+        held_ref[:, cols] = (x_ref[mine, cols].astype(f32) + gate_ref[:, cols] * total).astype(bf16)
         copies.append(
             pltpu.make_async_copy(held_ref.at[:, cols], out_ref.at[:, cols], sems.at[step])
         )
@@ -753,7 +749,7 @@
 
 
 def gathered_output(x, weight, blocks, pieces):
-    share, width = x.shape
+    share, width = x.shape[0] // 4, x.shape[1]
     return call(
         gather_kernel,
         array((share, width)),
@@ -866,8 +862,8 @@
     special = by_destination(latent.shape[0])
     fields = main_projections(latent, a, b, weights, edges[:4], TILE if special else 0)
     if special:
-        own, blocks = destination_attention(latent, *fields, table, contexts, first, second)
-        return gathered_output(own, out_weight, blocks, pieces)
+        blocks = destination_attention(*fields, table, contexts, first, second)
+        return gathered_output(latent, out_weight, blocks, pieces)
     inner, *fars = inner_attention(*fields, table, contexts)
     own, strips, early = middle_attention(inner, latent, *fields, *fars, table, first, second)
     early = sent(early)

time: 47.8 us -> 46.7 us (0.977); the launches traced: 47.1 us -> 46.5 us
  Pallas kernels: 24.4 us -> 23.3 us
  waiting for transfers between devices: 0.52 us -> 1.4 us
    pallas_call x1, Pallas kernels: 3.43 us -> 2.26 us  [destination_attention(): call(functools.partial(second_kernel, sp_count), [*padded, array((width,...]
    ppermute x14, waiting for transfers between devices: 0.51 us -> 1.39 us  [exchange(): return lax.ppermute(block, axis, [(i, i ^ step) for i in range(count)])]
  transfers between devices with their start and end apart: 16 -> 16, of which waited for: 1 -> 2; matrix products, arithmetic and copies ran while one was open for 0% -> 0% of each run, Pallas kernels for 38% -> 36%
where the time goes in v5:
time: 46.7 us; the launch traced here: 46.5 us
  Pallas kernels  23.3 us (50%)
  starting transfers between devices  21.5 us (46%)
  waiting for transfers between devices  1.4 us (3%)
    ppermute x14, starting transfers between devices, exchange(): return lax.ppermute(block, axis, [(i, i ^ step) for i in range(count)])  17.7 us
    pallas_call x1, Pallas kernels, main_projections(): call(functools.partial(main_kernel, pad), [array((tokens, out)), array((t...  4.92 us
    pallas_call x2, Pallas kernels, destination_attention(): call(functools.partial(near_kernel, step, sp_count), array((width, share)...  4.33 us
    pallas_call x1, Pallas kernels, gathered_output(): call(gather_kernel, array((share, width)), in_specs=[whole()] * 12, out_s...  2.84 us
    ppermute x1, starting transfers between devices, local(): second = lax.ppermute(edges[5], 'sp', pairs)  2.36 us
    pallas_call x1, Pallas kernels, destination_attention(): call(functools.partial(second_kernel, sp_count), [*padded, array((width,...  2.26 us
    pallas_call x1, Pallas kernels, destination_attention(): call(functools.partial(first_kernel, len(contexts)), [*padded, array((far...  2.15 us
    pallas_call x1, Pallas kernels, edge_projections(): call(functools.partial(edge_kernel, len(pieces)), [*[array((TILE, width))...  1.98 us
  transfers between devices with their start and end apart: 16, of which 2 were waited for; matrix products, arithmetic and copies ran while one was open for 0% of the time, Pallas kernels for 36%

profile of v5, /device:TPU:9, one launch (start us, length us, event | category | flops | bytes accessed | tf_op | source)
XLA Modules:
  0.0 46.5 jit_solution(1970207372344227693)
XLA Ops:
  0.0 1.7 %shard_map.127 = (f32[8,512]{1,0:T(8,128)S(1)}, f32[1,2048]{1,0:T(1,128)S(1)}) custom-call(bf16[2048]{0:T(1024)(128)(2,1)} %refs_0_.3, bf16[2048]{0:T(1024)(128)(2,1)} %refs_1_.2, bf16[512,512]{1,0:T(8,128)(2,1)} %refs_2_.1, bf16[512,512]{1,0:T(8,128)(2,1)} %refs_3_.1, bf16[512,512]{1,0:T(8,128)(2,1)} %refs_4_.1, bf16[2048]{0:T(1024)(128)(2,1)} %refs_5_.1), custom_call_target="tpu_custom_call" | custom-call | flops 3000000000 | tf_op jit(solution)/shard_map/pallas_call | solution.py:116
  1.7 1.4 %collective-permute-start.2 = (f32[8,512]{1,0:T(8,128)S(1)}, f32[8,512]{1,0:T(8,128)S(1)}, u32[]{:S(2)}, u32[]{:S(2)}) collective-permute-start(f32[8,512]{1,0:T(8,128)S(1)} %get-tuple-element.32.token_ref.refs_0_), channel_id=1, source_target_pairs={{0,12},{4,8},{8,4},{12,0},{1,13},{5,9},{9,5},{13,1},{2,14},{6,10},... | collective-permute-start | bytes 49160 | tf_op jit(solution)/shard_map/ppermute | solution.py:44
  3.1 1.1 %collective-permute-start.1 = (f32[8,512]{1,0:T(8,128)S(1)}, f32[8,512]{1,0:T(8,128)S(1)}, u32[]{:S(2)}, u32[]{:S(2)}) collective-permute-start(f32[8,512]{1,0:T(8,128)S(1)} %get-tuple-element.32.token_ref.refs_0_), channel_id=1, source_target_pairs={{0,8},{4,12},{8,0},{12,4},{1,9},{5,13},{9,1},{13,5},{2,10},{6,14},... | collective-permute-start | bytes 49160 | tf_op jit(solution)/shard_map/ppermute | solution.py:44
  4.2 1.1 %collective-permute-start = (f32[8,512]{1,0:T(8,128)S(1)}, f32[8,512]{1,0:T(8,128)S(1)}, u32[]{:S(2)}, u32[]{:S(2)}) collective-permute-start(f32[8,512]{1,0:T(8,128)S(1)} %get-tuple-element.32.token_ref.refs_0_), channel_id=1, source_target_pairs={{0,4},{4,0},{8,12},{12,8},{1,5},{5,1},{9,13},{13,9},{2,6},{6,2},{1... | collective-permute-start | bytes 49160 | tf_op jit(solution)/shard_map/ppermute | solution.py:44
  5.3 1.5 %shard_map.128 = (bf16[2048,256]{1,0:T(8,128)(2,1)S(1)}, f32[256,1024]{1,0:T(8,128)S(1)}) custom-call(f32[8,512]{1,0:T(8,128)S(1)} %get-tuple-element.32.token_ref.refs_0_, f32[15,4,31]{2,1,0:T(4,128)} %bitcast.1, bf16[2048,256]{1,0:T(8,128)(2,1)} %refs_0_.4), custom_call_target="tpu_custom_call" | custom-call | flops 500000000 | tf_op jit(solution)/shard_map/pallas_call | solution.py:180
  6.8 0.0 collective-permute-done.2.refs_3_
  6.8 0.0 collective-permute-done.1.refs_2_
  6.8 0.0 copy-start.2
  6.8 3.3 %collective-permute-start.5 = (f32[8,512]{1,0:T(8,128)S(1)}, f32[8,512]{1,0:T(8,128)S(1)}, u32[]{:S(2)}, u32[]{:S(2)}) collective-permute-start(f32[8,512]{1,0:T(8,128)S(1)} %shard_map.129.token_ref.rest_0_), channel_id=1, source_target_pairs={{0,3},{1,2},{2,1},{3,0},{4,7},{5,6},{6,5},{7,4},{8,11},{9,10},{10,... | collective-permute-start | bytes 49160 | tf_op jit(solution)/shard_map/ppermute | solution.py:44
  10.2 0.1 collective-permute-start.4
  10.3 0.4 collective-permute-start.3
  10.6 1.6 %shard_map.130 = (bf16[2048,256]{1,0:T(8,128)(2,1)S(1)}, bf16[2048,256]{1,0:T(8,128)(2,1)S(1)}, f32[1024,256]{1,0:T(8,128)S(1)}) custom-call(f32[8,512]{1,0:T(8,128)S(1)} %shard_map.129.token_ref.rest_0_, f32[256,1024]{1,0:T(8,128)S(1)} %get-tuple-element.33.token_ref.table_ref, bf16[2048,256]{1,0:T(8,128)(2,1)} %refs_0_.5, bf16[2048,256]{1,0:T(8,128)(2,1)} %refs_1_.3), custom_call_target="tpu_custom_call" | custom-call | flops 1000000000 | tf_op jit(solution)/shard_map/pallas_call | solution.py:217
  12.3 0.5 %collective-permute-done.4.rest_2_ = f32[8,512]{1,0:T(8,128)S(1)} collective-permute-done((f32[8,512]{1,0:T(8,128)S(1)}, f32[8,512]{1,0:T(8,128)S(1)}, u32[]{:S(2)}, u32[]{:S(2)}) %collective-permute-start.4) | collective-permute-done | bytes 16416 | tf_op jit(solution)/shard_map/ppermute | solution.py:44
  12.8 2.0 %shard_map.131 = (bf16[256,2048]{1,0:T(8,128)(2,1)S(1)}, bf16[256,2048]{1,0:T(8,128)(2,1)S(1)}, bf16[2,256,256]{2,1,0:T(8,128)(2,1)S(1)}, bf16[2,256,256]{2,1,0:...) custom-call(bf16[1536,2048]{1,0:T(8,128)(2,1)S(1)} %copy-done, ...), custom_call_target="tpu_custom_call" | custom-call | flops 2000000000 | tf_op jit(solution)/shard_map/pallas_call | solution.py:270
  14.8 2.5 %collective-permute-start.8 = (bf16[2,64,256]{2,1,0:T(8,128)(2,1)S(1)}, bf16[2,64,256]{2,1,0:T(8,128)(2,1)S(1)}, u32[]{:S(2)}, u32[]{:S(2)}) collective-permute-start(bf16[2,64,256]{2,1,0:T(8,128)(2,1)S(1)} %get-tuple-element.48.rest_0_), channel_id=1, source_target_pairs={{0,12},{4,8},{8,4},{12,0},{1,13},{5,9},{9,5},{13,1},{2,14},{6,10},... | collective-permute-start | bytes 196616 | tf_op jit(solution)/shard_map/ppermute | solution.py:44
  17.2 1.5 %collective-permute-start.7 = (bf16[2,64,256]{2,1,0:T(8,128)(2,1)S(1)}, bf16[2,64,256]{2,1,0:T(8,128)(2,1)S(1)}, u32[]{:S(2)}, u32[]{:S(2)}) collective-permute-start(bf16[2,64,256]{2,1,0:T(8,128)(2,1)S(1)} %get-tuple-element.48.rest_0_), channel_id=1, source_target_pairs={{0,8},{4,12},{8,0},{12,4},{1,9},{5,13},{9,1},{13,5},{2,10},{6,14},... | collective-permute-start | bytes 196616 | tf_op jit(solution)/shard_map/ppermute | solution.py:44
  18.8 0.0 collective-permute-start.6
  18.8 1.5 %collective-permute-start.9 = (bf16[2,256,256]{2,1,0:T(8,128)(2,1)S(1)}, bf16[2,256,256]{2,1,0:T(8,128)(2,1)S(1)}, u32[]{:S(2)}, u32[]{:S(2)}) collective-permute-start(bf16[2,256,256]{2,1,0:T(8,128)(2,1)S(1)} %get-tuple-element.53), channel_id=1, source_target_pairs={{0,4},{4,0},{8,12},{12,8},{1,5},{5,1},{9,13},{13,9},{2,6},{6,2},{1... | collective-permute-start | bytes 786440 | tf_op jit(solution)/shard_map/ppermute | solution.py:859
  20.2 2.4 %collective-permute-start.10 = (bf16[2,256,256]{2,1,0:T(8,128)(2,1)S(1)}, bf16[2,256,256]{2,1,0:T(8,128)(2,1)S(1)}, u32[]{:S(2)}, u32[]{:S(2)}) collective-permute-start(bf16[2,256,256]{2,1,0:T(8,128)(2,1)S(1)} %get-tuple-element.54), channel_id=1, source_target_pairs={{4,8},{8,4},{5,9},{9,5},{6,10},{10,6},{7,11},{11,7},{20,24},{24,20... | collective-permute-start | bytes 786440 | tf_op jit(solution)/shard_map/ppermute | solution.py:861
  22.6 4.9 %shard_map.132 = (bf16[1536,256]{1,0:T(8,128)(2,1)S(1)}, bf16[2048,256]{1,0:T(8,128)(2,1)S(1)}, bf16[2,272,2048]{2,1,0:T(8,128)(2,1)S(1)}) custom-call(bf16[1536,2048]{1,0:T(8,128)(2,1)S(1)} %copy-done, f32[1,2048]{1,0:T(1,128)S(1)} %get-tuple-element.37.a_ref, f32[1,2048]{1,0:T(1,128)S(1)} %get-tuple-element.38.b_ref, ...), custom_call_target="tpu_custom_call" | custom-call | flops 5000000000 | tf_op jit(solution)/shard_map/pallas_call | solution.py:335
  27.5 0.0 collective-permute-done.7.rest_2_
  27.6 2.1 %shard_map.133 = (bf16[2048,256]{1,0:T(8,128)(2,1)S(1)}, bf16[2,272,2048]{2,1,0:T(8,128)(2,1)S(1)}, bf16[256,256]{1,0:T(8,128)(2,1)S(1)}, bf16[272,256]{1,0:T(8,128)(2,1)S(1)}, bf16[256,384]{1,0:T(8,128)(2,1)S(1)}) custom-call(bf16[2048,256]{1,0:T(8,128)(2,1)S(1)} %get-tuple-element.44.k_in, ...), custom_call_target="tpu_custom_call", output_to_operand_aliasing={{0}: (0, {}), {1}: (1, {})} | custom-call | flops 3000000000 | tf_op jit(solution)/shard_map/pallas_call | solution.py:681
  29.7 0.6 %collective-permute-start.12 = (bf16[256,384]{1,0:T(8,128)(2,1)S(1)}, bf16[256,384]{1,0:T(8,128)(2,1)S(1)}, u32[]{:S(2)}, u32[]{:S(2)}) collective-permute-start(bf16[256,384]{1,0:T(8,128)(2,1)S(1)} %get-tuple-element.57), channel_id=1, source_target_pairs={{0,2},{1,3},{2,0},{3,1},{4,6},{5,7},{6,4},{7,5},{8,10},{9,11},{10,... | collective-permute-start | bytes 589832 | tf_op jit(solution)/shard_map/ppermute | solution.py:44
  30.4 2.3 %shard_map.134 = (bf16[2048,256]{1,0:T(8,128)(2,1)S(1)}, bf16[2,272,2048]{2,1,0:T(8,128)(2,1)S(1)}, bf16[256,384]{1,0:T(8,128)(2,1)S(1)}) custom-call(bf16[2048,256]{1,0:T(8,128)(2,1)S(1)} %get-tuple-element.49.k_in, bf16[2,272,2048]{2,1,0:T(8,128)(2,1)S(1)} %get-tuple-element.50.v_in, ...), custom_call_target="tpu_custom_call", output_to_operand_aliasing={{0}: (0, {}), {1}: (1, {})} | custom-call | flops 3000000000 | tf_op jit(solution)/shard_map/pallas_call | solution.py:691
  32.6 0.9 %collective-permute-start.13 = (bf16[256,384]{1,0:T(8,128)(2,1)S(1)}, bf16[256,384]{1,0:T(8,128)(2,1)S(1)}, u32[]{:S(2)}, u32[]{:S(2)}) collective-permute-start(bf16[256,384]{1,0:T(8,128)(2,1)S(1)} %get-tuple-element.58), channel_id=1, source_target_pairs={{0,2},{1,3},{2,0},{3,1},{4,6},{5,7},{6,4},{7,5},{8,10},{9,11},{10,... | collective-permute-start | bytes 589832 | tf_op jit(solution)/shard_map/ppermute | solution.py:44
  33.6 2.1 %shard_map.136 = bf16[256,384]{1,0:T(8,128)(2,1)S(1)} custom-call(bf16[2048,256]{1,0:T(8,128)(2,1)S(1)} %get-tuple-element.55.k_ref, bf16[2,272,2048]{2,1,0:T(8,128)(2,1)S(1)} %get-tuple-element.56.v_ref, bf16[1536,256]{1,0:T(8,128)(2,1)S(1)} %get-tuple-element.46.q_ref, bf16[256,256]{1,0:T(8,128)(2,1)S(1)} %get-tuple-element.51.kc_ref, ...), custom_call_target="tpu_custom_call" | custom-call | flops 3000000000 | tf_op jit(solution)/shard_map/pallas_call | solution.py:704
  35.7 2.2 %collective-permute-start.11 = (bf16[256,384]{1,0:T(8,128)(2,1)S(1)}, bf16[256,384]{1,0:T(8,128)(2,1)S(1)}, u32[]{:S(2)}, u32[]{:S(2)}) collective-permute-start(bf16[256,384]{1,0:T(8,128)(2,1)S(1)} %shard_map.136), channel_id=1, source_target_pairs={{0,1},{1,0},{2,3},{3,2},{4,5},{5,4},{6,7},{7,6},{8,9},{9,8},{10,11... | collective-permute-start | bytes 589832 | tf_op jit(solution)/shard_map/ppermute | solution.py:44
  37.9 0.5 collective-permute-start.14
  38.4 0.9 %collective-permute-done.13.rest_7_ = bf16[256,384]{1,0:T(8,128)(2,1)S(1)} collective-permute-done((bf16[256,384]{1,0:T(8,128)(2,1)S(1)}, bf16[256,384]{1,0:T(8,128)(2,1)S(1)}, u32[]{:S(2)}, u32[]{:S(2)}) %collective-permute-start.13) | collective-permute-done | bytes 196640 | tf_op jit(solution)/shard_map/ppermute | solution.py:44
  39.3 2.0 %collective-permute-start.15 = (bf16[256,384]{1,0:T(8,128)(2,1)S(1)}, bf16[256,384]{1,0:T(8,128)(2,1)S(1)}, u32[]{:S(2)}, u32[]{:S(2)}) collective-permute-start(bf16[256,384]{1,0:T(8,128)(2,1)S(1)} %collective-permute-done.13.rest_7_), channel_id=1, source_target_pairs={{0,1},{1,0},{2,3},{3,2},{4,5},{5,4},{6,7},{7,6},{8,9},{9,8},{10,11... | collective-permute-start | bytes 589832 | tf_op jit(solution)/shard_map/ppermute | solution.py:44
  41.3 2.2 %shard_map.135.rest_4_ = bf16[256,384]{1,0:T(8,128)(2,1)S(1)} custom-call(bf16[2048,256]{1,0:T(8,128)(2,1)S(1)} %get-tuple-element.55.k_ref, bf16[2,272,2048]{2,1,0:T(8,128)(2,1)S(1)} %get-tuple-element.56.v_ref, bf16[1536,256]{1,0:T(8,128)(2,1)S(1)} %get-tuple-element.46.q_ref, bf16[256,256]{1,0:T(8,128)(2,1)S(1)} %get-tuple-element.51.kc_ref, ...), custom_call_target="tpu_custom_call" | custom-call | flops 3000000000 | tf_op jit(solution)/shard_map/pallas_call | solution.py:704
  43.5 2.8 %shard_map.137 = bf16[384,2048]{1,0:T(8,128)(2,1)} custom-call(bf16[1536,2048]{1,0:T(8,128)(2,1)S(1)} %copy-done, bf16[1024,2048]{1,0:T(8,128)(2,1)S(1)} %copy-done.1, f32[8,512]{1,0:T(8,128)S(1)} %shard_map.129.token_ref.rest_0_, f32[8,512]{1,0:T(8,128)S(1)} %collective-permute-done.3.rest_1_, f32[8,512]{1,0:T(8,128)S(1)} %collective-permute-done.4.rest_2_, ...), custom_call_target="tpu_custom_call" | custom-call | flops 2000000000 | tf_op jit(solution)/shard_map/pallas_call | solution.py:753
  (17 shorter events, 0.0 us)
Async XLA Ops:
  1.7 5.1 %collective-permute-start.2 = (f32[8,512]{1,0:T(8,128)S(1)}, f32[8,512]{1,0:T(8,128)S(1)}, u32[]{:S(2)}, u32[]{:S(2)}) collective-permute-start(f32[8,512]{1,0:T(8,128)S(1)} %get-tuple-element.32.token_ref.refs_0_), channel_id=1, source_target_pairs={{0,12},{4,8},{8,4},{12,0},{1,13},{5,9},{9,5},{13,1},{2,14},{6,10},... | collective-permute-start | bytes 49160 | tf_op jit(solution)/shard_map/ppermute | solution.py:44
  3.1 3.7 %collective-permute-start.1 = (f32[8,512]{1,0:T(8,128)S(1)}, f32[8,512]{1,0:T(8,128)S(1)}, u32[]{:S(2)}, u32[]{:S(2)}) collective-permute-start(f32[8,512]{1,0:T(8,128)S(1)} %get-tuple-element.32.token_ref.refs_0_), channel_id=1, source_target_pairs={{0,8},{4,12},{8,0},{12,4},{1,9},{5,13},{9,1},{13,5},{2,10},{6,14},... | collective-permute-start | bytes 49160 | tf_op jit(solution)/shard_map/ppermute | solution.py:44
  4.2 2.6 %collective-permute-start = (f32[8,512]{1,0:T(8,128)S(1)}, f32[8,512]{1,0:T(8,128)S(1)}, u32[]{:S(2)}, u32[]{:S(2)}) collective-permute-start(f32[8,512]{1,0:T(8,128)S(1)} %get-tuple-element.32.token_ref.refs_0_), channel_id=1, source_target_pairs={{0,4},{4,0},{8,12},{12,8},{1,5},{5,1},{9,13},{13,9},{2,6},{6,2},{1... | collective-permute-start | bytes 49160 | tf_op jit(solution)/shard_map/ppermute | solution.py:44
  5.3 7.5 %copy-start = (bf16[1536,2048]{1,0:T(8,128)(2,1)S(1)}, bf16[1536,2048]{1,0:T(8,128)(2,1)}, u32[]{:S(2)}) copy-start(bf16[1536,2048]{1,0:T(8,128)(2,1)} %x_ref.5) | copy-start | bytes 18874372
  6.8 6.0 %copy-start.2 = (bf16[64,2048]{1,0:T(8,128)(2,1)S(1)}, bf16[64,2048]{1,0:T(8,128)(2,1)}, u32[]{:S(2)}) copy-start(bf16[64,2048]{1,0:T(8,128)(2,1)} %context_ref.1) | copy-start | bytes 786436
  6.8 5.5 %collective-permute-start.5 = (f32[8,512]{1,0:T(8,128)S(1)}, f32[8,512]{1,0:T(8,128)S(1)}, u32[]{:S(2)}, u32[]{:S(2)}) collective-permute-start(f32[8,512]{1,0:T(8,128)S(1)} %shard_map.129.token_ref.rest_0_), channel_id=1, source_target_pairs={{0,3},{1,2},{2,1},{3,0},{4,7},{5,6},{6,5},{7,4},{8,11},{9,10},{10,... | collective-permute-start | bytes 49160 | tf_op jit(solution)/shard_map/ppermute | solution.py:44
  10.2 2.6 %collective-permute-start.4 = (f32[8,512]{1,0:T(8,128)S(1)}, f32[8,512]{1,0:T(8,128)S(1)}, u32[]{:S(2)}, u32[]{:S(2)}) collective-permute-start(f32[8,512]{1,0:T(8,128)S(1)} %shard_map.129.token_ref.rest_0_), channel_id=1, source_target_pairs={{0,2},{1,3},{2,0},{3,1},{4,6},{5,7},{6,4},{7,5},{8,10},{9,11},{10,... | collective-permute-start | bytes 49160 | tf_op jit(solution)/shard_map/ppermute | solution.py:44
  10.3 2.5 %collective-permute-start.3 = (f32[8,512]{1,0:T(8,128)S(1)}, f32[8,512]{1,0:T(8,128)S(1)}, u32[]{:S(2)}, u32[]{:S(2)}) collective-permute-start(f32[8,512]{1,0:T(8,128)S(1)} %shard_map.129.token_ref.rest_0_), channel_id=1, source_target_pairs={{0,1},{1,0},{2,3},{3,2},{4,5},{5,4},{6,7},{7,6},{8,9},{9,8},{10,11... | collective-permute-start | bytes 49160 | tf_op jit(solution)/shard_map/ppermute | solution.py:44
  14.8 12.8 %collective-permute-start.8 = (bf16[2,64,256]{2,1,0:T(8,128)(2,1)S(1)}, bf16[2,64,256]{2,1,0:T(8,128)(2,1)S(1)}, u32[]{:S(2)}, u32[]{:S(2)}) collective-permute-start(bf16[2,64,256]{2,1,0:T(8,128)(2,1)S(1)} %get-tuple-element.48.rest_0_), channel_id=1, source_target_pairs={{0,12},{4,8},{8,4},{12,0},{1,13},{5,9},{9,5},{13,1},{2,14},{6,10},... | collective-permute-start | bytes 196616 | tf_op jit(solution)/shard_map/ppermute | solution.py:44
  17.2 10.3 %collective-permute-start.7 = (bf16[2,64,256]{2,1,0:T(8,128)(2,1)S(1)}, bf16[2,64,256]{2,1,0:T(8,128)(2,1)S(1)}, u32[]{:S(2)}, u32[]{:S(2)}) collective-permute-start(bf16[2,64,256]{2,1,0:T(8,128)(2,1)S(1)} %get-tuple-element.48.rest_0_), channel_id=1, source_target_pairs={{0,8},{4,12},{8,0},{12,4},{1,9},{5,13},{9,1},{13,5},{2,10},{6,14},... | collective-permute-start | bytes 196616 | tf_op jit(solution)/shard_map/ppermute | solution.py:44
  18.8 8.8 %collective-permute-start.6 = (bf16[2,64,256]{2,1,0:T(8,128)(2,1)S(1)}, bf16[2,64,256]{2,1,0:T(8,128)(2,1)S(1)}, u32[]{:S(2)}, u32[]{:S(2)}) collective-permute-start(bf16[2,64,256]{2,1,0:T(8,128)(2,1)S(1)} %get-tuple-element.48.rest_0_), channel_id=1, source_target_pairs={{0,4},{4,0},{8,12},{12,8},{1,5},{5,1},{9,13},{13,9},{2,6},{6,2},{1... | collective-permute-start | bytes 196616 | tf_op jit(solution)/shard_map/ppermute | solution.py:44
  18.8 11.6 %collective-permute-start.9 = (bf16[2,256,256]{2,1,0:T(8,128)(2,1)S(1)}, bf16[2,256,256]{2,1,0:T(8,128)(2,1)S(1)}, u32[]{:S(2)}, u32[]{:S(2)}) collective-permute-start(bf16[2,256,256]{2,1,0:T(8,128)(2,1)S(1)} %get-tuple-element.53), channel_id=1, source_target_pairs={{0,4},{4,0},{8,12},{12,8},{1,5},{5,1},{9,13},{13,9},{2,6},{6,2},{1... | collective-permute-start | bytes 786440 | tf_op jit(solution)/shard_map/ppermute | solution.py:859
  20.2 10.1 %collective-permute-start.10 = (bf16[2,256,256]{2,1,0:T(8,128)(2,1)S(1)}, bf16[2,256,256]{2,1,0:T(8,128)(2,1)S(1)}, u32[]{:S(2)}, u32[]{:S(2)}) collective-permute-start(bf16[2,256,256]{2,1,0:T(8,128)(2,1)S(1)} %get-tuple-element.54), channel_id=1, source_target_pairs={{4,8},{8,4},{5,9},{9,5},{6,10},{10,6},{7,11},{11,7},{20,24},{24,20... | collective-permute-start | bytes 786440 | tf_op jit(solution)/shard_map/ppermute | solution.py:861
  29.7 8.2 %collective-permute-start.12 = (bf16[256,384]{1,0:T(8,128)(2,1)S(1)}, bf16[256,384]{1,0:T(8,128)(2,1)S(1)}, u32[]{:S(2)}, u32[]{:S(2)}) collective-permute-start(bf16[256,384]{1,0:T(8,128)(2,1)S(1)} %get-tuple-element.57), channel_id=1, source_target_pairs={{0,2},{1,3},{2,0},{3,1},{4,6},{5,7},{6,4},{7,5},{8,10},{9,11},{10,... | collective-permute-start | bytes 589832 | tf_op jit(solution)/shard_map/ppermute | solution.py:44
  32.6 6.6 %collective-permute-start.13 = (bf16[256,384]{1,0:T(8,128)(2,1)S(1)}, bf16[256,384]{1,0:T(8,128)(2,1)S(1)}, u32[]{:S(2)}, u32[]{:S(2)}) collective-permute-start(bf16[256,384]{1,0:T(8,128)(2,1)S(1)} %get-tuple-element.58), channel_id=1, source_target_pairs={{0,2},{1,3},{2,0},{3,1},{4,6},{5,7},{6,4},{7,5},{8,10},{9,11},{10,... | collective-permute-start | bytes 589832 | tf_op jit(solution)/shard_map/ppermute | solution.py:44
  35.7 7.8 %collective-permute-start.11 = (bf16[256,384]{1,0:T(8,128)(2,1)S(1)}, bf16[256,384]{1,0:T(8,128)(2,1)S(1)}, u32[]{:S(2)}, u32[]{:S(2)}) collective-permute-start(bf16[256,384]{1,0:T(8,128)(2,1)S(1)} %shard_map.136), channel_id=1, source_target_pairs={{0,1},{1,0},{2,3},{3,2},{4,5},{5,4},{6,7},{7,6},{8,9},{9,8},{10,11... | collective-permute-start | bytes 589832 | tf_op jit(solution)/shard_map/ppermute | solution.py:44
  37.9 5.6 %collective-permute-start.14 = (bf16[256,384]{1,0:T(8,128)(2,1)S(1)}, bf16[256,384]{1,0:T(8,128)(2,1)S(1)}, u32[]{:S(2)}, u32[]{:S(2)}) collective-permute-start(bf16[256,384]{1,0:T(8,128)(2,1)S(1)} %collective-permute-done.12.rest_6_), channel_id=1, source_target_pairs={{0,1},{1,0},{2,3},{3,2},{4,5},{5,4},{6,7},{7,6},{8,9},{9,8},{10,11... | collective-permute-start | bytes 589832 | tf_op jit(solution)/shard_map/ppermute | solution.py:44
  39.3 4.3 %collective-permute-start.15 = (bf16[256,384]{1,0:T(8,128)(2,1)S(1)}, bf16[256,384]{1,0:T(8,128)(2,1)S(1)}, u32[]{:S(2)}, u32[]{:S(2)}) collective-permute-start(bf16[256,384]{1,0:T(8,128)(2,1)S(1)} %collective-permute-done.13.rest_7_), channel_id=1, source_target_pairs={{0,1},{1,0},{2,3},{3,2},{4,5},{5,4},{6,7},{7,6},{8,9},{9,8},{10,11... | collective-permute-start | bytes 589832 | tf_op jit(solution)/shard_map/ppermute | solution.py:44
  41.3 2.2 %copy-start.1 = (bf16[1024,2048]{1,0:T(8,128)(2,1)S(1)}, bf16[1024,2048]{1,0:T(8,128)(2,1)}, u32[]{:S(2)}) copy-start(bf16[1024,2048]{1,0:T(8,128)(2,1)} %w_ref.1) | copy-start | bytes 12582916

commit v6 on v5

--- a/solution.py
+++ b/solution.py
@@ -398,14 +398,14 @@
 
     peaks, outs = {}, {}
     for index in range(len(rows) + 2):
-        if index < len(rows):
-            peaks[index] = score(index)
-        if 0 <= index - 1 < len(rows):
-            weigh(index - 1, peaks.pop(index - 1))
         if 0 <= index - 2:
             outs[index - 2] = gather(index - 2)
             if (index - 2) % 2:
                 store(index - 3, outs.pop(index - 3), outs.pop(index - 2))
+        if 0 <= index - 1 < len(rows):
+            weigh(index - 1, peaks.pop(index - 1))
+        if index < len(rows):
+            peaks[index] = score(index)
 
 
 def part(start, unit, size):
@@ -716,29 +716,49 @@
     return blocks[1], neighbour, x1, x2, passed1, passed2
 
 
-def gather_kernel(x_ref, w_ref, *rest):
-    pieces, blocks, (out_ref, gate_ref, held_ref, block_ref, sems) = rest[:4], rest[4:10], rest[10:]
-    mine_ref, neighbour_ref, x1_ref, x2_ref, passed1_ref, passed2_ref = blocks
+def weight_rows(step, height):
+    return part(origin("tp", step) * height, LANES, height)
+
+
+def is_free_target():
+    tp = lax.axis_index("tp")
+    return (tp == 1) | (tp == 2)
+
+
+def partial_kernel(w_ref, mine_ref, neighbour_ref, x1_ref, x2_ref, sum_ref, *turned):
     height = mine_ref.shape[0]
     tile = w_ref.shape[1] // 4
-    tp = lax.axis_index("tp")
-    free = (tp == 1) | (tp == 2)
-    mine = part(tp * held_ref.shape[0], GRID_W, held_ref.shape[0])
-    for index in range(4):
-        gate_ref[:, part(origin("tp", index) * tile, LANES, tile)] = pieces[index][4:5, :]
     values = (
         mine_ref[...],
         neighbour_ref[...],
-        jnp.where(free, x1_ref[...], x2_ref[...]),
-        jnp.where(free, passed1_ref[...], passed2_ref[...]),
+        jnp.where(is_free_target(), x1_ref[...], x2_ref[...]),
     )
-    for index, value in enumerate(values):
-        rows = part(origin("tp", index) * height, LANES, height)
-        block_ref[:, rows] = value.astype(f32).T.astype(bf16)
+    for ref, value in zip(turned, values):
+        ref[...] = value.astype(f32).T.astype(bf16)
+    for step in range(4):
+        cols = slice(step * tile, (step + 1) * tile)
+        total = None
+        for index, ref in enumerate(turned):
+            weight = w_ref[weight_rows(index, height), cols]
+            term = jnp.dot(ref[...], weight, preferred_element_type=f32)
+            total = term if total is None else total + term
+        sum_ref[:, cols] = total
+
+
+def gather_kernel(x_ref, w_ref, sum_ref, one_ref, two_ref, *rest):
+    pieces, (out_ref, gate_ref, held_ref, turned_ref, sems) = rest[:4], rest[4:]
+    height, share = one_ref.shape
+    tile = w_ref.shape[1] // 4
+    mine = part(lax.axis_index("tp") * share, GRID_W, share)
+    for index in range(4):
+        gate_ref[:, part(origin("tp", index) * tile, LANES, tile)] = pieces[index][4:5, :]
+    value = jnp.where(is_free_target(), one_ref[...], two_ref[...])
+    turned_ref[...] = value.astype(f32).T.astype(bf16)
     copies = []
     for step in range(4):
         cols = slice(step * tile, (step + 1) * tile)
-        total = jnp.dot(block_ref[...], w_ref[:, cols], preferred_element_type=f32)
+        weight = w_ref[weight_rows(3, height), cols]
+        total = sum_ref[:, cols] + jnp.dot(turned_ref[...], weight, preferred_element_type=f32)
         held_ref[:, cols] = (x_ref[mine, cols].astype(f32) + gate_ref[:, cols] * total).astype(bf16)
         copies.append(
             pltpu.make_async_copy(held_ref.at[:, cols], out_ref.at[:, cols], sems.at[step])
@@ -749,20 +769,30 @@
 
 
 def gathered_output(x, weight, blocks, pieces):
+    mine, neighbour, x1, x2, passed1, passed2 = blocks
     share, width = x.shape[0] // 4, x.shape[1]
+    height = mine.shape[0]
+    total = call(
+        partial_kernel,
+        array((share, width), f32),
+        in_specs=[whole()] * 5,
+        out_specs=whole(),
+        scratch_shapes=[VMEM((share, height), bf16)] * 3,
+        flops=2_000_000_000,
+    )(weight, mine, neighbour, x1, x2)
     return call(
         gather_kernel,
         array((share, width)),
-        in_specs=[whole()] * 12,
+        in_specs=[whole()] * 9,
         out_specs=whole(HBM),
         scratch_shapes=[
             VMEM((1, width), f32),
             VMEM((share, width), bf16),
-            VMEM((share, weight.shape[0]), bf16),
+            VMEM((share, height), bf16),
             pltpu.SemaphoreType.DMA((4,)),
         ],
         flops=2_000_000_000,
-    )(x, weight, *pieces, *blocks)
+    )(x, weight, total, passed1, passed2, *pieces)
 
 
 def output_kernel(count, late, *refs):

time: 46.7 us -> 47.1 us (level)
  Pallas kernels: 23.3 us -> 24 us
    pallas_call x1 -> x2, Pallas kernels: 2.84 us -> 3.01 us  [the longest x1 1.57 us: gathered_output(): call(gather_kernel, array((share, width)), in_specs=[whole()] * 9, out_sp...]
  transfers between devices with their start and end apart: 16 -> 16, of which waited for: 2 -> 2; matrix products, arithmetic and copies ran while one was open for 0% -> 0% of each run, Pallas kernels for 36% -> 40%
where the time goes in v6:
time: 47.1 us; the launch traced here: 46.9 us
  Pallas kernels  24 us (51%)
  starting transfers between devices  21.2 us (45%)
  waiting for transfers between devices  1.27 us (3%)
    ppermute x14, starting transfers between devices, exchange(): return lax.ppermute(block, axis, [(i, i ^ step) for i in range(count)])  17.4 us
    pallas_call x1, Pallas kernels, main_projections(): call(functools.partial(main_kernel, pad), [array((tokens, out)), array((t...  4.76 us
    pallas_call x2, Pallas kernels, destination_attention(): call(functools.partial(near_kernel, step, sp_count), array((width, share)...  4.7 us
    pallas_call x1, Pallas kernels, destination_attention(): call(functools.partial(second_kernel, sp_count), [*padded, array((width,...  2.43 us
    ppermute x1, starting transfers between devices, local(): second = lax.ppermute(edges[5], 'sp', pairs)  2.36 us
    pallas_call x1, Pallas kernels, destination_attention(): call(functools.partial(first_kernel, len(contexts)), [*padded, array((far...  2.35 us
    pallas_call x1, Pallas kernels, edge_projections(): call(functools.partial(edge_kernel, len(pieces)), [*[array((TILE, width))...  1.98 us
    pallas_call x1, Pallas kernels, modulation_terms(): call(modulation_kernel, [array((8, width), f32), array((1, *rest[-1].shap...  1.69 us
  transfers between devices with their start and end apart: 16, of which 2 were waited for; matrix products, arithmetic and copies ran while one was open for 0% of the time, Pallas kernels for 40%

profile of v6, /device:TPU:9, one launch (start us, length us, event | category | flops | bytes accessed | tf_op | source)
XLA Modules:
  0.0 46.9 jit_solution(10416383662796880752)
XLA Ops:
  0.0 1.7 %shard_map.127 = (f32[8,512]{1,0:T(8,128)S(1)}, f32[1,2048]{1,0:T(1,128)S(1)}) custom-call(bf16[2048]{0:T(1024)(128)(2,1)} %refs_0_.3, bf16[2048]{0:T(1024)(128)(2,1)} %refs_1_.2, bf16[512,512]{1,0:T(8,128)(2,1)} %refs_2_.1, bf16[512,512]{1,0:T(8,128)(2,1)} %refs_3_.1, bf16[512,512]{1,0:T(8,128)(2,1)} %refs_4_.1, bf16[2048]{0:T(1024)(128)(2,1)} %refs_5_.1), custom_call_target="tpu_custom_call" | custom-call | flops 3000000000 | tf_op jit(solution)/shard_map/pallas_call | solution.py:116
  1.7 1.4 %collective-permute-start.2 = (f32[8,512]{1,0:T(8,128)S(1)}, f32[8,512]{1,0:T(8,128)S(1)}, u32[]{:S(2)}, u32[]{:S(2)}) collective-permute-start(f32[8,512]{1,0:T(8,128)S(1)} %get-tuple-element.33.token_ref.refs_0_), channel_id=1, source_target_pairs={{0,12},{4,8},{8,4},{12,0},{1,13},{5,9},{9,5},{13,1},{2,14},{6,10},... | collective-permute-start | bytes 49160 | tf_op jit(solution)/shard_map/ppermute | solution.py:44
  3.1 1.1 %collective-permute-start.1 = (f32[8,512]{1,0:T(8,128)S(1)}, f32[8,512]{1,0:T(8,128)S(1)}, u32[]{:S(2)}, u32[]{:S(2)}) collective-permute-start(f32[8,512]{1,0:T(8,128)S(1)} %get-tuple-element.33.token_ref.refs_0_), channel_id=1, source_target_pairs={{0,8},{4,12},{8,0},{12,4},{1,9},{5,13},{9,1},{13,5},{2,10},{6,14},... | collective-permute-start | bytes 49160 | tf_op jit(solution)/shard_map/ppermute | solution.py:44
  4.2 1.1 %collective-permute-start = (f32[8,512]{1,0:T(8,128)S(1)}, f32[8,512]{1,0:T(8,128)S(1)}, u32[]{:S(2)}, u32[]{:S(2)}) collective-permute-start(f32[8,512]{1,0:T(8,128)S(1)} %get-tuple-element.33.token_ref.refs_0_), channel_id=1, source_target_pairs={{0,4},{4,0},{8,12},{12,8},{1,5},{5,1},{9,13},{13,9},{2,6},{6,2},{1... | collective-permute-start | bytes 49160 | tf_op jit(solution)/shard_map/ppermute | solution.py:44
  5.3 1.5 %shard_map.128 = (bf16[2048,256]{1,0:T(8,128)(2,1)S(1)}, f32[256,1024]{1,0:T(8,128)S(1)}) custom-call(f32[8,512]{1,0:T(8,128)S(1)} %get-tuple-element.33.token_ref.refs_0_, f32[15,4,31]{2,1,0:T(4,128)} %bitcast.1, bf16[2048,256]{1,0:T(8,128)(2,1)} %refs_0_.4), custom_call_target="tpu_custom_call" | custom-call | flops 500000000 | tf_op jit(solution)/shard_map/pallas_call | solution.py:180
  6.8 0.0 collective-permute-done.2.refs_3_
  6.8 0.0 collective-permute-done.1.refs_2_
  6.8 0.0 copy-start.2
  6.8 3.3 %collective-permute-start.5 = (f32[8,512]{1,0:T(8,128)S(1)}, f32[8,512]{1,0:T(8,128)S(1)}, u32[]{:S(2)}, u32[]{:S(2)}) collective-permute-start(f32[8,512]{1,0:T(8,128)S(1)} %shard_map.129.token_ref.rest_0_), channel_id=1, source_target_pairs={{0,3},{1,2},{2,1},{3,0},{4,7},{5,6},{6,5},{7,4},{8,11},{9,10},{10,... | collective-permute-start | bytes 49160 | tf_op jit(solution)/shard_map/ppermute | solution.py:44
  10.2 0.1 collective-permute-start.4
  10.3 0.4 collective-permute-start.3
  10.6 1.6 %shard_map.130 = (bf16[2048,256]{1,0:T(8,128)(2,1)S(1)}, bf16[2048,256]{1,0:T(8,128)(2,1)S(1)}, f32[1024,256]{1,0:T(8,128)S(1)}) custom-call(f32[8,512]{1,0:T(8,128)S(1)} %shard_map.129.token_ref.rest_0_, f32[256,1024]{1,0:T(8,128)S(1)} %get-tuple-element.35.token_ref.table_ref, bf16[2048,256]{1,0:T(8,128)(2,1)} %refs_0_.5, bf16[2048,256]{1,0:T(8,128)(2,1)} %refs_1_.3), custom_call_target="tpu_custom_call" | custom-call | flops 1000000000 | tf_op jit(solution)/shard_map/pallas_call | solution.py:217
  12.3 0.5 %collective-permute-done.4.rest_2_ = f32[8,512]{1,0:T(8,128)S(1)} collective-permute-done((f32[8,512]{1,0:T(8,128)S(1)}, f32[8,512]{1,0:T(8,128)S(1)}, u32[]{:S(2)}, u32[]{:S(2)}) %collective-permute-start.4) | collective-permute-done | bytes 16416 | tf_op jit(solution)/shard_map/ppermute | solution.py:44
  12.8 2.0 %shard_map.131 = (bf16[256,2048]{1,0:T(8,128)(2,1)S(1)}, bf16[256,2048]{1,0:T(8,128)(2,1)S(1)}, bf16[2,256,256]{2,1,0:T(8,128)(2,1)S(1)}, bf16[2,256,256]{2,1,0:...) custom-call(bf16[1536,2048]{1,0:T(8,128)(2,1)S(1)} %copy-done, ...), custom_call_target="tpu_custom_call" | custom-call | flops 2000000000 | tf_op jit(solution)/shard_map/pallas_call | solution.py:270
  14.8 2.5 %collective-permute-start.8 = (bf16[2,64,256]{2,1,0:T(8,128)(2,1)S(1)}, bf16[2,64,256]{2,1,0:T(8,128)(2,1)S(1)}, u32[]{:S(2)}, u32[]{:S(2)}) collective-permute-start(bf16[2,64,256]{2,1,0:T(8,128)(2,1)S(1)} %get-tuple-element.48.rest_0_), channel_id=1, source_target_pairs={{0,12},{4,8},{8,4},{12,0},{1,13},{5,9},{9,5},{13,1},{2,14},{6,10},... | collective-permute-start | bytes 196616 | tf_op jit(solution)/shard_map/ppermute | solution.py:44
  17.2 1.5 %collective-permute-start.7 = (bf16[2,64,256]{2,1,0:T(8,128)(2,1)S(1)}, bf16[2,64,256]{2,1,0:T(8,128)(2,1)S(1)}, u32[]{:S(2)}, u32[]{:S(2)}) collective-permute-start(bf16[2,64,256]{2,1,0:T(8,128)(2,1)S(1)} %get-tuple-element.48.rest_0_), channel_id=1, source_target_pairs={{0,8},{4,12},{8,0},{12,4},{1,9},{5,13},{9,1},{13,5},{2,10},{6,14},... | collective-permute-start | bytes 196616 | tf_op jit(solution)/shard_map/ppermute | solution.py:44
  18.8 1.5 %collective-permute-start.9 = (bf16[2,256,256]{2,1,0:T(8,128)(2,1)S(1)}, bf16[2,256,256]{2,1,0:T(8,128)(2,1)S(1)}, u32[]{:S(2)}, u32[]{:S(2)}) collective-permute-start(bf16[2,256,256]{2,1,0:T(8,128)(2,1)S(1)} %get-tuple-element.53), channel_id=1, source_target_pairs={{0,4},{4,0},{8,12},{12,8},{1,5},{5,1},{9,13},{13,9},{2,6},{6,2},{1... | collective-permute-start | bytes 786440 | tf_op jit(solution)/shard_map/ppermute | solution.py:889
  20.2 2.4 %collective-permute-start.10 = (bf16[2,256,256]{2,1,0:T(8,128)(2,1)S(1)}, bf16[2,256,256]{2,1,0:T(8,128)(2,1)S(1)}, u32[]{:S(2)}, u32[]{:S(2)}) collective-permute-start(bf16[2,256,256]{2,1,0:T(8,128)(2,1)S(1)} %get-tuple-element.54), channel_id=1, source_target_pairs={{4,8},{8,4},{5,9},{9,5},{6,10},{10,6},{7,11},{11,7},{20,24},{24,20... | collective-permute-start | bytes 786440 | tf_op jit(solution)/shard_map/ppermute | solution.py:891
  22.6 4.8 %shard_map.132 = (bf16[1536,256]{1,0:T(8,128)(2,1)S(1)}, bf16[2048,256]{1,0:T(8,128)(2,1)S(1)}, bf16[2,272,2048]{2,1,0:T(8,128)(2,1)S(1)}) custom-call(bf16[1536,2048]{1,0:T(8,128)(2,1)S(1)} %copy-done, f32[1,2048]{1,0:T(1,128)S(1)} %get-tuple-element.37.a_ref, f32[1,2048]{1,0:T(1,128)S(1)} %get-tuple-element.38.b_ref, ...), custom_call_target="tpu_custom_call" | custom-call | flops 5000000000 | tf_op jit(solution)/shard_map/pallas_call | solution.py:335
  27.4 2.4 %shard_map.133 = (bf16[2048,256]{1,0:T(8,128)(2,1)S(1)}, bf16[2,272,2048]{2,1,0:T(8,128)(2,1)S(1)}, bf16[256,256]{1,0:T(8,128)(2,1)S(1)}, bf16[272,256]{1,0:T(8,128)(2,1)S(1)}, bf16[256,384]{1,0:T(8,128)(2,1)S(1)}) custom-call(bf16[2048,256]{1,0:T(8,128)(2,1)S(1)} %get-tuple-element.44.k_in, ...), custom_call_target="tpu_custom_call", output_to_operand_aliasing={{0}: (0, {}), {1}: (1, {})} | custom-call | flops 3000000000 | tf_op jit(solution)/shard_map/pallas_call | solution.py:681
  29.8 0.7 %collective-permute-start.12 = (bf16[256,384]{1,0:T(8,128)(2,1)S(1)}, bf16[256,384]{1,0:T(8,128)(2,1)S(1)}, u32[]{:S(2)}, u32[]{:S(2)}) collective-permute-start(bf16[256,384]{1,0:T(8,128)(2,1)S(1)} %get-tuple-element.57), channel_id=1, source_target_pairs={{0,2},{1,3},{2,0},{3,1},{4,6},{5,7},{6,4},{7,5},{8,10},{9,11},{10,... | collective-permute-start | bytes 589832 | tf_op jit(solution)/shard_map/ppermute | solution.py:44
  30.4 2.4 %shard_map.134 = (bf16[2048,256]{1,0:T(8,128)(2,1)S(1)}, bf16[2,272,2048]{2,1,0:T(8,128)(2,1)S(1)}, bf16[256,384]{1,0:T(8,128)(2,1)S(1)}) custom-call(bf16[2048,256]{1,0:T(8,128)(2,1)S(1)} %get-tuple-element.49.k_in, bf16[2,272,2048]{2,1,0:T(8,128)(2,1)S(1)} %get-tuple-element.50.v_in, ...), custom_call_target="tpu_custom_call", output_to_operand_aliasing={{0}: (0, {}), {1}: (1, {})} | custom-call | flops 3000000000 | tf_op jit(solution)/shard_map/pallas_call | solution.py:691
  32.8 0.9 %collective-permute-start.13 = (bf16[256,384]{1,0:T(8,128)(2,1)S(1)}, bf16[256,384]{1,0:T(8,128)(2,1)S(1)}, u32[]{:S(2)}, u32[]{:S(2)}) collective-permute-start(bf16[256,384]{1,0:T(8,128)(2,1)S(1)} %get-tuple-element.58), channel_id=1, source_target_pairs={{0,2},{1,3},{2,0},{3,1},{4,6},{5,7},{6,4},{7,5},{8,10},{9,11},{10,... | collective-permute-start | bytes 589832 | tf_op jit(solution)/shard_map/ppermute | solution.py:44
  33.8 2.3 %shard_map.136 = bf16[256,384]{1,0:T(8,128)(2,1)S(1)} custom-call(bf16[2048,256]{1,0:T(8,128)(2,1)S(1)} %get-tuple-element.55.k_ref, bf16[2,272,2048]{2,1,0:T(8,128)(2,1)S(1)} %get-tuple-element.56.v_ref, bf16[1536,256]{1,0:T(8,128)(2,1)S(1)} %get-tuple-element.46.q_ref, bf16[256,256]{1,0:T(8,128)(2,1)S(1)} %get-tuple-element.51.kc_ref, ...), custom_call_target="tpu_custom_call" | custom-call | flops 3000000000 | tf_op jit(solution)/shard_map/pallas_call | solution.py:704
  36.1 0.0 copy-start.1
  36.1 2.2 %collective-permute-start.11 = (bf16[256,384]{1,0:T(8,128)(2,1)S(1)}, bf16[256,384]{1,0:T(8,128)(2,1)S(1)}, u32[]{:S(2)}, u32[]{:S(2)}) collective-permute-start(bf16[256,384]{1,0:T(8,128)(2,1)S(1)} %shard_map.136), channel_id=1, source_target_pairs={{0,1},{1,0},{2,3},{3,2},{4,5},{5,4},{6,7},{7,6},{8,9},{9,8},{10,11... | collective-permute-start | bytes 589832 | tf_op jit(solution)/shard_map/ppermute | solution.py:44
  38.3 0.1 collective-permute-start.14
  38.4 0.8 %collective-permute-done.13.x2_ref = bf16[256,384]{1,0:T(8,128)(2,1)S(1)} collective-permute-done((bf16[256,384]{1,0:T(8,128)(2,1)S(1)}, bf16[256,384]{1,0:T(8,128)(2,1)S(1)}, u32[]{:S(2)}, u32[]{:S(2)}) %collective-permute-start.13) | collective-permute-done | bytes 196640 | tf_op jit(solution)/shard_map/ppermute | solution.py:44
  39.2 2.2 %collective-permute-start.15 = (bf16[256,384]{1,0:T(8,128)(2,1)S(1)}, bf16[256,384]{1,0:T(8,128)(2,1)S(1)}, u32[]{:S(2)}, u32[]{:S(2)}) collective-permute-start(bf16[256,384]{1,0:T(8,128)(2,1)S(1)} %collective-permute-done.13.x2_ref), channel_id=1, source_target_pairs={{0,1},{1,0},{2,3},{3,2},{4,5},{5,4},{6,7},{7,6},{8,9},{9,8},{10,11... | collective-permute-start | bytes 589832 | tf_op jit(solution)/shard_map/ppermute | solution.py:44
  41.3 2.4 %shard_map.135.mine_ref = bf16[256,384]{1,0:T(8,128)(2,1)S(1)} custom-call(bf16[2048,256]{1,0:T(8,128)(2,1)S(1)} %get-tuple-element.55.k_ref, bf16[2,272,2048]{2,1,0:T(8,128)(2,1)S(1)} %get-tuple-element.56.v_ref, bf16[1536,256]{1,0:T(8,128)(2,1)S(1)} %get-tuple-element.46.q_ref, bf16[256,256]{1,0:T(8,128)(2,1)S(1)} %get-tuple-element.51.kc_ref, ...), custom_call_target="tpu_custom_call" | custom-call | flops 3000000000 | tf_op jit(solution)/shard_map/pallas_call | solution.py:704
  43.7 1.4 %shard_map.137.sum_ref = f32[384,2048]{1,0:T(8,128)S(1)} custom-call(bf16[1024,2048]{1,0:T(8,128)(2,1)S(1)} %copy-done.1, bf16[256,384]{1,0:T(8,128)(2,1)S(1)} %shard_map.135.mine_ref, bf16[256,384]{1,0:T(8,128)(2,1)S(1)} %collective-permute-done.11.neighbour_ref, bf16[256,384]{1,0:T(8,128)(2,1)S(1)} %collective-permute-done.12.x1_ref, ...), custom_call_target="tpu_custom_call" | custom-call | flops 2000000000 | tf_op jit(solution)/shard_map/pallas_call | solution.py:775
  45.2 1.6 %shard_map.138 = bf16[384,2048]{1,0:T(8,128)(2,1)} custom-call(bf16[1536,2048]{1,0:T(8,128)(2,1)S(1)} %copy-done, bf16[1024,2048]{1,0:T(8,128)(2,1)S(1)} %copy-done.1, f32[384,2048]{1,0:T(8,128)S(1)} %shard_map.137.sum_ref, bf16[256,384]{1,0:T(8,128)(2,1)S(1)} %collective-permute-done.14.one_ref, bf16[256,384]{1,0:T(8,128)(2,1)S(1)} %collective-permute-done.15.two_ref, ...), custom_call_target="tpu_custom_call" | custom-call | flops 2000000000 | tf_op jit(solution)/shard_map/pallas_call | solution.py:783
  (18 shorter events, 0.1 us)
Async XLA Ops:
  1.7 5.1 %collective-permute-start.2 = (f32[8,512]{1,0:T(8,128)S(1)}, f32[8,512]{1,0:T(8,128)S(1)}, u32[]{:S(2)}, u32[]{:S(2)}) collective-permute-start(f32[8,512]{1,0:T(8,128)S(1)} %get-tuple-element.33.token_ref.refs_0_), channel_id=1, source_target_pairs={{0,12},{4,8},{8,4},{12,0},{1,13},{5,9},{9,5},{13,1},{2,14},{6,10},... | collective-permute-start | bytes 49160 | tf_op jit(solution)/shard_map/ppermute | solution.py:44
  3.1 3.7 %collective-permute-start.1 = (f32[8,512]{1,0:T(8,128)S(1)}, f32[8,512]{1,0:T(8,128)S(1)}, u32[]{:S(2)}, u32[]{:S(2)}) collective-permute-start(f32[8,512]{1,0:T(8,128)S(1)} %get-tuple-element.33.token_ref.refs_0_), channel_id=1, source_target_pairs={{0,8},{4,12},{8,0},{12,4},{1,9},{5,13},{9,1},{13,5},{2,10},{6,14},... | collective-permute-start | bytes 49160 | tf_op jit(solution)/shard_map/ppermute | solution.py:44
  4.2 2.6 %collective-permute-start = (f32[8,512]{1,0:T(8,128)S(1)}, f32[8,512]{1,0:T(8,128)S(1)}, u32[]{:S(2)}, u32[]{:S(2)}) collective-permute-start(f32[8,512]{1,0:T(8,128)S(1)} %get-tuple-element.33.token_ref.refs_0_), channel_id=1, source_target_pairs={{0,4},{4,0},{8,12},{12,8},{1,5},{5,1},{9,13},{13,9},{2,6},{6,2},{1... | collective-permute-start | bytes 49160 | tf_op jit(solution)/shard_map/ppermute | solution.py:44
  5.3 7.5 %copy-start = (bf16[1536,2048]{1,0:T(8,128)(2,1)S(1)}, bf16[1536,2048]{1,0:T(8,128)(2,1)}, u32[]{:S(2)}) copy-start(bf16[1536,2048]{1,0:T(8,128)(2,1)} %x_ref.5) | copy-start | bytes 18874372
  6.8 6.0 %copy-start.2 = (bf16[64,2048]{1,0:T(8,128)(2,1)S(1)}, bf16[64,2048]{1,0:T(8,128)(2,1)}, u32[]{:S(2)}) copy-start(bf16[64,2048]{1,0:T(8,128)(2,1)} %context_ref.1) | copy-start | bytes 786436
  6.8 5.5 %collective-permute-start.5 = (f32[8,512]{1,0:T(8,128)S(1)}, f32[8,512]{1,0:T(8,128)S(1)}, u32[]{:S(2)}, u32[]{:S(2)}) collective-permute-start(f32[8,512]{1,0:T(8,128)S(1)} %shard_map.129.token_ref.rest_0_), channel_id=1, source_target_pairs={{0,3},{1,2},{2,1},{3,0},{4,7},{5,6},{6,5},{7,4},{8,11},{9,10},{10,... | collective-permute-start | bytes 49160 | tf_op jit(solution)/shard_map/ppermute | solution.py:44
  10.2 2.6 %collective-permute-start.4 = (f32[8,512]{1,0:T(8,128)S(1)}, f32[8,512]{1,0:T(8,128)S(1)}, u32[]{:S(2)}, u32[]{:S(2)}) collective-permute-start(f32[8,512]{1,0:T(8,128)S(1)} %shard_map.129.token_ref.rest_0_), channel_id=1, source_target_pairs={{0,2},{1,3},{2,0},{3,1},{4,6},{5,7},{6,4},{7,5},{8,10},{9,11},{10,... | collective-permute-start | bytes 49160 | tf_op jit(solution)/shard_map/ppermute | solution.py:44
  10.3 2.5 %collective-permute-start.3 = (f32[8,512]{1,0:T(8,128)S(1)}, f32[8,512]{1,0:T(8,128)S(1)}, u32[]{:S(2)}, u32[]{:S(2)}) collective-permute-start(f32[8,512]{1,0:T(8,128)S(1)} %shard_map.129.token_ref.rest_0_), channel_id=1, source_target_pairs={{0,1},{1,0},{2,3},{3,2},{4,5},{5,4},{6,7},{7,6},{8,9},{9,8},{10,11... | collective-permute-start | bytes 49160 | tf_op jit(solution)/shard_map/ppermute | solution.py:44
  14.8 12.6 %collective-permute-start.8 = (bf16[2,64,256]{2,1,0:T(8,128)(2,1)S(1)}, bf16[2,64,256]{2,1,0:T(8,128)(2,1)S(1)}, u32[]{:S(2)}, u32[]{:S(2)}) collective-permute-start(bf16[2,64,256]{2,1,0:T(8,128)(2,1)S(1)} %get-tuple-element.48.rest_0_), channel_id=1, source_target_pairs={{0,12},{4,8},{8,4},{12,0},{1,13},{5,9},{9,5},{13,1},{2,14},{6,10},... | collective-permute-start | bytes 196616 | tf_op jit(solution)/shard_map/ppermute | solution.py:44
  17.2 10.1 %collective-permute-start.7 = (bf16[2,64,256]{2,1,0:T(8,128)(2,1)S(1)}, bf16[2,64,256]{2,1,0:T(8,128)(2,1)S(1)}, u32[]{:S(2)}, u32[]{:S(2)}) collective-permute-start(bf16[2,64,256]{2,1,0:T(8,128)(2,1)S(1)} %get-tuple-element.48.rest_0_), channel_id=1, source_target_pairs={{0,8},{4,12},{8,0},{12,4},{1,9},{5,13},{9,1},{13,5},{2,10},{6,14},... | collective-permute-start | bytes 196616 | tf_op jit(solution)/shard_map/ppermute | solution.py:44
  18.8 8.6 %collective-permute-start.6 = (bf16[2,64,256]{2,1,0:T(8,128)(2,1)S(1)}, bf16[2,64,256]{2,1,0:T(8,128)(2,1)S(1)}, u32[]{:S(2)}, u32[]{:S(2)}) collective-permute-start(bf16[2,64,256]{2,1,0:T(8,128)(2,1)S(1)} %get-tuple-element.48.rest_0_), channel_id=1, source_target_pairs={{0,4},{4,0},{8,12},{12,8},{1,5},{5,1},{9,13},{13,9},{2,6},{6,2},{1... | collective-permute-start | bytes 196616 | tf_op jit(solution)/shard_map/ppermute | solution.py:44
  18.8 11.6 %collective-permute-start.9 = (bf16[2,256,256]{2,1,0:T(8,128)(2,1)S(1)}, bf16[2,256,256]{2,1,0:T(8,128)(2,1)S(1)}, u32[]{:S(2)}, u32[]{:S(2)}) collective-permute-start(bf16[2,256,256]{2,1,0:T(8,128)(2,1)S(1)} %get-tuple-element.53), channel_id=1, source_target_pairs={{0,4},{4,0},{8,12},{12,8},{1,5},{5,1},{9,13},{13,9},{2,6},{6,2},{1... | collective-permute-start | bytes 786440 | tf_op jit(solution)/shard_map/ppermute | solution.py:889
  20.2 10.2 %collective-permute-start.10 = (bf16[2,256,256]{2,1,0:T(8,128)(2,1)S(1)}, bf16[2,256,256]{2,1,0:T(8,128)(2,1)S(1)}, u32[]{:S(2)}, u32[]{:S(2)}) collective-permute-start(bf16[2,256,256]{2,1,0:T(8,128)(2,1)S(1)} %get-tuple-element.54), channel_id=1, source_target_pairs={{4,8},{8,4},{5,9},{9,5},{6,10},{10,6},{7,11},{11,7},{20,24},{24,20... | collective-permute-start | bytes 786440 | tf_op jit(solution)/shard_map/ppermute | solution.py:891
  29.8 8.6 %collective-permute-start.12 = (bf16[256,384]{1,0:T(8,128)(2,1)S(1)}, bf16[256,384]{1,0:T(8,128)(2,1)S(1)}, u32[]{:S(2)}, u32[]{:S(2)}) collective-permute-start(bf16[256,384]{1,0:T(8,128)(2,1)S(1)} %get-tuple-element.57), channel_id=1, source_target_pairs={{0,2},{1,3},{2,0},{3,1},{4,6},{5,7},{6,4},{7,5},{8,10},{9,11},{10,... | collective-permute-start | bytes 589832 | tf_op jit(solution)/shard_map/ppermute | solution.py:44
  32.8 6.3 %collective-permute-start.13 = (bf16[256,384]{1,0:T(8,128)(2,1)S(1)}, bf16[256,384]{1,0:T(8,128)(2,1)S(1)}, u32[]{:S(2)}, u32[]{:S(2)}) collective-permute-start(bf16[256,384]{1,0:T(8,128)(2,1)S(1)} %get-tuple-element.58), channel_id=1, source_target_pairs={{0,2},{1,3},{2,0},{3,1},{4,6},{5,7},{6,4},{7,5},{8,10},{9,11},{10,... | collective-permute-start | bytes 589832 | tf_op jit(solution)/shard_map/ppermute | solution.py:44
  36.1 7.6 %copy-start.1 = (bf16[1024,2048]{1,0:T(8,128)(2,1)S(1)}, bf16[1024,2048]{1,0:T(8,128)(2,1)}, u32[]{:S(2)}) copy-start(bf16[1024,2048]{1,0:T(8,128)(2,1)} %w_ref.3) | copy-start | bytes 12582916
  36.1 7.6 %collective-permute-start.11 = (bf16[256,384]{1,0:T(8,128)(2,1)S(1)}, bf16[256,384]{1,0:T(8,128)(2,1)S(1)}, u32[]{:S(2)}, u32[]{:S(2)}) collective-permute-start(bf16[256,384]{1,0:T(8,128)(2,1)S(1)} %shard_map.136), channel_id=1, source_target_pairs={{0,1},{1,0},{2,3},{3,2},{4,5},{5,4},{6,7},{7,6},{8,9},{9,8},{10,11... | collective-permute-start | bytes 589832 | tf_op jit(solution)/shard_map/ppermute | solution.py:44
  38.3 6.9 %collective-permute-start.14 = (bf16[256,384]{1,0:T(8,128)(2,1)S(1)}, bf16[256,384]{1,0:T(8,128)(2,1)S(1)}, u32[]{:S(2)}, u32[]{:S(2)}) collective-permute-start(bf16[256,384]{1,0:T(8,128)(2,1)S(1)} %collective-permute-done.12.x1_ref), channel_id=1, source_target_pairs={{0,1},{1,0},{2,3},{3,2},{4,5},{5,4},{6,7},{7,6},{8,9},{9,8},{10,11... | collective-permute-start | bytes 589832 | tf_op jit(solution)/shard_map/ppermute | solution.py:44
  39.2 6.0 %collective-permute-start.15 = (bf16[256,384]{1,0:T(8,128)(2,1)S(1)}, bf16[256,384]{1,0:T(8,128)(2,1)S(1)}, u32[]{:S(2)}, u32[]{:S(2)}) collective-permute-start(bf16[256,384]{1,0:T(8,128)(2,1)S(1)} %collective-permute-done.13.x2_ref), channel_id=1, source_target_pairs={{0,1},{1,0},{2,3},{3,2},{4,5},{5,4},{6,7},{7,6},{8,9},{9,8},{10,11... | collective-permute-start | bytes 589832 | tf_op jit(solution)/shard_map/ppermute | solution.py:44
